TPU v7x, 32 devices: a whole 2x2x4 slice. The times are simulated.
32 devices in a mesh: ep: 16 (over z, y, core), tp: 2 (over x).
Axes of the slice: x: 2, y: 2, z: 4, core: 2. Of those that a mesh axis runs over, the one named last changes fastest.
Arguments:
- tokens: bfloat16 [128, 1024], P('ep'), may hold values from -6 to 6
- ssm_state: float32 [128, 32, 64, 128], P('ep', 'tp'), may hold values from -6 to 6
- conv_x: bfloat16 [128, 3, 2048], P('ep', None, 'tp'), may hold values from -6 to 6
- conv_b: bfloat16 [128, 3, 1024], P('ep', None, 'tp'), may hold values from -6 to 6
- conv_c: bfloat16 [128, 3, 1024], P('ep', None, 'tp'), may hold values from -6 to 6
- w_x: bfloat16 [1024, 2048], P(None, 'tp'), may hold values from -0.1875 to 0.1875
- w_z: bfloat16 [1024, 2048], P(None, 'tp'), may hold values from -0.1875 to 0.1875
- w_b: bfloat16 [1024, 1024], P(None, 'tp'), may hold values from -0.1875 to 0.1875
- w_c: bfloat16 [1024, 1024], P(None, 'tp'), may hold values from -0.1875 to 0.1875
- w_dt: bfloat16 [1024, 32], replicated, may hold values from -0.1875 to 0.1875
- dt_bias: float32 [32], P('tp'), may hold values from -2 to 1
- a_log: float32 [32], P('tp'), may hold values from -3 to 1
- d_skip: float32 [32], P('tp'), may hold values from 0.1 to 1.9
- taps_x: bfloat16 [4, 2048], P(None, 'tp'), may hold values from -3 to 3
- taps_b: bfloat16 [4, 1024], P(None, 'tp'), may hold values from -3 to 3
- taps_c: bfloat16 [4, 1024], P(None, 'tp'), may hold values from -3 to 3
- norm1_gain: float32 [1024], replicated, may hold values from 0.1 to 1.9
- group_gain: float32 [2048], P('tp'), may hold values from 0.1 to 1.9
- w_out: bfloat16 [2048, 1024], P('tp'), may hold values from -0.125 to 0.125
- norm2_gain: float32 [1024], replicated, may hold values from 0.1 to 1.9
- route_ids: int32 [128, 6], P('ep'), may hold values from 0 to 15, all different within a row; in each aligned block of 8 rows (0 to 7, 8 to 15, ...) at most 6 rows name the same one
- route_weights: float32 [128, 6], P('ep'), may hold values from 0.1 to 1
- exp_gate: bfloat16 [16, 1024, 512], P('ep', None, 'tp'), may hold values from -0.1875 to 0.1875
- exp_up: bfloat16 [16, 1024, 512], P('ep', None, 'tp'), may hold values from -0.1875 to 0.1875
- exp_down: bfloat16 [16, 512, 1024], P('ep', 'tp'), may hold values from -0.25 to 0.25
- dense_gate: bfloat16 [1024, 1024], P('ep', 'tp'), may hold values from -0.1875 to 0.1875
- dense_up: bfloat16 [1024, 1024], P('ep', 'tp'), may hold values from -0.1875 to 0.1875
- dense_down: bfloat16 [1024, 1024], P('tp', 'ep'), may hold values from -0.1875 to 0.1875
- branch_gate: bfloat16 [1024], replicated, may hold values from -0.375 to 0.375
Outputs:
- mixed: bfloat16 [128, 1024], P('ep', 'tp')
- state_next: float32 [128, 32, 64, 128], P('ep', 'tp')
- conv_x_next: bfloat16 [128, 3, 2048], P('ep', None, 'tp')
- conv_b_next: bfloat16 [128, 3, 1024], P('ep', None, 'tp')
- conv_c_next: bfloat16 [128, 3, 1024], P('ep', None, 'tp')
Inputs may be any that keep to these rules, and one draw needn't show every extreme that they name: `route_ids`: each row names 6 different experts. Among the rows of one device no expert is named by more than 6 rows, a bound that some block reaches.
All inputs are finite; a program needn't handle non-finite values.
Results may differ from a plain program's by a relative error of at most 0.019.
Values may be sent and summed in bfloat16 or wider, within the bound.
No kernel may reach another device: no remote copies, remote signals or barrier semaphores. Data moves between devices by JAX's collectives and lax.ppermute only.
A program may use at most 64 MiB of HBM per device.

v0:
```python
import jax
import jax.numpy as jnp
from jax import lax
from jax.sharding import PartitionSpec as P

epsilon = 1e-06


def rms_rows(values, gain):
    return values * lax.rsqrt(jnp.mean(values * values, axis=-1, keepdims=True) + epsilon) * gain


def short_conv(previous, fresh, taps):
    window = jnp.concatenate((previous, fresh[:, None]), axis=1)
    summed = jnp.sum(window.astype(jnp.float32) * taps.astype(jnp.float32)[None], axis=1)
    return (jax.nn.silu(summed), window[:, 1:])


def mixer_core(
    x_new,
    z_new,
    b_new,
    c_new,
    dt_raw,
    ssm_state,
    conv_x,
    conv_b,
    conv_c,
    dt_bias,
    a_log,
    d_skip,
    taps_x,
    taps_b,
    taps_c,
    group_gain,
):
    seqs, heads, head_dim, state_dim = ssm_state.shape
    groups = b_new.shape[1] // state_dim
    x_conv, conv_x_next = short_conv(conv_x, x_new, taps_x)
    b_conv, conv_b_next = short_conv(conv_b, b_new, taps_b)
    c_conv, conv_c_next = short_conv(conv_c, c_new, taps_c)
    x_heads = x_conv.reshape(seqs, heads, head_dim)
    b_heads = jnp.repeat(b_conv.reshape(seqs, groups, state_dim), heads // groups, axis=1)
    c_heads = jnp.repeat(c_conv.reshape(seqs, groups, state_dim), heads // groups, axis=1)
    step = jax.nn.softplus(dt_raw + dt_bias)
    decay = jnp.exp(-step * jnp.exp(a_log))
    state_next = (
        decay[:, :, None, None] * ssm_state
        + (step[:, :, None] * x_heads)[:, :, :, None] * b_heads[:, :, None, :]
    )
    readout = (
        jnp.einsum("shpn,shn->shp", state_next, c_heads, precision=lax.Precision.HIGHEST)
        + d_skip[None, :, None] * x_heads
    )
    gated = readout.reshape(seqs, heads * head_dim) * jax.nn.silu(z_new.astype(jnp.float32))
    grouped = gated.reshape(seqs, groups, -1)
    grouped = grouped * lax.rsqrt(jnp.mean(grouped * grouped, axis=-1, keepdims=True) + epsilon)
    mixed_heads = (grouped.reshape(seqs, heads * head_dim) * group_gain).astype(jnp.bfloat16)
    return (mixed_heads, state_next, conv_x_next, conv_b_next, conv_c_next)


def body(
    tokens,
    ssm_state,
    conv_x,
    conv_b,
    conv_c,
    w_x,
    w_z,
    w_b,
    w_c,
    w_dt,
    dt_bias,
    a_log,
    d_skip,
    taps_x,
    taps_b,
    taps_c,
    norm1_gain,
    group_gain,
    w_out,
    norm2_gain,
    route_ids,
    route_weights,
    exp_gate,
    exp_up,
    exp_down,
    dense_gate,
    dense_up,
    dense_down,
    branch_gate,
):
    seqs = tokens.shape[0]
    model_width = tokens.shape[1]
    stream = tokens.astype(jnp.float32)
    normed = rms_rows(stream, norm1_gain).astype(jnp.bfloat16)
    x_proj = jnp.dot(normed, w_x, preferred_element_type=jnp.float32).astype(jnp.bfloat16)
    z_proj = jnp.dot(normed, w_z, preferred_element_type=jnp.float32).astype(jnp.bfloat16)
    b_proj = jnp.dot(normed, w_b, preferred_element_type=jnp.float32).astype(jnp.bfloat16)
    c_proj = jnp.dot(normed, w_c, preferred_element_type=jnp.float32).astype(jnp.bfloat16)
    local_heads = ssm_state.shape[1]
    dt_columns = lax.dynamic_slice_in_dim(w_dt, lax.axis_index("tp") * local_heads, local_heads, 1)
    dt_raw = jnp.dot(normed, dt_columns, preferred_element_type=jnp.float32)
    mixed_heads, state_next, conv_x_next, conv_b_next, conv_c_next = mixer_core(
        x_proj,
        z_proj,
        b_proj,
        c_proj,
        dt_raw,
        ssm_state,
        conv_x,
        conv_b,
        conv_c,
        dt_bias,
        a_log,
        d_skip,
        taps_x,
        taps_b,
        taps_c,
        group_gain,
    )
    partial_out = jnp.dot(mixed_heads, w_out, preferred_element_type=jnp.float32)
    quarter = model_width // lax.axis_size("tp")
    column = lax.axis_index("tp") * quarter
    summed = lax.psum(partial_out.astype(jnp.bfloat16), "tp").astype(jnp.float32)
    residual = (stream + summed).astype(jnp.bfloat16)
    normed2 = rms_rows(residual.astype(jnp.float32), norm2_gain).astype(jnp.bfloat16)
    own_rows = lax.dynamic_slice_in_dim(residual, column, quarter, 1)
    experts_all = lax.axis_size("ep") * exp_gate.shape[0]
    top_count = route_ids.shape[1]
    capacity = min(seqs, max(2, 2 * seqs * top_count // experts_all))
    expert_iota = jnp.arange(experts_all, dtype=jnp.int32)
    matches = route_ids[:, :, None] == expert_iota[None, None, :]
    routed = jnp.sum(matches.astype(jnp.int32), axis=1)
    weight_of = jnp.sum(jnp.where(matches, route_weights[:, :, None], jnp.float32(0.0)), axis=1)
    ranked = jnp.cumsum(routed, axis=0) - routed
    slot_iota = jnp.arange(capacity, dtype=jnp.int32)
    slot_onehot = routed[:, :, None] * (ranked[:, :, None] == slot_iota[None, None, :]).astype(
        jnp.int32
    )
    dispatch = slot_onehot.reshape(seqs, experts_all * capacity).astype(jnp.bfloat16)
    outgoing = jnp.einsum(
        "sk,sd->kd", dispatch, normed2, preferred_element_type=jnp.float32
    ).astype(jnp.bfloat16)
    outgoing = outgoing.reshape(experts_all, capacity, model_width)
    arrived = lax.all_to_all(outgoing, "ep", split_axis=0, concat_axis=0, tiled=True)
    arrived_rows = arrived.reshape(-1, model_width)
    gate_pre = jnp.dot(arrived_rows, exp_gate[0], preferred_element_type=jnp.float32)
    up_pre = jnp.dot(arrived_rows, exp_up[0], preferred_element_type=jnp.float32)
    active = (jax.nn.silu(gate_pre) * up_pre).astype(jnp.bfloat16)
    expert_partial = jnp.dot(active, exp_down[0], preferred_element_type=jnp.float32)
    expert_part = lax.psum_scatter(
        expert_partial.astype(jnp.bfloat16), "tp", scatter_dimension=1, tiled=True
    )
    returned = lax.all_to_all(
        expert_part.reshape(-1, capacity, quarter), "ep", split_axis=0, concat_axis=0, tiled=True
    )
    combine = (weight_of[:, :, None] * slot_onehot.astype(jnp.float32)).reshape(
        seqs, experts_all * capacity
    )
    expert_sum = jnp.dot(
        combine,
        returned.reshape(experts_all * capacity, quarter).astype(jnp.float32),
        precision=lax.Precision.HIGHEST,
    )
    hidden_width = dense_gate.shape[1]
    spread = lax.all_to_all(normed2, "ep", split_axis=1, concat_axis=0, tiled=True)
    stacked = jnp.concatenate((dense_gate, dense_up), axis=1)
    joined = lax.psum_scatter(
        jnp.dot(spread, stacked, preferred_element_type=jnp.float32),
        "ep",
        scatter_dimension=0,
        tiled=True,
    )
    dense_active = (jax.nn.silu(joined[:, :hidden_width]) * joined[:, hidden_width:]).astype(
        jnp.bfloat16
    )
    every_active = lax.all_gather(dense_active, "ep", axis=0, tiled=True)
    column_part = jnp.dot(every_active, dense_down, preferred_element_type=jnp.float32).astype(
        jnp.bfloat16
    )
    dense_partial = lax.all_to_all(
        column_part, "ep", split_axis=0, concat_axis=1, tiled=True
    ).astype(jnp.float32)
    dense_out = lax.psum_scatter(
        dense_partial.astype(jnp.bfloat16), "tp", scatter_dimension=1, tiled=True
    ).astype(jnp.float32)
    branch = jax.nn.sigmoid(
        jnp.dot(normed2, branch_gate[:, None], preferred_element_type=jnp.float32)
    )
    mixed = (own_rows.astype(jnp.float32) + expert_sum + branch * dense_out).astype(jnp.bfloat16)
    return (mixed, state_next, conv_x_next, conv_b_next, conv_c_next)


def solution(mesh):
    return jax.shard_map(
        body,
        mesh=mesh,
        in_specs=(
            P("ep", None),
            P("ep", "tp", None, None),
            P("ep", None, "tp"),
            P("ep", None, "tp"),
            P("ep", None, "tp"),
            P(None, "tp"),
            P(None, "tp"),
            P(None, "tp"),
            P(None, "tp"),
            P(),
            P("tp"),
            P("tp"),
            P("tp"),
            P(None, "tp"),
            P(None, "tp"),
            P(None, "tp"),
            P(),
            P("tp"),
            P("tp", None),
            P(),
            P("ep", None),
            P("ep", None),
            P("ep", None, "tp"),
            P("ep", None, "tp"),
            P("ep", "tp", None),
            P("ep", "tp"),
            P("ep", "tp"),
            P("tp", "ep"),
            P(),
        ),
        out_specs=(
            P("ep", "tp"),
            P("ep", "tp", None, None),
            P("ep", None, "tp"),
            P("ep", None, "tp"),
            P("ep", None, "tp"),
        ),
        check_vma=False,
    )
```

profile of v0, /device:TPU:0, one launch (start us, length us, event | category | flops | bytes accessed | tf_op | source)
XLA Modules:
  0.0 177.8 jit_solution(14721564418474552331)
XLA Ops:
  7.3 1.0 fusion.32
  8.9 0.7 convert_element_type.98
  9.6 2.0 %fusion.2 = bf16[8,1,1024]{2,0,1:T(8,128)(2,1)S(1)} fusion(bf16[1024,1024]{1,0:T(8,128)(2,1)} %param.34, bf16[8,1024]{1,0:T(8,128)(2,1)} %param.29, f32[1024]{0:T(1024)} %param.45, f32[8]{0:T(128)S(1)} %add_rsqrt_fusion.2), kind=kOutput, calls=%fused_computation.10 | convolution fusion | flops 16818176 | bytes 2134048 | tf_op jit(solution)/shard_map/dot_general | solution.py:97
  11.7 0.8 multiply_reduce_fusion
  12.6 1.5 fusion.6
  14.8 0.7 multiply_reduce_fusion.2
  15.6 1.5 fusion.7
  17.6 3.8 %multiply_add_fusion = f32[8,16,64,128]{3,2,1,0:T(8,128)S(1)} fusion(f32[8,16,64,128]{3,2,1,0:T(8,128)} %param.30, f32[8,16,128]{2,1,0:T(8,128)S(1)} %bitcast.75, f32[8,16,64]{2,1,0:T(8,128)S(1)} %broadcast_multiply_fusion, f32[8,16]{1,0:T(8,128)S(1)} %get-tuple-element.7), kind=kLoop, calls=%fused_computation | loop fusion | flops 3145728 | bytes 8487424 | tf_op jit(solution)/shard_map/add | solution.py:48
  21.4 2.0 %copy-done.1 = f32[8,16,64,128]{3,2,1,0:T(8,128)} copy-done((f32[8,16,64,128]{3,2,1,0:T(8,128)}, f32[8,16,64,128]{3,2,1,0:T(8,128)S(1)}, u32[]{:S(2)}) %copy-start.1) | copy-done | bytes 4194328
  23.4 6.6 %fusion.58 = f32[8,16,1,64]{3,2,1,0:T(1,128)S(1)} fusion(f32[8,16,64,128]{3,2,1,0:T(8,128)S(1)} %multiply_add_fusion, f32[8,16,128,1]{2,3,1,0:T(1,128)S(1)} %bitcast.76), kind=kOutput, calls=%fused_computation.99 | convolution fusion | flops 12582912 | bytes 4292608 | tf_op jit(solution)/shard_map/shpn,shn->shp/dot_general | solution.py:52
  30.8 2.0 %convolution_convert_fusion.3 = bf16[8,1024]{1,0:T(8,128)(2,1)S(1)} fusion(bf16[1024,1024]{1,0:T(8,128)(2,1)} %param.47, f32[8,1024]{1,0:T(8,128)S(1)} %get-tuple-element.10, f32[8,1024]{1,0:T(8,128)S(1)} %bitcast.78, f32[1024]{0:T(1024)S(1)} %copy-done.11), kind=kOutput, calls=%fused_computation.6 | convolution fusion | flops 16809984 | bytes 2183168 | tf_op jit(solution)/shard_map/dot_general | solution.py:122
  32.8 9.8 %psum.7 = bf16[8,1024]{1,0:T(8,128)(2,1)S(1)} all-reduce(bf16[8,1024]{1,0:T(8,128)(2,1)S(1)} %convolution_convert_fusion.3), channel_id=1, replica_groups=mesh['ep'=16,'tp'=2] {'tp'}, use_global_device_ids=true, to_apply=%region_5.6 | all-reduce | flops 8192 | bytes 32768 | tf_op jit(solution)/shard_map/psum | solution.py:125
  43.0 0.7 reshape.127
  43.7 5.9 %all-to-all-start.2 = ((bf16[16,2,256]{2,1,0:T(2,128)(2,1)}), bf16[16,2,256]{2,1,0:T(2,128)(2,1)S(1)}, u32[]{:S(2)}, u32[]{:S(2)}) async-start(bf16[16,2,256]{2,1,0:T(2,128)(2,1)} %reshape.127), calls=%async_computation.3 | async-start | bytes 32768 | tf_op jit(solution)/shard_map/all_to_all | solution.py:167
  50.5 0.8 reshape.119
  51.3 4.7 %all-to-all-done.2 = bf16[16,2,256]{2,1,0:T(2,128)(2,1)S(1)} async-done(((bf16[16,2,256]{2,1,0:T(2,128)(2,1)}), bf16[16,2,256]{2,1,0:T(2,128)(2,1)S(1)}, u32[]{:S(2)}, u32[]{:S(2)}) %all-to-all-start.2) | async-done | bytes 16416 | tf_op jit(solution)/shard_map/all_to_all | solution.py:167
  56.1 3.5 %all-to-all-start = ((bf16[16,6,1024]{2,1,0:T(8,128)(2,1)}), bf16[16,6,1024]{2,1,0:T(8,128)(2,1)S(1)}, u32[]{:S(2)}, u32[]{:S(2)}) async-start(bf16[16,6,1024]{2,1,0:T(8,128)(2,1)} %reshape.119), calls=%async_computation | async-start | bytes 524288 | tf_op jit(solution)/shard_map/all_to_all | solution.py:146
  59.8 1.0 fusion.17
  61.1 8.5 %all-to-all-done = bf16[16,6,1024]{2,1,0:T(8,128)(2,1)S(1)} async-done(((bf16[16,6,1024]{2,1,0:T(8,128)(2,1)}), bf16[16,6,1024]{2,1,0:T(8,128)(2,1)S(1)}, u32[]{:S(2)}, u32[]{:S(2)}) %all-to-all-start) | async-done | bytes 196640 | tf_op jit(solution)/shard_map/all_to_all | solution.py:146
  69.6 1.3 fusion.15
  70.9 2.2 %convolution_convert_fusion = bf16[96,1024]{1,0:T(8,128)(2,1)} fusion(bf16[96,1024]{1,0:T(8,128)(2,1)S(1)} %reshape.120, bf16[1,256,1024]{2,1,0:T(8,128)(2,1)S(1)} %copy-done.3, bf16[1,1024,256]{2,1,0:T(8,128)(2,1)} %param.52, f32[96,256]{1,0:T(8,128)S(1)} %fusion.15), kind=kOutput, calls=%fused_computation.1 | convolution fusion | flops 100909056 | bytes 1540096 | tf_op jit(solution)/shard_map/dot_general | solution.py:151
  73.2 47.3 %reduce-scatter.6.cloned.1.call-done = f32[8,1024]{1,0:T(8,128)} async-done(((f32[128,1024]{1,0:T(8,128)}), f32[8,1024]{1,0:T(8,128)}) %reduce-scatter.6.cloned.1.call-update) | async-done | bytes 32784 | tf_op jit(solution)/shard_map/reduce_scatter | solution.py:169
  120.5 0.7 fusion.40
  121.3 19.8 %all_gather.3 = bf16[128,512]{1,0:T(8,128)(2,1)S(1)} all-gather(bf16[8,512]{1,0:T(8,128)(2,1)S(1)} %fusion.40), channel_id=1, replica_groups=mesh['ep'=16,'tp'=2] {'ep'}, dimensions={0}, use_global_device_ids=true | all-gather | bytes 139264 | tf_op jit(solution)/shard_map/all_gather | solution.py:178
  141.3 0.7 reshape.129
  142.0 3.5 %all-to-all-start.3 = ((bf16[16,2,256]{2,1,0:T(2,128)(2,1)}), bf16[16,2,256]{2,1,0:T(2,128)(2,1)S(1)}, u32[]{:S(2)}, u32[]{:S(2)}) async-start(bf16[16,2,256]{2,1,0:T(2,128)(2,1)} %reshape.129), calls=%async_computation.5 | async-start | bytes 32768 | tf_op jit(solution)/shard_map/all_to_all | solution.py:182
  145.7 1.6 reshape.121
  147.2 4.7 %all-to-all-done.3 = bf16[16,2,256]{2,1,0:T(2,128)(2,1)S(1)} async-done(((bf16[16,2,256]{2,1,0:T(2,128)(2,1)}), bf16[16,2,256]{2,1,0:T(2,128)(2,1)S(1)}, u32[]{:S(2)}, u32[]{:S(2)}) %all-to-all-start.3) | async-done | bytes 16416 | tf_op jit(solution)/shard_map/all_to_all | solution.py:182
  152.0 3.5 %all-to-all-start.1 = ((bf16[16,6,512]{2,1,0:T(8,128)(2,1)}), bf16[16,6,512]{2,1,0:T(8,128)(2,1)S(1)}, u32[]{:S(2)}, u32[]{:S(2)}) async-start(bf16[16,6,512]{2,1,0:T(8,128)(2,1)} %reshape.121), calls=%async_computation.2 | async-start | bytes 262144 | tf_op jit(solution)/shard_map/all_to_all | solution.py:155
  156.3 0.7 all_to_all.43
  157.8 12.0 %reduce-scatter.8.cloned.1.call-done = bf16[8,512]{1,0:T(8,128)(2,1)} async-done(((bf16[8,1024]{1,0:T(8,128)(2,1)}), bf16[8,512]{1,0:T(8,128)(2,1)}) %reduce-scatter.8.cloned.1.call-update) | async-done | bytes 8208 | tf_op jit(solution)/shard_map/reduce_scatter | solution.py:185
  169.8 1.5 fusion.5
  (97 shorter events, 6.4 us)
Async XLA Ops:
  7.2 23.0 %copy-start = (bf16[1024,1024]{1,0:T(8,128)(2,1)S(1)}, bf16[1024,1024]{1,0:T(8,128)(2,1)}, u32[]{:S(2)}) copy-start(bf16[1024,1024]{1,0:T(8,128)(2,1)} %param.35) | copy-start | bytes 6291460
  7.2 10.0 %copy-start.2 = (bf16[8,1024]{1,0:T(8,128)(2,1)S(1)}, bf16[8,1024]{1,0:T(8,128)(2,1)}, u32[]{:S(2)}) copy-start(bf16[8,1024]{1,0:T(8,128)(2,1)} %param.29) | copy-start | bytes 49156
  7.2 10.0 %copy-start.7 = (f32[1024]{0:T(1024)S(1)}, f32[1024]{0:T(1024)}, u32[]{:S(2)}) copy-start(f32[1024]{0:T(1024)} %param.45) | copy-start | bytes 12292
  7.2 9.9 %copy-start.12 = (bf16[4,512]{1,0:T(4,128)(2,1)S(1)}, bf16[4,512]{1,0:T(4,128)(2,1)}, u32[]{:S(2)}) copy-start(bf16[4,512]{1,0:T(4,128)(2,1)} %param.44) | copy-start | bytes 12292
  7.2 9.9 %copy-start.6 = (bf16[8,3,512]{2,0,1:T(8,128)(2,1)S(1)}, bf16[8,3,512]{2,0,1:T(8,128)(2,1)}, u32[]{:S(2)}) copy-start(bf16[8,3,512]{2,0,1:T(8,128)(2,1)} %param.33) | copy-start | bytes 73732
  7.2 10.0 %copy-start.18 = (bf16[1024,32]{0,1:T(8,128)(2,1)S(1)}, bf16[1024,32]{0,1:T(8,128)(2,1)}, u32[]{:S(2)}) copy-start(bf16[1024,32]{0,1:T(8,128)(2,1)} %param.38) | copy-start | bytes 196612
  7.2 10.0 %copy-start.19 = (f32[16]{0:T(128)S(1)}, f32[16]{0:T(128)}, u32[]{:S(2)}) copy-start(f32[16]{0:T(128)} %param.39) | copy-start | bytes 196
  21.4 2.0 %copy-start.1 = (f32[8,16,64,128]{3,2,1,0:T(8,128)}, f32[8,16,64,128]{3,2,1,0:T(8,128)S(1)}, u32[]{:S(2)}) copy-start(f32[8,16,64,128]{3,2,1,0:T(8,128)S(1)} %multiply_add_fusion) | copy-start | bytes 12582916
  21.4 8.6 %copy-start.17 = (f32[16]{0:T(128)S(1)}, f32[16]{0:T(128)}, u32[]{:S(2)}) copy-start(f32[16]{0:T(128)} %param.41) | copy-start | bytes 196
  21.4 9.4 %copy-start.11 = (f32[1024]{0:T(1024)S(1)}, f32[1024]{0:T(1024)}, u32[]{:S(2)}) copy-start(f32[1024]{0:T(1024)} %param.46) | copy-start | bytes 12292
  23.4 19.4 %copy-start.13 = (f32[1024]{0:T(1024)S(1)}, f32[1024]{0:T(1024)}, u32[]{:S(2)}) copy-start(f32[1024]{0:T(1024)} %param.48) | copy-start | bytes 12292
  23.4 26.2 %copy-start.14 = (s32[8,6]{1,0:T(8,128)S(1)}, s32[8,6]{1,0:T(8,128)}, u32[]{:S(2)}) copy-start(s32[8,6]{1,0:T(8,128)} %param.49) | copy-start | bytes 580
  23.4 27.8 %copy-start.15 = (f32[8,6]{1,0:T(8,128)S(1)}, f32[8,6]{1,0:T(8,128)}, u32[]{:S(2)}) copy-start(f32[8,6]{1,0:T(8,128)} %param.50) | copy-start | bytes 580
  30.0 29.8 %copy-start.9 = (bf16[64,512]{1,0:T(8,128)(2,1)S(1)}, bf16[64,512]{1,0:T(8,128)(2,1)}, u32[]{:S(2)}) copy-start(bf16[64,512]{1,0:T(8,128)(2,1)} %param.55) | copy-start | bytes 196612
  30.0 29.8 %copy-start.10 = (bf16[64,512]{1,0:T(8,128)(2,1)S(1)}, bf16[64,512]{1,0:T(8,128)(2,1)}, u32[]{:S(2)}) copy-start(bf16[64,512]{1,0:T(8,128)(2,1)} %param.54) | copy-start | bytes 196612
  30.0 30.9 %copy-start.16 = (bf16[1024]{0:T(1024)(128)(2,1)S(1)}, bf16[1024]{0:T(1024)(128)(2,1)}, u32[]{:S(2)}) copy-start(bf16[1024]{0:T(1024)(128)(2,1)} %param.57) | copy-start | bytes 6148
  30.2 40.7 %copy-start.3 = (bf16[1,256,1024]{2,1,0:T(8,128)(2,1)S(1)}, bf16[1,256,1024]{2,1,0:T(8,128)(2,1)}, u32[]{:S(2)}) copy-start(bf16[1,256,1024]{2,1,0:T(8,128)(2,1)} %param.53) | copy-start | bytes 1572868
  30.8 110.2 %copy-start.8 = (bf16[512,64]{0,1:T(8,128)(2,1)S(1)}, bf16[512,64]{0,1:T(8,128)(2,1)}, u32[]{:S(2)}) copy-start(bf16[512,64]{0,1:T(8,128)(2,1)} %param.56) | copy-start | bytes 196612
  32.8 122.8 %copy-start.5 = (bf16[8,3,512]{2,0,1:T(8,128)(2,1)S(1)}, bf16[8,3,512]{2,0,1:T(8,128)(2,1)}, u32[]{:S(2)}) copy-start(bf16[8,3,512]{2,0,1:T(8,128)(2,1)} %param.32) | copy-start | bytes 73732
  32.8 124.2 %copy-start.4 = (bf16[8,3,1024]{2,0,1:T(8,128)(2,1)S(1)}, bf16[8,3,1024]{2,0,1:T(8,128)(2,1)}, u32[]{:S(2)}) copy-start(bf16[8,3,1024]{2,0,1:T(8,128)(2,1)} %param.31) | copy-start | bytes 147460
  43.7 12.4 %all-to-all-start.2 = ((bf16[16,2,256]{2,1,0:T(2,128)(2,1)}), bf16[16,2,256]{2,1,0:T(2,128)(2,1)S(1)}, u32[]{:S(2)}, u32[]{:S(2)}) async-start(bf16[16,2,256]{2,1,0:T(2,128)(2,1)} %reshape.127), calls=%async_computation.3 | async-start | bytes 32768 | tf_op jit(solution)/shard_map/all_to_all | solution.py:167
  56.1 13.5 %all-to-all-start = ((bf16[16,6,1024]{2,1,0:T(8,128)(2,1)}), bf16[16,6,1024]{2,1,0:T(8,128)(2,1)S(1)}, u32[]{:S(2)}, u32[]{:S(2)}) async-start(bf16[16,6,1024]{2,1,0:T(8,128)(2,1)} %reshape.119), calls=%async_computation | async-start | bytes 524288 | tf_op jit(solution)/shard_map/all_to_all | solution.py:146
  59.6 60.9 %reduce-scatter.6.cloned.1.call-start = ((), (), s32[]{:S(2)}) async-start(), calls=%async_computation.8 | async-start | bytes 557056 | tf_op jit(solution)/shard_map/reduce_scatter | solution.py:169
  60.8 84.9 %reduce-scatter.4.cloned.1.call-start = ((), (), s32[]{:S(2)}) async-start(), calls=%async_computation.7 | async-start | bytes 294912 | tf_op jit(solution)/shard_map/reduce_scatter | solution.py:152
  142.0 10.0 %all-to-all-start.3 = ((bf16[16,2,256]{2,1,0:T(2,128)(2,1)}), bf16[16,2,256]{2,1,0:T(2,128)(2,1)S(1)}, u32[]{:S(2)}, u32[]{:S(2)}) async-start(bf16[16,2,256]{2,1,0:T(2,128)(2,1)} %reshape.129), calls=%async_computation.5 | async-start | bytes 32768 | tf_op jit(solution)/shard_map/all_to_all | solution.py:182
  152.0 17.8 %all-to-all-start.1 = ((bf16[16,6,512]{2,1,0:T(8,128)(2,1)}), bf16[16,6,512]{2,1,0:T(8,128)(2,1)S(1)}, u32[]{:S(2)}, u32[]{:S(2)}) async-start(bf16[16,6,512]{2,1,0:T(8,128)(2,1)} %reshape.121), calls=%async_computation.2 | async-start | bytes 262144 | tf_op jit(solution)/shard_map/all_to_all | solution.py:155
  155.5 14.2 %reduce-scatter.8.cloned.1.call-start = ((), (), s32[]{:S(2)}) async-start(), calls=%async_computation.9 | async-start | bytes 24576 | tf_op jit(solution)/shard_map/reduce_scatter | solution.py:185
Sparse Core Ops, SparseCore 0:
  64.0 56.5 reduce-scatter.5
  122.7 10.0 reduce-scatter.3
  158.5 11.1 reduce-scatter.7
where the time goes:
time: 179 us; the launch traced here: 178 us
  waiting for transfers between devices  77.3 us (43%)
  blocking collectives  29.6 us (17%)
  matrix products  20.9 us (12%)
  starting transfers between devices  16.5 us (9%)
  between operations  14.2 us (8%)
  other arithmetic  10.6 us (6%)
  local copies, waits for them, and re-layouts  8.7 us (5%)
    reduce_scatter x1, waiting for transfers between devices, body(): lax.psum_scatter(jnp.dot(spread, stacked, preferred_element_type=jnp.floa...  47.3 us
    all_gather x1, blocking collectives, body(): every_active = lax.all_gather(dense_active, 'ep', axis=0, tiled=True)  19.8 us
    reduce_scatter x1, waiting for transfers between devices, body(): lax.psum_scatter(dense_partial.astype(jnp.bfloat16), 'tp', scatter_dimens...  12 us
    psum x1, blocking collectives, body(): lax.psum(partial_out.astype(jnp.bfloat16), 'tp').astype(jnp.float32)  9.81 us
    all_to_all x1, waiting for transfers between devices, body(): lax.all_to_all(outgoing, 'ep', split_axis=0, concat_axis=0, tiled=True)  8.5 us
    dot_general x1, matrix products, mixer_core(): jnp.einsum('shpn,shn->shp', state_next, c_heads, precision=lax.Precision....  6.58 us
    all_to_all x1, starting transfers between devices, body(): lax.all_to_all(normed2, 'ep', split_axis=1, concat_axis=0, tiled=True)  5.88 us
    all_to_all x1, waiting for transfers between devices, body(): lax.all_to_all(column_part, 'ep', split_axis=0, concat_axis=1, tiled=True)  4.75 us
  transfers between devices with their start and end apart: 7, of which 5 were waited for; matrix products, arithmetic and copies ran while one was open for 6% of the time, Pallas kernels for 0%

commit v1 on v0

v1 whole, which is shorter than its diff:
```python
import functools
import math

import jax
import jax.numpy as jnp
from jax import lax
from jax.experimental import pallas as pl
from jax.experimental.pallas import tpu as pltpu
from jax.sharding import PartitionSpec as P

epsilon = 1e-06
f32 = jnp.float32
bf16 = jnp.bfloat16
VMEM = pl.BlockSpec(memory_space=pltpu.VMEM)
SMEM = pl.BlockSpec(memory_space=pltpu.SMEM)
HBM = pl.BlockSpec(memory_space=pltpu.HBM)
MIB = 1 << 20


def dot(left, right):
    return lax.dot_general(left, right, (((1,), (0,)), ((), ())), preferred_element_type=f32)


def dot_nt(left, right):
    return lax.dot_general(left, right, (((1,), (1,)), ((), ())), preferred_element_type=f32)


def silu(value):
    return value / (1.0 + jnp.exp(-value))


def sigmoid(value):
    return 1.0 / (1.0 + jnp.exp(-value))


def rms_rows(values, gain):
    return values * lax.rsqrt(jnp.mean(values * values, axis=-1, keepdims=True) + epsilon) * gain


def spread_heads(values, width):
    rows, heads = values.shape
    return jnp.concatenate(
        [jnp.broadcast_to(values[:, h : h + 1], (rows, width)) for h in range(heads)], axis=1
    )


def pack_kernel(gate_ref, up_ref, down_ref, ids_ref, weights_ref, out_ref, *, dests):
    rows, hidden = gate_ref.shape
    share = hidden // dests
    lanes = out_ref.shape[2]
    seqs, top_count = ids_ref.shape
    gate = gate_ref[...].astype(f32)
    up = up_ref[...].astype(f32)
    down = down_ref[...].astype(f32).T
    ids = ids_ref[...]
    weights = weights_ref[...]
    expert = lax.broadcasted_iota(jnp.int32, (seqs, dests), 1)
    weight_of = jnp.zeros((seqs, dests), f32)
    for k in range(top_count):
        weight_of += jnp.where(ids[:, k : k + 1] == expert, weights[:, k : k + 1], 0.0)
    high = weight_of.astype(bf16).astype(f32)
    low = weight_of - high
    if rows > seqs:
        rest = jnp.zeros((rows - seqs, dests), f32)
        high = jnp.concatenate((high, rest), axis=0)
        low = jnp.concatenate((low, rest), axis=0)
    for j in range(dests):
        part = slice(j * share, (j + 1) * share)
        block = [gate[:, part], up[:, part], down[:, part], high[:, j : j + 1], low[:, j : j + 1]]
        spare = lanes - 3 * share - 2
        if spare:
            block.append(jnp.zeros((rows, spare), f32))
        out_ref[j] = jnp.concatenate(block, axis=1).astype(bf16)


def mixer_kernel(
    tp_ref,
    tokens_ref,
    gain_ref,
    w_dt_ref,
    dt_bias_ref,
    a_log_ref,
    d_skip_ref,
    taps_x_ref,
    taps_b_ref,
    taps_c_ref,
    group_gain_ref,
    conv_x_ref,
    conv_b_ref,
    conv_c_ref,
    w_x_hbm,
    w_z_hbm,
    w_b_hbm,
    w_c_hbm,
    w_out_hbm,
    state_hbm,
    part_ref,
    conv_x_out,
    conv_b_out,
    conv_c_out,
    state_out,
    w_x,
    w_z,
    w_b,
    w_c,
    w_out,
    state,
    in_sems,
    state_sems,
    out_sems,
    *,
    n_tp,
):
    seqs, heads, head_dim, state_dim = state.shape
    channels = heads * head_dim
    groups = w_b.shape[1] // state_dim
    per_group = heads // groups
    width = channels // groups
    copy = pltpu.make_async_copy
    moves = {}
    for index, (name, source, target) in enumerate(
        (("x", w_x_hbm, w_x), ("b", w_b_hbm, w_b), ("c", w_c_hbm, w_c))
    ):
        moves[name] = copy(source, target, in_sems.at[index])
        moves[name].start()
    loads = [copy(state_hbm.at[s], state.at[s], state_sems.at[s]) for s in range(seqs)]
    stores = [copy(state.at[s], state_out.at[s], out_sems.at[s]) for s in range(seqs)]
    for load in loads:
        load.start()
    for index, (name, source, target) in enumerate((("z", w_z_hbm, w_z), ("o", w_out_hbm, w_out))):
        moves[name] = copy(source, target, in_sems.at[3 + index])
        moves[name].start()

    normed = rms_rows(tokens_ref[...].astype(f32), gain_ref[...]).astype(bf16)
    dt_all = dot(normed, w_dt_ref[...])
    own = tp_ref[0]
    dt_raw = jnp.zeros((seqs, heads), f32)
    for i in range(n_tp):
        dt_raw += jnp.where(own == i, dt_all[:, i * heads : (i + 1) * heads], 0.0)
    shifted = dt_raw + dt_bias_ref[...]
    step = jnp.maximum(shifted, 0.0) + jnp.log1p(jnp.exp(-jnp.abs(shifted)))
    decay = jnp.exp(-step * jnp.exp(a_log_ref[...]))

    def short_conv(previous_ref, fresh, taps_ref, out_ref):
        previous = previous_ref[...].astype(f32)
        taps = taps_ref[...].astype(f32)
        last = taps.shape[0] - 1
        total = jnp.sum(previous * taps[None, :last], axis=1) + fresh * taps[last:]
        out_ref[...] = jnp.concatenate((previous[:, 1:], fresh[:, None]), axis=1).astype(bf16)
        return silu(total)

    def projected(name, ref):
        moves[name].wait()
        return dot(normed, ref[...]).astype(bf16).astype(f32)

    xs = short_conv(conv_x_ref, projected("x", w_x), taps_x_ref, conv_x_out)
    bs = short_conv(conv_b_ref, projected("b", w_b), taps_b_ref, conv_b_out)
    cs = short_conv(conv_c_ref, projected("c", w_c), taps_c_ref, conv_c_out).astype(bf16)
    scaled = (spread_heads(step, head_dim) * xs).T
    row = lax.broadcasted_iota(jnp.int32, (seqs, width), 0)
    readout = [jnp.zeros((seqs, width), f32) for _ in range(groups)]
    for s in range(seqs):
        loads[s].wait()
        for g in range(groups):
            key = bs[s : s + 1, g * state_dim : (g + 1) * state_dim]
            fresh = []
            for h in range(g * per_group, (g + 1) * per_group):
                column = scaled[h * head_dim : (h + 1) * head_dim, s : s + 1]
                updated = decay[s : s + 1, h : h + 1] * state[s, h] + column * key
                state[s, h] = updated
                fresh.append(updated.astype(bf16))
            read = dot_nt(
                cs[:, g * state_dim : (g + 1) * state_dim], jnp.concatenate(fresh, axis=0)
            )
            readout[g] = jnp.where(row == s, read, readout[g])
        stores[s].start()
    z_gate = silu(projected("z", w_z))
    skip = spread_heads(d_skip_ref[...], head_dim) * xs
    mixed = []
    for g in range(groups):
        part = slice(g * width, (g + 1) * width)
        gated = (readout[g] + skip[:, part]) * z_gate[:, part]
        mixed.append(rms_rows(gated, group_gain_ref[:, part]).astype(bf16))
    moves["o"].wait()
    part_ref[...] = dot(jnp.concatenate(mixed, axis=1), w_out[...]).astype(bf16)
    for store in stores:
        store.wait()


def norm_kernel(tokens_ref, own_ref, other_ref, gain_ref, spread_ref, residual_ref):
    seqs = tokens_ref.shape[0]
    summed = own_ref[...].astype(f32) + other_ref[...].astype(f32)
    residual = (tokens_ref[...].astype(f32) + summed).astype(bf16)
    residual_ref[...] = residual
    normed = rms_rows(residual.astype(f32), gain_ref[...]).astype(bf16)
    for j in range(spread_ref.shape[0] // seqs):
        spread_ref[j * seqs : (j + 1) * seqs] = normed


def experts_kernel(
    rows_ref, packed_ref, gate_ref, up_ref, down_ref, branch_ref, out_ref, *, share, seqs, n_tp
):
    blocks, block_rows, lanes = packed_ref.shape
    count, model = rows_ref.shape
    rows = rows_ref[...]
    active = (silu(dot(rows, gate_ref[0])) * dot(rows, up_ref[0])).astype(bf16)
    routed = dot(active, down_ref[0])
    packed = packed_ref[...].reshape(blocks * block_rows, lanes)
    hidden = dot(rows, packed)
    lane = lax.broadcasted_iota(jnp.int32, (count, lanes), 1)
    dense = silu(pltpu.roll(hidden, 2 * share, 1)) * pltpu.roll(hidden, share, 1)
    chosen = (lane >= 2 * share) & (lane < 3 * share)
    dense = jnp.where(chosen, dense, 0.0).astype(bf16)
    dense_out = dot_nt(dense, packed)
    branch = sigmoid(
        jnp.sum(rows.astype(f32) * branch_ref[...].astype(f32), axis=1, keepdims=True)
    )
    table = jnp.concatenate(
        [packed_ref[i, :seqs].astype(f32) for i in range(blocks)], axis=0
    )
    weight = jnp.sum(
        jnp.where((lane >= 3 * share) & (lane < 3 * share + 2), table, 0.0), axis=1, keepdims=True
    )
    result = weight * routed + branch * dense_out
    half = model // n_tp
    for j in range(blocks):
        for q in range(n_tp):
            place = (j * n_tp + q) * seqs
            out_ref[place : place + seqs] = result[
                j * seqs : (j + 1) * seqs, q * half : (q + 1) * half
            ].astype(bf16)


def sum_kernel(tp_ref, parts_ref, residual_ref, out_ref, *, n_tp):
    seqs, half = out_ref.shape
    own = tp_ref[0]
    total = jnp.zeros((seqs, half), f32)
    for q in range(n_tp):
        total += jnp.where(
            own == q, residual_ref[:, q * half : (q + 1) * half].astype(f32), 0.0
        )
    for i in range(parts_ref.shape[0] // seqs):
        total += parts_ref[i * seqs : (i + 1) * seqs].astype(f32)
    out_ref[...] = total.astype(bf16)


def body(
    tokens,
    ssm_state,
    conv_x,
    conv_b,
    conv_c,
    w_x,
    w_z,
    w_b,
    w_c,
    w_dt,
    dt_bias,
    a_log,
    d_skip,
    taps_x,
    taps_b,
    taps_c,
    norm1_gain,
    group_gain,
    w_out,
    norm2_gain,
    route_ids,
    route_weights,
    exp_gate,
    exp_up,
    exp_down,
    dense_gate,
    dense_up,
    dense_down,
    branch_gate,
):
    seqs, model = tokens.shape
    n_ep = lax.axis_size("ep")
    n_tp = lax.axis_size("tp")
    tp_index = lax.axis_index("tp").astype(jnp.int32)[None]
    sds = jax.ShapeDtypeStruct

    rows, hidden = dense_gate.shape
    share = hidden // n_ep
    lanes = 128 * math.ceil((3 * share + 2) / 128)
    packed = pl.pallas_call(
        functools.partial(pack_kernel, dests=n_ep),
        out_shape=sds((n_ep, rows, lanes), bf16),
        in_specs=[VMEM] * 5,
        out_specs=VMEM,
        name="pack",
    )(dense_gate, dense_up, dense_down, route_ids, route_weights)
    packed = lax.all_to_all(packed, "ep", split_axis=0, concat_axis=0, tiled=True)

    part, conv_x_next, conv_b_next, conv_c_next, state_next = pl.pallas_call(
        functools.partial(mixer_kernel, n_tp=n_tp),
        out_shape=(
            sds((seqs, model), bf16),
            sds(conv_x.shape, bf16),
            sds(conv_b.shape, bf16),
            sds(conv_c.shape, bf16),
            sds(ssm_state.shape, f32),
        ),
        in_specs=[SMEM] + [VMEM] * 13 + [HBM] * 6,
        out_specs=(VMEM, VMEM, VMEM, VMEM, HBM),
        scratch_shapes=[
            pltpu.VMEM(w_x.shape, bf16),
            pltpu.VMEM(w_z.shape, bf16),
            pltpu.VMEM(w_b.shape, bf16),
            pltpu.VMEM(w_c.shape, bf16),
            pltpu.VMEM(w_out.shape, bf16),
            pltpu.VMEM(ssm_state.shape, f32),
            pltpu.SemaphoreType.DMA((5,)),
            pltpu.SemaphoreType.DMA((seqs,)),
            pltpu.SemaphoreType.DMA((seqs,)),
        ],
        compiler_params=pltpu.CompilerParams(vmem_limit_bytes=30 * MIB),
        name="mixer",
    )(
        tp_index,
        tokens,
        norm1_gain[None],
        w_dt,
        dt_bias[None],
        a_log[None],
        d_skip[None],
        taps_x,
        taps_b,
        taps_c,
        group_gain[None],
        conv_x,
        conv_b,
        conv_c,
        w_x,
        w_z,
        w_b,
        w_c,
        w_out,
        ssm_state,
    )

    if n_tp == 2:
        other = lax.ppermute(part, "tp", [(0, 1), (1, 0)])
    else:
        gathered = lax.all_gather(part, "tp", axis=0).astype(f32)
        total = gathered[0]
        for i in range(1, n_tp):
            total = total + gathered[i]
        other = total - part.astype(f32)

    spread, residual = pl.pallas_call(
        norm_kernel,
        out_shape=(sds((n_ep * seqs, model), bf16), sds((seqs, model), bf16)),
        in_specs=[VMEM] * 4,
        out_specs=(VMEM, VMEM),
        name="norm",
    )(tokens, part, other, norm2_gain[None])
    everyone = lax.all_to_all(spread, "ep", split_axis=0, concat_axis=0, tiled=True)

    outgoing = pl.pallas_call(
        functools.partial(experts_kernel, share=share, seqs=seqs, n_tp=n_tp),
        out_shape=sds((n_ep * n_tp * seqs, model // n_tp), bf16),
        in_specs=[VMEM] * 6,
        out_specs=VMEM,
        name="experts",
    )(everyone, packed, exp_gate, exp_up, exp_down, branch_gate[None])
    parts = lax.all_to_all(outgoing, ("ep", "tp"), split_axis=0, concat_axis=0, tiled=True)

    mixed = pl.pallas_call(
        functools.partial(sum_kernel, n_tp=n_tp),
        out_shape=sds((seqs, model // n_tp), bf16),
        in_specs=[SMEM, VMEM, VMEM],
        out_specs=VMEM,
        name="total",
    )(tp_index, parts, residual)
    return (mixed, state_next, conv_x_next, conv_b_next, conv_c_next)


def solution(mesh):
    return jax.shard_map(
        body,
        mesh=mesh,
        in_specs=(
            P("ep", None),
            P("ep", "tp", None, None),
            P("ep", None, "tp"),
            P("ep", None, "tp"),
            P("ep", None, "tp"),
            P(None, "tp"),
            P(None, "tp"),
            P(None, "tp"),
            P(None, "tp"),
            P(),
            P("tp"),
            P("tp"),
            P("tp"),
            P(None, "tp"),
            P(None, "tp"),
            P(None, "tp"),
            P(),
            P("tp"),
            P("tp", None),
            P(),
            P("ep", None),
            P("ep", None),
            P("ep", None, "tp"),
            P("ep", None, "tp"),
            P("ep", "tp", None),
            P("ep", "tp"),
            P("ep", "tp"),
            P("tp", "ep"),
            P(),
        ),
        out_specs=(
            P("ep", "tp"),
            P("ep", "tp", None, None),
            P("ep", None, "tp"),
            P("ep", None, "tp"),
            P("ep", None, "tp"),
        ),
        check_vma=False,
    )
```

time: 179 us -> 78.5 us (0.44)
  waiting for transfers between devices: 77.3 us -> 20.4 us
  blocking collectives: 29.6 us -> 0 us
  matrix products: 20.9 us -> 0 us
  local copies, waits for them, and re-layouts: 8.7 us -> 23.8 us
  Pallas kernels: 0 us -> 14.5 us
  between operations: 14.2 us -> 0.75 us
  other arithmetic: 10.6 us -> 0 us
    reduce_scatter x3 -> x0, waiting for transfers between devices: 59.3 us -> none  [the longest x1 47.3 us: body(): lax.psum_scatter(jnp.dot(spread, stacked, preferred_element_type=jnp.floa...]
    dot_general x14 -> x0, matrix products: 20.9 us -> none  [the longest x1 6.58 us: mixer_core(): jnp.einsum('shpn,shn->shp', state_next, c_heads, precision=lax.Precision....]
    all_gather x1 -> x0, blocking collectives: 19.8 us -> none  [body(): every_active = lax.all_gather(dense_active, 'ep', axis=0, tiled=True)]
    unnamed x47 -> x50, local copies, waits for them, and re-layouts: 3.83 us -> 23.3 us
    pallas_call x0 -> x5, Pallas kernels: none -> 14.5 us  [the longest x1 6.21 us: body(): pl.pallas_call(functools.partial(mixer_kernel, n_tp=n_tp), out_shape=(sds...]
    psum x1 -> x0, blocking collectives: 9.81 us -> none  [body(): lax.psum(partial_out.astype(jnp.bfloat16), 'tp').astype(jnp.float32)]
    add x2 -> x0, other arithmetic: 3.86 us -> none  [the longest x1 3.79 us: mixer_core(): decay[:, :, None, None] * ssm_state]
    reduce_sum x8 -> x0, other arithmetic: 2.94 us -> none  [the longest x3 1.59 us: short_conv(): jnp.sum(window.astype(jnp.float32) * taps.astype(jnp.float32)[None], axis=1)]
  transfers between devices with their start and end apart: 7 -> 4, of which waited for: 5 -> 3; matrix products, arithmetic and copies ran while one was open for 6% -> 8% of each run, Pallas kernels for 0% -> 10%
where the time goes in v1:
time: 78.5 us; the launch traced here: 77.3 us
  local copies, waits for them, and re-layouts  23.8 us (30%)
  waiting for transfers between devices  20.4 us (26%)
  starting transfers between devices  17.8 us (23%)
  Pallas kernels  14.5 us (18%)
    unnamed x50, local copies, waits for them, and re-layouts  23.3 us
    all_to_all x1, waiting for transfers between devices, body(): lax.all_to_all(spread, 'ep', split_axis=0, concat_axis=0, tiled=True)  9.41 us
    all_to_all x1, waiting for transfers between devices, body(): lax.all_to_all(outgoing, ('ep', 'tp'), split_axis=0, concat_axis=0, tiled...  8.79 us
    all_to_all x1, starting transfers between devices, body(): lax.all_to_all(packed, 'ep', split_axis=0, concat_axis=0, tiled=True)  7.41 us
    pallas_call x1, Pallas kernels, body(): pl.pallas_call(functools.partial(mixer_kernel, n_tp=n_tp), out_shape=(sds...  6.21 us
    all_to_all x1, starting transfers between devices, body(): lax.all_to_all(spread, 'ep', split_axis=0, concat_axis=0, tiled=True)  6.01 us
    pallas_call x1, Pallas kernels, body(): pl.pallas_call(functools.partial(experts_kernel, share=share, seqs=seqs,...  3.07 us
    all_to_all x1, starting transfers between devices, body(): lax.all_to_all(outgoing, ('ep', 'tp'), split_axis=0, concat_axis=0, tiled...  2.78 us
  transfers between devices with their start and end apart: 4, of which 3 were waited for; matrix products, arithmetic and copies ran while one was open for 8% of the time, Pallas kernels for 10%

profile of v1, /device:TPU:0, one launch (start us, length us, event | category | flops | bytes accessed | tf_op | source)
XLA Modules:
  0.0 77.3 jit_solution(1970724119473262733)
XLA Ops:
  0.6 1.7 %copy.38.down_ref = bf16[512,64]{1,0:T(8,128)(2,1)} copy(bf16[512,64]{0,1:T(8,128)(2,1)} %param.56) | data formatting | bytes 131072 | tf_op args[27]
  2.3 2.1 %pack.1 = bf16[16,64,128]{2,1,0:T(8,128)(2,1)} custom-call(bf16[64,512]{1,0:T(8,128)(2,1)} %gate_ref.2, bf16[64,512]{1,0:T(8,128)(2,1)} %up_ref.2, bf16[512,64]{1,0:T(8,128)(2,1)} %copy.38.down_ref, s32[8,6]{1,0:T(8,128)} %ids_ref.1, f32[8,6]{1,0:T(8,128)} %weights_ref.1), custom_call_target="tpu_custom_call" | custom-call | tf_op jit(solution)/shard_map/pack/pallas_call | solution.py:287
  4.4 7.4 %all-to-all-start.1 = ((bf16[16,64,128]{2,1,0:T(8,128)(2,1)}), bf16[16,64,128]{2,1,0:T(8,128)(2,1)S(1)}, u32[]{:S(2)}, u32[]{:S(2)}) async-start(bf16[16,64,128]{2,1,0:T(8,128)(2,1)} %pack.1), calls=%async_computation.1 | async-start | bytes 524288 | tf_op jit(solution)/shard_map/all_to_all | solution.py:294
  11.8 0.8 copy.36.conv_b_ref
  12.6 0.8 copy.37.conv_c_ref
  13.4 0.8 %copy.35.conv_x_ref = bf16[8,3,1024]{2,1,0:T(4,128)(2,1)S(1)} copy(bf16[8,3,1024]{2,0,1:T(8,128)(2,1)} %param.31) | data formatting | bytes 98304 | tf_op args[2]
  14.2 1.0 %copy.34.w_dt_ref = bf16[1024,32]{1,0:T(8,128)(2,1)S(1)} copy(bf16[1024,32]{0,1:T(8,128)(2,1)} %param.38) | data formatting | bytes 131072 | tf_op args[9]
  15.2 2.2 %copy-done = f32[8,16,64,128]{3,2,1,0:T(8,128)S(1)} copy-done((f32[8,16,64,128]{3,2,1,0:T(8,128)S(1)}, f32[8,16,64,128]{3,2,1,0:T(8,128)}, u32[]{:S(2)}) %copy-start) | copy-done | bytes 4194328
  17.4 1.6 %copy-done.1 = bf16[1024,1024]{1,0:T(8,128)(2,1)S(1)} copy-done((bf16[1024,1024]{1,0:T(8,128)(2,1)S(1)}, bf16[1024,1024]{1,0:T(8,128)(2,1)}, u32[]{:S(2)}) %copy-start.1) | copy-done | bytes 2097176
  19.0 1.6 %copy-done.2 = bf16[1024,1024]{1,0:T(8,128)(2,1)S(1)} copy-done((bf16[1024,1024]{1,0:T(8,128)(2,1)S(1)}, bf16[1024,1024]{1,0:T(8,128)(2,1)}, u32[]{:S(2)}) %copy-start.2) | copy-done | bytes 2097176
  20.6 1.6 %copy-done.3 = bf16[1024,1024]{1,0:T(8,128)(2,1)S(1)} copy-done((bf16[1024,1024]{1,0:T(8,128)(2,1)S(1)}, bf16[1024,1024]{1,0:T(8,128)(2,1)}, u32[]{:S(2)}) %copy-start.3) | copy-done | bytes 2097176
  22.2 1.2 %copy-done.5 = bf16[1024,512]{1,0:T(8,128)(2,1)S(1)} copy-done((bf16[1024,512]{1,0:T(8,128)(2,1)S(1)}, bf16[1024,512]{1,0:T(8,128)(2,1)}, u32[]{:S(2)}) %copy-start.5) | copy-done | bytes 1048600
  23.4 0.7 copy-done.6
  24.1 0.7 copy-done.8
  24.8 0.7 copy-done.9
  25.5 0.7 copy-done.10
  26.2 0.7 copy-done.11
  26.9 0.7 copy-done.12
  27.6 0.7 copy-done.13
  28.2 0.7 copy-done.14
  29.6 6.2 %mixer.1 = (bf16[8,1024]{1,0:T(8,128)(2,1)S(1)}, bf16[8,3,1024]{2,1,0:T(4,128)(2,1)S(1)}, bf16[8,3,512]{2,1,0:T(4,128)(2,1)S(1)}, bf16[8,3,512]{2,1,0:T(4,128)(2,1)S(1)}, f32[8,16,64,128]{3,2,1,0:T(8,128)}) custom-call(s32[1]{0:T(128)} %bitcast.tp_ref, bf16[8,1024]{1,0:T(8,128)(2,1)S(1)} %copy-done.6, f32[1,1024]{1,0:T(1,128)S(1)} %bitcast.11, ...), custom_call_target="tpu_custom_call" | custom-call | tf_op jit(solution)/shard_map/mixer/pallas_call | solution.py:296
  35.8 1.6 %collective-permute-start = (bf16[8,1024]{1,0:T(8,128)(2,1)S(1)}, bf16[8,1024]{1,0:T(8,128)(2,1)S(1)}, u32[]{:S(2)}, u32[]{:S(2)}) collective-permute-start(bf16[8,1024]{1,0:T(8,128)(2,1)S(1)} %get-tuple-element.12.own_ref), channel_id=1, source_target_pairs={{0,1},{1,0},{2,3},{3,2},{4,5},{5,4},{6,7},{7,6},{8,9},{9,8},{10,11... | collective-permute-start | bytes 49160 | tf_op jit(solution)/shard_map/ppermute | solution.py:344
  37.3 2.2 %collective-permute-done.other_ref = bf16[8,1024]{1,0:T(8,128)(2,1)S(1)} collective-permute-done((bf16[8,1024]{1,0:T(8,128)(2,1)S(1)}, bf16[8,1024]{1,0:T(8,128)(2,1)S(1)}, u32[]{:S(2)}, u32[]{:S(2)}) %collective-permute-start) | collective-permute-done | bytes 16416 | tf_op jit(solution)/shard_map/ppermute | solution.py:344
  40.2 1.6 %norm.1 = (bf16[128,1024]{1,0:T(8,128)(2,1)}, bf16[8,1024]{1,0:T(8,128)(2,1)}) custom-call(bf16[8,1024]{1,0:T(8,128)(2,1)} %tokens_ref.3, bf16[8,1024]{1,0:T(8,128)(2,1)} %copy-done.7, bf16[8,1024]{1,0:T(8,128)(2,1)} %copy-done.19, f32[1,1024]{1,0:T(1,128)} %bitcast.20), custom_call_target="tpu_custom_call" | custom-call | tf_op jit(solution)/shard_map/norm/pallas_call | solution.py:352
  41.8 6.0 %all-to-all-start = ((bf16[16,8,1024]{2,1,0:T(8,128)(2,1)}), bf16[16,8,1024]{2,1,0:T(8,128)(2,1)S(1)}, u32[]{:S(2)}, u32[]{:S(2)}) async-start(bf16[16,8,1024]{2,1,0:T(8,128)(2,1)} %bitcast.19), calls=%async_computation | async-start | bytes 524288 | tf_op jit(solution)/shard_map/all_to_all | solution.py:359
  48.4 9.4 %all-to-all-done = bf16[16,8,1024]{2,1,0:T(8,128)(2,1)S(1)} async-done(((bf16[16,8,1024]{2,1,0:T(8,128)(2,1)}), bf16[16,8,1024]{2,1,0:T(8,128)(2,1)S(1)}, u32[]{:S(2)}, u32[]{:S(2)}) %all-to-all-start) | async-done | bytes 262176 | tf_op jit(solution)/shard_map/all_to_all | solution.py:359
  57.8 0.7 copy-done.17
  58.5 3.1 %experts.1 = bf16[256,512]{1,0:T(8,128)(2,1)} custom-call(bf16[128,1024]{1,0:T(8,128)(2,1)} %bitcast.17, bf16[16,64,128]{2,1,0:T(8,128)(2,1)} %copy-done.16, bf16[1,1024,256]{2,1,0:T(8,128)(2,1)} %gate_ref.3, bf16[1,1024,256]{2,1,0:T(8,128)(2,1)} %up_ref.3, bf16[1,256,1024]{2,1,0:T(8,128)(2,1)} %down_ref.2, bf16[1,1024]{1,0:T(2,128)(2,1)} %broadcast_in_dim.31.branch_ref), custom_call_target="tpu_custom_call" | custom-call | tf_op jit(solution)/shard_map/experts/pallas_call | solution.py:361
  61.6 2.8 %all-to-all-start.2 = ((bf16[32,8,512]{2,1,0:T(8,128)(2,1)}), bf16[32,8,512]{2,1,0:T(8,128)(2,1)S(1)}, u32[]{:S(2)}, u32[]{:S(2)}) async-start(bf16[32,8,512]{2,1,0:T(8,128)(2,1)} %bitcast.16), calls=%async_computation.2 | async-start | bytes 524288 | tf_op jit(solution)/shard_map/all_to_all | solution.py:368
  66.3 8.8 %all-to-all-done.2 = bf16[32,8,512]{2,1,0:T(8,128)(2,1)S(1)} async-done(((bf16[32,8,512]{2,1,0:T(8,128)(2,1)}), bf16[32,8,512]{2,1,0:T(8,128)(2,1)S(1)}, u32[]{:S(2)}, u32[]{:S(2)}) %all-to-all-start.2) | async-done | bytes 262176 | tf_op jit(solution)/shard_map/all_to_all | solution.py:368
  75.0 0.7 copy-done.18
  75.7 1.6 %total.1 = bf16[8,512]{1,0:T(8,128)(2,1)} custom-call(s32[1]{0:T(128)} %bitcast.tp_ref, bf16[256,512]{1,0:T(8,128)(2,1)} %bitcast.18, bf16[8,1024]{1,0:T(8,128)(2,1)} %get-tuple-element.14.residual_ref), custom_call_target="tpu_custom_call" | custom-call | tf_op jit(solution)/shard_map/total/pallas_call | solution.py:370
  (32 shorter events, 3.8 us)
Async XLA Ops:
  0.6 14.6 %copy-start.4 = (bf16[1024,512]{1,0:T(8,128)(2,1)S(1)}, bf16[1024,512]{1,0:T(8,128)(2,1)}, u32[]{:S(2)}) copy-start(bf16[1024,512]{1,0:T(8,128)(2,1)} %w_b_hbm.1) | copy-start | bytes 3145732
  4.4 37.4 %all-to-all-start.1 = ((bf16[16,64,128]{2,1,0:T(8,128)(2,1)}), bf16[16,64,128]{2,1,0:T(8,128)(2,1)S(1)}, u32[]{:S(2)}, u32[]{:S(2)}) async-start(bf16[16,64,128]{2,1,0:T(8,128)(2,1)} %pack.1), calls=%async_computation.1 | async-start | bytes 524288 | tf_op jit(solution)/shard_map/all_to_all | solution.py:294
  15.2 2.2 %copy-start = (f32[8,16,64,128]{3,2,1,0:T(8,128)S(1)}, f32[8,16,64,128]{3,2,1,0:T(8,128)}, u32[]{:S(2)}) copy-start(f32[8,16,64,128]{3,2,1,0:T(8,128)} %state_hbm.1) | copy-start | bytes 12582916
  17.4 1.6 %copy-start.1 = (bf16[1024,1024]{1,0:T(8,128)(2,1)S(1)}, bf16[1024,1024]{1,0:T(8,128)(2,1)}, u32[]{:S(2)}) copy-start(bf16[1024,1024]{1,0:T(8,128)(2,1)} %w_x_hbm.1) | copy-start | bytes 6291460
  19.0 1.6 %copy-start.2 = (bf16[1024,1024]{1,0:T(8,128)(2,1)S(1)}, bf16[1024,1024]{1,0:T(8,128)(2,1)}, u32[]{:S(2)}) copy-start(bf16[1024,1024]{1,0:T(8,128)(2,1)} %w_z_hbm.1) | copy-start | bytes 6291460
  20.6 1.6 %copy-start.3 = (bf16[1024,1024]{1,0:T(8,128)(2,1)S(1)}, bf16[1024,1024]{1,0:T(8,128)(2,1)}, u32[]{:S(2)}) copy-start(bf16[1024,1024]{1,0:T(8,128)(2,1)} %w_out_hbm.1) | copy-start | bytes 6291460
  22.2 1.2 %copy-start.5 = (bf16[1024,512]{1,0:T(8,128)(2,1)S(1)}, bf16[1024,512]{1,0:T(8,128)(2,1)}, u32[]{:S(2)}) copy-start(bf16[1024,512]{1,0:T(8,128)(2,1)} %w_c_hbm.1) | copy-start | bytes 3145732
  23.4 0.7 copy-start.6
  24.1 0.7 copy-start.8
  24.8 0.7 copy-start.9
  25.5 0.7 copy-start.10
  26.2 0.7 copy-start.11
  26.9 0.7 copy-start.12
  27.6 0.7 copy-start.13
  28.2 0.7 copy-start.14
  28.9 0.7 copy-start.15
  29.6 18.3 %copy-start.20 = (bf16[1024]{0:T(1024)(128)(2,1)S(1)}, bf16[1024]{0:T(1024)(128)(2,1)}, u32[]{:S(2)}) copy-start(bf16[1024]{0:T(1024)(128)(2,1)} %param.57) | copy-start | bytes 6148
  35.8 3.8 %copy-start.7 = (bf16[8,1024]{1,0:T(8,128)(2,1)}, bf16[8,1024]{1,0:T(8,128)(2,1)S(1)}, u32[]{:S(2)}) copy-start(bf16[8,1024]{1,0:T(8,128)(2,1)S(1)} %get-tuple-element.12.own_ref) | copy-start | bytes 49156
  35.8 3.8 %collective-permute-start = (bf16[8,1024]{1,0:T(8,128)(2,1)S(1)}, bf16[8,1024]{1,0:T(8,128)(2,1)S(1)}, u32[]{:S(2)}, u32[]{:S(2)}) collective-permute-start(bf16[8,1024]{1,0:T(8,128)(2,1)S(1)} %get-tuple-element.12.own_ref), channel_id=1, source_target_pairs={{0,1},{1,0},{2,3},{3,2},{4,5},{5,4},{6,7},{7,6},{8,9},{9,8},{10,11... | collective-permute-start | bytes 49160 | tf_op jit(solution)/shard_map/ppermute | solution.py:344
  39.6 0.6 copy-start.19
  41.8 16.0 %copy-start.16 = (bf16[16,64,128]{2,1,0:T(8,128)(2,1)}, bf16[16,64,128]{2,1,0:T(8,128)(2,1)S(1)}, u32[]{:S(2)}) copy-start(bf16[16,64,128]{2,1,0:T(8,128)(2,1)S(1)} %all-to-all-done.1.packed_ref) | copy-start | bytes 786436
  41.8 16.0 %all-to-all-start = ((bf16[16,8,1024]{2,1,0:T(8,128)(2,1)}), bf16[16,8,1024]{2,1,0:T(8,128)(2,1)S(1)}, u32[]{:S(2)}, u32[]{:S(2)}) async-start(bf16[16,8,1024]{2,1,0:T(8,128)(2,1)} %bitcast.19), calls=%async_computation | async-start | bytes 524288 | tf_op jit(solution)/shard_map/all_to_all | solution.py:359
  57.8 0.7 copy-start.17
  61.6 13.5 %all-to-all-start.2 = ((bf16[32,8,512]{2,1,0:T(8,128)(2,1)}), bf16[32,8,512]{2,1,0:T(8,128)(2,1)S(1)}, u32[]{:S(2)}, u32[]{:S(2)}) async-start(bf16[32,8,512]{2,1,0:T(8,128)(2,1)} %bitcast.16), calls=%async_computation.2 | async-start | bytes 524288 | tf_op jit(solution)/shard_map/all_to_all | solution.py:368
  75.0 0.7 copy-start.18

commit v2 on v1

--- a/solution.py
+++ b/solution.py
@@ -7,6 +7,7 @@
 from jax.experimental import pallas as pl
 from jax.experimental.pallas import tpu as pltpu
 from jax.sharding import PartitionSpec as P
+
 
 epsilon = 1e-06
 f32 = jnp.float32
@@ -15,6 +16,7 @@
 SMEM = pl.BlockSpec(memory_space=pltpu.SMEM)
 HBM = pl.BlockSpec(memory_space=pltpu.HBM)
 MIB = 1 << 20
+LONG = pl.CostEstimate(flops=10**10, bytes_accessed=10**6, transcendentals=0)
 
 
 def dot(left, right):
@@ -42,6 +44,14 @@
     return jnp.concatenate(
         [jnp.broadcast_to(values[:, h : h + 1], (rows, width)) for h in range(heads)], axis=1
     )
+
+
+def in_hbm(values):
+    return pltpu.with_memory_space_constraint(values, pltpu.HBM)
+
+
+def taps_first(values):
+    return values.transpose(1, 0, 2)
 
 
 def pack_kernel(gate_ref, up_ref, down_ref, ids_ref, weights_ref, out_ref, *, dests):
@@ -51,7 +61,7 @@
     seqs, top_count = ids_ref.shape
     gate = gate_ref[...].astype(f32)
     up = up_ref[...].astype(f32)
-    down = down_ref[...].astype(f32).T
+    down = down_ref[...].astype(f32)
     ids = ids_ref[...]
     weights = weights_ref[...]
     expert = lax.broadcasted_iota(jnp.int32, (seqs, dests), 1)
@@ -73,66 +83,48 @@
         out_ref[j] = jnp.concatenate(block, axis=1).astype(bf16)
 
 
-def mixer_kernel(
-    tp_ref,
-    tokens_ref,
-    gain_ref,
-    w_dt_ref,
-    dt_bias_ref,
-    a_log_ref,
-    d_skip_ref,
-    taps_x_ref,
-    taps_b_ref,
-    taps_c_ref,
-    group_gain_ref,
-    conv_x_ref,
-    conv_b_ref,
-    conv_c_ref,
-    w_x_hbm,
-    w_z_hbm,
-    w_b_hbm,
-    w_c_hbm,
-    w_out_hbm,
-    state_hbm,
-    part_ref,
-    conv_x_out,
-    conv_b_out,
-    conv_c_out,
-    state_out,
-    w_x,
-    w_z,
-    w_b,
-    w_c,
-    w_out,
-    state,
-    in_sems,
-    state_sems,
-    out_sems,
-    *,
-    n_tp,
-):
+def mixer_kernel(*refs, n_tp, held):
+    tp_ref, w_x, w_b = refs[:3]
+    sources = refs[3 : 3 + held]
+    part_ref, conv_x_out, conv_b_out, conv_c_out, state_out = refs[3 + held : 8 + held]
+    targets = refs[8 + held : 8 + 2 * held]
+    in_sems, state_sems, out_sems = refs[8 + 2 * held :]
+    (
+        tokens_ref,
+        gain_ref,
+        w_dt_ref,
+        dt_bias_ref,
+        a_log_ref,
+        d_skip_ref,
+        taps_x_ref,
+        taps_b_ref,
+        taps_c_ref,
+        group_gain_ref,
+        conv_x_ref,
+        conv_b_ref,
+        conv_c_ref,
+        w_c,
+        w_z,
+        w_out,
+        state,
+    ) = targets
     seqs, heads, head_dim, state_dim = state.shape
     channels = heads * head_dim
     groups = w_b.shape[1] // state_dim
     per_group = heads // groups
     width = channels // groups
     copy = pltpu.make_async_copy
-    moves = {}
-    for index, (name, source, target) in enumerate(
-        (("x", w_x_hbm, w_x), ("b", w_b_hbm, w_b), ("c", w_c_hbm, w_c))
-    ):
-        moves[name] = copy(source, target, in_sems.at[index])
-        moves[name].start()
-    loads = [copy(state_hbm.at[s], state.at[s], state_sems.at[s]) for s in range(seqs)]
+    loads = [copy(sources[i], targets[i], in_sems.at[i]) for i in range(held - 1)]
+    *small_loads, load_c, load_z, load_out = loads
+    state_loads = [copy(sources[-1].at[s], state.at[s], state_sems.at[s]) for s in range(seqs)]
     stores = [copy(state.at[s], state_out.at[s], out_sems.at[s]) for s in range(seqs)]
-    for load in loads:
+    for load in [*small_loads, load_c, *state_loads, load_z, load_out]:
         load.start()
-    for index, (name, source, target) in enumerate((("z", w_z_hbm, w_z), ("o", w_out_hbm, w_out))):
-        moves[name] = copy(source, target, in_sems.at[3 + index])
-        moves[name].start()
+    for load in small_loads:
+        load.wait()
 
     normed = rms_rows(tokens_ref[...].astype(f32), gain_ref[...]).astype(bf16)
-    dt_all = dot(normed, w_dt_ref[...])
+    dt_all = dot_nt(normed, w_dt_ref[...])
     own = tp_ref[0]
     dt_raw = jnp.zeros((seqs, heads), f32)
     for i in range(n_tp):
@@ -142,25 +134,26 @@
     decay = jnp.exp(-step * jnp.exp(a_log_ref[...]))
 
     def short_conv(previous_ref, fresh, taps_ref, out_ref):
-        previous = previous_ref[...].astype(f32)
         taps = taps_ref[...].astype(f32)
         last = taps.shape[0] - 1
-        total = jnp.sum(previous * taps[None, :last], axis=1) + fresh * taps[last:]
-        out_ref[...] = jnp.concatenate((previous[:, 1:], fresh[:, None]), axis=1).astype(bf16)
+        total = fresh * taps[last:]
+        for k in range(last):
+            total += previous_ref[k].astype(f32) * taps[k : k + 1]
+            out_ref[k] = previous_ref[k + 1] if k + 1 < last else fresh.astype(bf16)
         return silu(total)
 
-    def projected(name, ref):
-        moves[name].wait()
+    def projected(ref):
         return dot(normed, ref[...]).astype(bf16).astype(f32)
 
-    xs = short_conv(conv_x_ref, projected("x", w_x), taps_x_ref, conv_x_out)
-    bs = short_conv(conv_b_ref, projected("b", w_b), taps_b_ref, conv_b_out)
-    cs = short_conv(conv_c_ref, projected("c", w_c), taps_c_ref, conv_c_out).astype(bf16)
+    xs = short_conv(conv_x_ref, projected(w_x), taps_x_ref, conv_x_out)
+    bs = short_conv(conv_b_ref, projected(w_b), taps_b_ref, conv_b_out)
+    load_c.wait()
+    cs = short_conv(conv_c_ref, projected(w_c), taps_c_ref, conv_c_out).astype(bf16)
     scaled = (spread_heads(step, head_dim) * xs).T
     row = lax.broadcasted_iota(jnp.int32, (seqs, width), 0)
     readout = [jnp.zeros((seqs, width), f32) for _ in range(groups)]
     for s in range(seqs):
-        loads[s].wait()
+        state_loads[s].wait()
         for g in range(groups):
             key = bs[s : s + 1, g * state_dim : (g + 1) * state_dim]
             fresh = []
@@ -174,14 +167,15 @@
             )
             readout[g] = jnp.where(row == s, read, readout[g])
         stores[s].start()
-    z_gate = silu(projected("z", w_z))
+    load_z.wait()
+    z_gate = silu(projected(w_z))
     skip = spread_heads(d_skip_ref[...], head_dim) * xs
     mixed = []
     for g in range(groups):
         part = slice(g * width, (g + 1) * width)
         gated = (readout[g] + skip[:, part]) * z_gate[:, part]
         mixed.append(rms_rows(gated, group_gain_ref[:, part]).astype(bf16))
-    moves["o"].wait()
+    load_out.wait()
     part_ref[...] = dot(jnp.concatenate(mixed, axis=1), w_out[...]).astype(bf16)
     for store in stores:
         store.wait()
@@ -286,42 +280,19 @@
     lanes = 128 * math.ceil((3 * share + 2) / 128)
     packed = pl.pallas_call(
         functools.partial(pack_kernel, dests=n_ep),
-        out_shape=sds((n_ep, rows, lanes), bf16),
+        out_shape=pltpu.HBM((n_ep, rows, lanes), bf16),
         in_specs=[VMEM] * 5,
         out_specs=VMEM,
+        compiler_params=pltpu.CompilerParams(vmem_limit_bytes=4 * MIB),
+        cost_estimate=LONG,
         name="pack",
-    )(dense_gate, dense_up, dense_down, route_ids, route_weights)
+    )(*map(in_hbm, (dense_gate, dense_up, dense_down.T, route_ids, route_weights)))
     packed = lax.all_to_all(packed, "ep", split_axis=0, concat_axis=0, tiled=True)
 
-    part, conv_x_next, conv_b_next, conv_c_next, state_next = pl.pallas_call(
-        functools.partial(mixer_kernel, n_tp=n_tp),
-        out_shape=(
-            sds((seqs, model), bf16),
-            sds(conv_x.shape, bf16),
-            sds(conv_b.shape, bf16),
-            sds(conv_c.shape, bf16),
-            sds(ssm_state.shape, f32),
-        ),
-        in_specs=[SMEM] + [VMEM] * 13 + [HBM] * 6,
-        out_specs=(VMEM, VMEM, VMEM, VMEM, HBM),
-        scratch_shapes=[
-            pltpu.VMEM(w_x.shape, bf16),
-            pltpu.VMEM(w_z.shape, bf16),
-            pltpu.VMEM(w_b.shape, bf16),
-            pltpu.VMEM(w_c.shape, bf16),
-            pltpu.VMEM(w_out.shape, bf16),
-            pltpu.VMEM(ssm_state.shape, f32),
-            pltpu.SemaphoreType.DMA((5,)),
-            pltpu.SemaphoreType.DMA((seqs,)),
-            pltpu.SemaphoreType.DMA((seqs,)),
-        ],
-        compiler_params=pltpu.CompilerParams(vmem_limit_bytes=30 * MIB),
-        name="mixer",
-    )(
-        tp_index,
+    held = (
         tokens,
         norm1_gain[None],
-        w_dt,
+        w_dt.T,
         dt_bias[None],
         a_log[None],
         d_skip[None],
@@ -329,16 +300,34 @@
         taps_b,
         taps_c,
         group_gain[None],
-        conv_x,
-        conv_b,
-        conv_c,
-        w_x,
+        taps_first(conv_x),
+        taps_first(conv_b),
+        taps_first(conv_c),
+        w_c,
         w_z,
-        w_b,
-        w_c,
         w_out,
         ssm_state,
     )
+    part, conv_x_next, conv_b_next, conv_c_next, state_next = pl.pallas_call(
+        functools.partial(mixer_kernel, n_tp=n_tp, held=len(held)),
+        out_shape=(
+            sds((seqs, model), bf16),
+            sds(taps_first(conv_x).shape, bf16),
+            sds(taps_first(conv_b).shape, bf16),
+            sds(taps_first(conv_c).shape, bf16),
+            sds(ssm_state.shape, f32),
+        ),
+        in_specs=[SMEM] + [VMEM] * 2 + [HBM] * len(held),
+        out_specs=(VMEM, VMEM, VMEM, VMEM, HBM),
+        scratch_shapes=[pltpu.VMEM(value.shape, value.dtype) for value in held]
+        + [
+            pltpu.SemaphoreType.DMA((len(held) - 1,)),
+            pltpu.SemaphoreType.DMA((seqs,)),
+            pltpu.SemaphoreType.DMA((seqs,)),
+        ],
+        compiler_params=pltpu.CompilerParams(vmem_limit_bytes=20 * MIB),
+        name="mixer",
+    )(tp_index, w_x, w_b, *map(in_hbm, held))
 
     if n_tp == 2:
         other = lax.ppermute(part, "tp", [(0, 1), (1, 0)])
@@ -354,6 +343,8 @@
         out_shape=(sds((n_ep * seqs, model), bf16), sds((seqs, model), bf16)),
         in_specs=[VMEM] * 4,
         out_specs=(VMEM, VMEM),
+        compiler_params=pltpu.CompilerParams(vmem_limit_bytes=4 * MIB),
+        cost_estimate=LONG,
         name="norm",
     )(tokens, part, other, norm2_gain[None])
     everyone = lax.all_to_all(spread, "ep", split_axis=0, concat_axis=0, tiled=True)
@@ -363,6 +354,7 @@
         out_shape=sds((n_ep * n_tp * seqs, model // n_tp), bf16),
         in_specs=[VMEM] * 6,
         out_specs=VMEM,
+        compiler_params=pltpu.CompilerParams(vmem_limit_bytes=12 * MIB),
         name="experts",
     )(everyone, packed, exp_gate, exp_up, exp_down, branch_gate[None])
     parts = lax.all_to_all(outgoing, ("ep", "tp"), split_axis=0, concat_axis=0, tiled=True)
@@ -372,9 +364,16 @@
         out_shape=sds((seqs, model // n_tp), bf16),
         in_specs=[SMEM, VMEM, VMEM],
         out_specs=VMEM,
+        compiler_params=pltpu.CompilerParams(vmem_limit_bytes=4 * MIB),
         name="total",
     )(tp_index, parts, residual)
-    return (mixed, state_next, conv_x_next, conv_b_next, conv_c_next)
+    return (
+        mixed,
+        state_next,
+        taps_first(conv_x_next),
+        taps_first(conv_b_next),
+        taps_first(conv_c_next),
+    )
 
 
 def solution(mesh):

time: 78.5 us -> 59.5 us (0.76)
  local copies, waits for them, and re-layouts: 23.8 us -> 2.85 us
  blocking collectives: 0 us -> 12.4 us
  starting transfers between devices: 17.8 us -> 12.5 us
  Pallas kernels: 14.5 us -> 11.5 us
  waiting for transfers between devices: 20.4 us -> 19.1 us
    unnamed x50 -> x16, local copies, waits for them, and re-layouts: 23.3 us -> 2.84 us
    all_to_all x0 -> x1, blocking collectives: none -> 12.4 us  [body(): lax.all_to_all(outgoing, ('ep', 'tp'), split_axis=0, concat_axis=0, tiled...]
    all_to_all x1, waiting for transfers between devices: 0.01 us -> 9.11 us  [body(): lax.all_to_all(packed, 'ep', split_axis=0, concat_axis=0, tiled=True)]
    all_to_all x1 -> x0, waiting for transfers between devices: 8.79 us -> none  [body(): lax.all_to_all(outgoing, ('ep', 'tp'), split_axis=0, concat_axis=0, tiled...]
    all_to_all x1 -> x0, starting transfers between devices: 2.78 us -> none  [body(): lax.all_to_all(outgoing, ('ep', 'tp'), split_axis=0, concat_axis=0, tiled...]
    all_to_all x1, starting transfers between devices: 6.01 us -> 3.53 us  [body(): lax.all_to_all(spread, 'ep', split_axis=0, concat_axis=0, tiled=True)]
    ppermute x1, waiting for transfers between devices: 2.25 us -> 0.01 us  [body(): other = lax.ppermute(part, 'tp', [(0, 1), (1, 0)])]
    pallas_call x1, Pallas kernels: 3.07 us -> 0.84 us  [body(): pl.pallas_call(functools.partial(experts_kernel, share=share, seqs=seqs,...]
  transfers between devices with their start and end apart: 4 -> 3, of which waited for: 3 -> 2; matrix products, arithmetic and copies ran while one was open for 8% -> 0% of each run, Pallas kernels for 10% -> 5%
where the time goes in v2:
time: 59.5 us; the launch traced here: 59 us
  waiting for transfers between devices  19.1 us (32%)
  starting transfers between devices  12.5 us (21%)
  blocking collectives  12.4 us (21%)
  Pallas kernels  11.5 us (19%)
  local copies, waits for them, and re-layouts  2.85 us (5%)
  between operations  0.76 us (1%)
    all_to_all x1, blocking collectives, body(): lax.all_to_all(outgoing, ('ep', 'tp'), split_axis=0, concat_axis=0, tiled...  12.4 us
    all_to_all x1, waiting for transfers between devices, body(): lax.all_to_all(spread, 'ep', split_axis=0, concat_axis=0, tiled=True)  9.96 us
    all_to_all x1, waiting for transfers between devices, body(): lax.all_to_all(packed, 'ep', split_axis=0, concat_axis=0, tiled=True)  9.11 us
    pallas_call x1, Pallas kernels, body(): pl.pallas_call(functools.partial(mixer_kernel, n_tp=n_tp, held=len(held))...  7.22 us
    all_to_all x1, starting transfers between devices, body(): lax.all_to_all(packed, 'ep', split_axis=0, concat_axis=0, tiled=True)  5.94 us
    all_to_all x1, starting transfers between devices, body(): lax.all_to_all(spread, 'ep', split_axis=0, concat_axis=0, tiled=True)  3.53 us
    ppermute x1, starting transfers between devices, body(): other = lax.ppermute(part, 'tp', [(0, 1), (1, 0)])  3.03 us
    unnamed x16, local copies, waits for them, and re-layouts  2.84 us
  transfers between devices with their start and end apart: 3, of which 2 were waited for; matrix products, arithmetic and copies ran while one was open for 0% of the time, Pallas kernels for 5%

profile of v2, /device:TPU:0, one launch (start us, length us, event | category | flops | bytes accessed | tf_op | source)
XLA Modules:
  0.0 59.0 jit_solution(4736994293012706840)
XLA Ops:
  0.6 0.0 copy-start
  0.7 1.6 %copy-done = bf16[1024,1024]{1,0:T(8,128)(2,1)S(1)} copy-done((bf16[1024,1024]{1,0:T(8,128)(2,1)S(1)}, bf16[1024,1024]{1,0:T(8,128)(2,1)}, u32[]{:S(2)}) %copy-start) | copy-done | bytes 2097176
  2.2 0.0 copy-start.1
  2.2 1.2 %copy-done.1 = bf16[1024,512]{1,0:T(8,128)(2,1)S(1)} copy-done((bf16[1024,512]{1,0:T(8,128)(2,1)S(1)}, bf16[1024,512]{1,0:T(8,128)(2,1)}, u32[]{:S(2)}) %copy-start.1) | copy-done | bytes 1048600
  3.5 7.2 %mixer.1 = (bf16[8,1024]{1,0:T(8,128)(2,1)S(1)}, bf16[3,8,1024]{2,1,0:T(8,128)(2,1)}, bf16[3,8,512]{2,1,0:T(8,128)(2,1)}, bf16[3,8,512]{2,1,0:T(8,128)(2,1)}, f32[8,16,64,128]{3,2,1,0:T(8,128)}) custom-call(s32[1]{0:T(128)} %bitcast.refs_0_.tp_ref, bf16[1024,1024]{1,0:T(8,128)(2,1)S(1)} %copy-done, bf16[1024,512]{1,0:T(8,128)(2,1)S(1)} %copy-done.1, ...), custom_call_target="tpu_custom_call" | custom-call | tf_op jit(solution)/shard_map/mixer/pallas_call | solution.py:311
  10.7 3.0 %collective-permute-start = (bf16[8,1024]{1,0:T(8,128)(2,1)S(1)}, bf16[8,1024]{1,0:T(8,128)(2,1)S(1)}, u32[]{:S(2)}, u32[]{:S(2)}) collective-permute-start(bf16[8,1024]{1,0:T(8,128)(2,1)S(1)} %get-tuple-element.12.own_ref), channel_id=1, source_target_pairs={{0,1},{1,0},{2,3},{3,2},{4,5},{5,4},{6,7},{7,6},{8,9},{9,8},{10,11... | collective-permute-start | bytes 49160 | tf_op jit(solution)/shard_map/ppermute | solution.py:333
  13.7 0.0 copy-start.5
  13.7 0.0 copy-start.6
  13.7 1.9 %pack.1 = bf16[16,64,128]{2,1,0:T(8,128)(2,1)} custom-call(bf16[64,512]{1,0:T(8,128)(2,1)} %gate_ref.2, bf16[64,512]{1,0:T(8,128)(2,1)} %up_ref.2, bf16[64,512]{1,0:T(8,128)(2,1)} %bitcast.32, s32[8,6]{1,0:T(8,128)} %ids_ref.1, f32[8,6]{1,0:T(8,128)} %weights_ref.1), custom_call_target="tpu_custom_call" | custom-call | flops 10000000000 | bytes 1000000 | tf_op jit(solution)/shard_map/pack/pallas_call | solution.py:281
  15.7 5.9 %all-to-all-start.1 = ((bf16[16,64,128]{2,1,0:T(8,128)(2,1)}), bf16[16,64,128]{2,1,0:T(8,128)(2,1)S(1)}, u32[]{:S(2)}, u32[]{:S(2)}) async-start(bf16[16,64,128]{2,1,0:T(8,128)(2,1)} %pack.1), calls=%async_computation.1 | async-start | bytes 524288 | tf_op jit(solution)/shard_map/all_to_all | solution.py:290
  21.6 0.0 collective-permute-done.other_ref
  21.6 0.0 copy-done.5
  21.6 0.0 copy-done.6
  21.6 0.0 copy-start.7
  21.7 0.0 copy-start.2
  21.7 0.0 copy-start.3
  21.7 0.0 copy-start.4
  21.7 0.8 %norm.1 = (bf16[128,1024]{1,0:T(8,128)(2,1)}, bf16[8,1024]{1,0:T(8,128)(2,1)S(1)}) custom-call(bf16[8,1024]{1,0:T(8,128)(2,1)S(1)} %copy-done.5, bf16[8,1024]{1,0:T(8,128)(2,1)S(1)} %get-tuple-element.12.own_ref, bf16[8,1024]{1,0:T(8,128)(2,1)S(1)} %collective-permute-done.other_ref, f32[1,1024]{1,0:T(1,128)S(1)} %bitcast.22), custom_call_target="tpu_custom_call" | custom-call | flops 10000000000 | bytes 1000000 | tf_op jit(solution)/shard_map/norm/pallas_call | solution.py:341
  22.5 9.1 %all-to-all-done.1.packed_ref = bf16[16,64,128]{2,1,0:T(8,128)(2,1)S(1)} async-done(((bf16[16,64,128]{2,1,0:T(8,128)(2,1)}), bf16[16,64,128]{2,1,0:T(8,128)(2,1)S(1)}, u32[]{:S(2)}, u32[]{:S(2)}) %all-to-all-start.1) | async-done | bytes 262176 | tf_op jit(solution)/shard_map/all_to_all | solution.py:290
  31.6 3.5 %all-to-all-start = ((bf16[16,8,1024]{2,1,0:T(8,128)(2,1)}), bf16[16,8,1024]{2,1,0:T(8,128)(2,1)S(1)}, u32[]{:S(2)}, u32[]{:S(2)}) async-start(bf16[16,8,1024]{2,1,0:T(8,128)(2,1)} %bitcast.11), calls=%async_computation | async-start | bytes 524288 | tf_op jit(solution)/shard_map/all_to_all | solution.py:350
  35.2 0.0 copy-done.7
  35.2 10.0 %all-to-all-done = bf16[16,8,1024]{2,1,0:T(8,128)(2,1)S(1)} async-done(((bf16[16,8,1024]{2,1,0:T(8,128)(2,1)}), bf16[16,8,1024]{2,1,0:T(8,128)(2,1)S(1)}, u32[]{:S(2)}, u32[]{:S(2)}) %all-to-all-start) | async-done | bytes 262176 | tf_op jit(solution)/shard_map/all_to_all | solution.py:350
  45.1 0.0 copy-done.2
  45.1 0.0 copy-done.3
  45.2 0.0 copy-done.4
  45.2 0.8 %experts.1 = bf16[256,512]{1,0:T(8,128)(2,1)S(1)} custom-call(bf16[128,1024]{1,0:T(8,128)(2,1)S(1)} %bitcast.19, bf16[16,64,128]{2,1,0:T(8,128)(2,1)S(1)} %all-to-all-done.1.packed_ref, bf16[1,1024,256]{2,1,0:T(8,128)(2,1)S(1)} %copy-done.2, bf16[1,1024,256]{2,1,0:T(8,128)(2,1)S(1)} %copy-done.3, bf16[1,256,1024]{2,1,0:T(8,128)(2,1)S(1)} %copy-done.4, ...), custom_call_target="tpu_custom_call" | custom-call | tf_op jit(solution)/shard_map/experts/pallas_call | solution.py:352
  46.0 12.4 %all_to_all.27 = bf16[32,8,512]{2,1,0:T(8,128)(2,1)S(1)} all-to-all(bf16[32,8,512]{2,1,0:T(8,128)(2,1)S(1)} %bitcast.20), channel_id=1, replica_groups=mesh['ep'=16,'tp'=2] {'ep','tp'}, dimensions={0} | all-to-all | bytes 524288 | tf_op jit(solution)/shard_map/all_to_all | solution.py:360
  58.4 0.6 %total.1 = bf16[8,512]{1,0:T(8,128)(2,1)} custom-call(s32[1]{0:T(128)} %bitcast.refs_0_.tp_ref, bf16[256,512]{1,0:T(8,128)(2,1)S(1)} %bitcast.21, bf16[8,1024]{1,0:T(8,128)(2,1)S(1)} %get-tuple-element.14.residual_ref), custom_call_target="tpu_custom_call" | custom-call | tf_op jit(solution)/shard_map/total/pallas_call | solution.py:362
  (1 shorter events, 0.0 us)
Async XLA Ops:
  0.6 1.6 %copy-start = (bf16[1024,1024]{1,0:T(8,128)(2,1)S(1)}, bf16[1024,1024]{1,0:T(8,128)(2,1)}, u32[]{:S(2)}) copy-start(bf16[1024,1024]{1,0:T(8,128)(2,1)} %refs_1_.1) | copy-start | bytes 6291460
  2.2 1.2 %copy-start.1 = (bf16[1024,512]{1,0:T(8,128)(2,1)S(1)}, bf16[1024,512]{1,0:T(8,128)(2,1)}, u32[]{:S(2)}) copy-start(bf16[1024,512]{1,0:T(8,128)(2,1)} %refs_2_.1) | copy-start | bytes 3145732
  10.7 10.9 %collective-permute-start = (bf16[8,1024]{1,0:T(8,128)(2,1)S(1)}, bf16[8,1024]{1,0:T(8,128)(2,1)S(1)}, u32[]{:S(2)}, u32[]{:S(2)}) collective-permute-start(bf16[8,1024]{1,0:T(8,128)(2,1)S(1)} %get-tuple-element.12.own_ref), channel_id=1, source_target_pairs={{0,1},{1,0},{2,3},{3,2},{4,5},{5,4},{6,7},{7,6},{8,9},{9,8},{10,11... | collective-permute-start | bytes 49160 | tf_op jit(solution)/shard_map/ppermute | solution.py:333
  13.7 7.9 %copy-start.5 = (bf16[8,1024]{1,0:T(8,128)(2,1)S(1)}, bf16[8,1024]{1,0:T(8,128)(2,1)}, u32[]{:S(2)}) copy-start(bf16[8,1024]{1,0:T(8,128)(2,1)} %tokens_ref.1) | copy-start | bytes 49156
  13.7 7.9 %copy-start.6 = (f32[1024]{0:T(1024)S(1)}, f32[1024]{0:T(1024)}, u32[]{:S(2)}) copy-start(f32[1024]{0:T(1024)} %param.48) | copy-start | bytes 12292
  15.7 16.0 %all-to-all-start.1 = ((bf16[16,64,128]{2,1,0:T(8,128)(2,1)}), bf16[16,64,128]{2,1,0:T(8,128)(2,1)S(1)}, u32[]{:S(2)}, u32[]{:S(2)}) async-start(bf16[16,64,128]{2,1,0:T(8,128)(2,1)} %pack.1), calls=%async_computation.1 | async-start | bytes 524288 | tf_op jit(solution)/shard_map/all_to_all | solution.py:290
  21.6 13.5 %copy-start.7 = (bf16[1024]{0:T(1024)(128)(2,1)S(1)}, bf16[1024]{0:T(1024)(128)(2,1)}, u32[]{:S(2)}) copy-start(bf16[1024]{0:T(1024)(128)(2,1)} %param.57) | copy-start | bytes 6148
  21.7 23.5 %copy-start.2 = (bf16[1,1024,256]{2,1,0:T(8,128)(2,1)S(1)}, bf16[1,1024,256]{2,1,0:T(8,128)(2,1)}, u32[]{:S(2)}) copy-start(bf16[1,1024,256]{2,1,0:T(8,128)(2,1)} %gate_ref.3) | copy-start | bytes 1572868
  21.7 23.5 %copy-start.3 = (bf16[1,1024,256]{2,1,0:T(8,128)(2,1)S(1)}, bf16[1,1024,256]{2,1,0:T(8,128)(2,1)}, u32[]{:S(2)}) copy-start(bf16[1,1024,256]{2,1,0:T(8,128)(2,1)} %up_ref.3) | copy-start | bytes 1572868
  21.7 23.5 %copy-start.4 = (bf16[1,256,1024]{2,1,0:T(8,128)(2,1)S(1)}, bf16[1,256,1024]{2,1,0:T(8,128)(2,1)}, u32[]{:S(2)}) copy-start(bf16[1,256,1024]{2,1,0:T(8,128)(2,1)} %down_ref.1) | copy-start | bytes 1572868
  31.6 13.5 %all-to-all-start = ((bf16[16,8,1024]{2,1,0:T(8,128)(2,1)}), bf16[16,8,1024]{2,1,0:T(8,128)(2,1)S(1)}, u32[]{:S(2)}, u32[]{:S(2)}) async-start(bf16[16,8,1024]{2,1,0:T(8,128)(2,1)} %bitcast.11), calls=%async_computation | async-start | bytes 524288 | tf_op jit(solution)/shard_map/all_to_all | solution.py:350

commit v3 on v2

--- a/solution.py
+++ b/solution.py
@@ -86,9 +86,11 @@
 def mixer_kernel(*refs, n_tp, held):
     tp_ref, w_x, w_b = refs[:3]
     sources = refs[3 : 3 + held]
-    part_ref, conv_x_out, conv_b_out, conv_c_out, state_out = refs[3 + held : 8 + held]
-    targets = refs[8 + held : 8 + 2 * held]
-    in_sems, state_sems, out_sems = refs[8 + 2 * held :]
+    part_ref, scaled_ref, key_ref, decay_ref = refs[3 + held : 7 + held]
+    conv_outs = refs[7 + held : 10 + held]
+    targets = refs[10 + held : 10 + 2 * held]
+    conv_x_next, conv_b_next, conv_c_next = conv_next = refs[10 + 2 * held : 13 + 2 * held]
+    in_sems, state_sems, out_sems = refs[13 + 2 * held :]
     (
         tokens_ref,
         gain_ref,
@@ -117,7 +119,7 @@
     loads = [copy(sources[i], targets[i], in_sems.at[i]) for i in range(held - 1)]
     *small_loads, load_c, load_z, load_out = loads
     state_loads = [copy(sources[-1].at[s], state.at[s], state_sems.at[s]) for s in range(seqs)]
-    stores = [copy(state.at[s], state_out.at[s], out_sems.at[s]) for s in range(seqs)]
+    stores = [copy(conv_next[i], conv_outs[i], out_sems.at[i]) for i in range(3)]
     for load in [*small_loads, load_c, *state_loads, load_z, load_out]:
         load.start()
     for load in small_loads:
@@ -145,38 +147,64 @@
     def projected(ref):
         return dot(normed, ref[...]).astype(bf16).astype(f32)
 
-    xs = short_conv(conv_x_ref, projected(w_x), taps_x_ref, conv_x_out)
-    bs = short_conv(conv_b_ref, projected(w_b), taps_b_ref, conv_b_out)
+    xs = short_conv(conv_x_ref, projected(w_x), taps_x_ref, conv_x_next)
+    bs = short_conv(conv_b_ref, projected(w_b), taps_b_ref, conv_b_next)
     load_c.wait()
-    cs = short_conv(conv_c_ref, projected(w_c), taps_c_ref, conv_c_out).astype(bf16)
-    scaled = (spread_heads(step, head_dim) * xs).T
+    cs = short_conv(conv_c_ref, projected(w_c), taps_c_ref, conv_c_next)
+    for store in stores:
+        store.start()
+    queries = cs.astype(bf16)
+    scaled = spread_heads(step, head_dim) * xs
+    scaled_ref[...] = scaled
+    key_ref[...] = bs
+    decay_ref[...] = decay
     row = lax.broadcasted_iota(jnp.int32, (seqs, width), 0)
     readout = [jnp.zeros((seqs, width), f32) for _ in range(groups)]
     for s in range(seqs):
         state_loads[s].wait()
         for g in range(groups):
-            key = bs[s : s + 1, g * state_dim : (g + 1) * state_dim]
-            fresh = []
-            for h in range(g * per_group, (g + 1) * per_group):
-                column = scaled[h * head_dim : (h + 1) * head_dim, s : s + 1]
-                updated = decay[s : s + 1, h : h + 1] * state[s, h] + column * key
-                state[s, h] = updated
-                fresh.append(updated.astype(bf16))
-            read = dot_nt(
-                cs[:, g * state_dim : (g + 1) * state_dim], jnp.concatenate(fresh, axis=0)
-            )
+            block = state[s, g * per_group : (g + 1) * per_group].reshape(width, state_dim)
+            read = dot_nt(queries[:, g * state_dim : (g + 1) * state_dim], block.astype(bf16))
             readout[g] = jnp.where(row == s, read, readout[g])
-        stores[s].start()
     load_z.wait()
     z_gate = silu(projected(w_z))
     skip = spread_heads(d_skip_ref[...], head_dim) * xs
+    kept = spread_heads(decay, head_dim)
     mixed = []
     for g in range(groups):
         part = slice(g * width, (g + 1) * width)
-        gated = (readout[g] + skip[:, part]) * z_gate[:, part]
+        own = slice(g * state_dim, (g + 1) * state_dim)
+        match = jnp.sum(bs[:, own] * cs[:, own], axis=1, keepdims=True)
+        read = kept[:, part] * readout[g] + scaled[:, part] * match
+        gated = (read + skip[:, part]) * z_gate[:, part]
         mixed.append(rms_rows(gated, group_gain_ref[:, part]).astype(bf16))
     load_out.wait()
     part_ref[...] = dot(jnp.concatenate(mixed, axis=1), w_out[...]).astype(bf16)
+    for store in stores:
+        store.wait()
+
+
+def advance_kernel(
+    scaled_ref, key_ref, decay_ref, state_hbm, state_out, state, in_sems, out_sems
+):
+    seqs, heads, head_dim, state_dim = state.shape
+    per_group = heads * state_dim // key_ref.shape[1]
+    copy = pltpu.make_async_copy
+    loads = [copy(state_hbm.at[s], state.at[s], in_sems.at[s]) for s in range(seqs)]
+    stores = [copy(state.at[s], state_out.at[s], out_sems.at[s]) for s in range(seqs)]
+    for load in loads:
+        load.start()
+    scaled = scaled_ref[...].T
+    keys = key_ref[...]
+    decay = decay_ref[...]
+    for s in range(seqs):
+        loads[s].wait()
+        for h in range(heads):
+            g = h // per_group
+            key = keys[s : s + 1, g * state_dim : (g + 1) * state_dim]
+            column = scaled[h * head_dim : (h + 1) * head_dim, s : s + 1]
+            state[s, h] = decay[s : s + 1, h : h + 1] * state[s, h] + column * key
+        stores[s].start()
     for store in stores:
         store.wait()
 
@@ -192,11 +220,26 @@
 
 
 def experts_kernel(
-    rows_ref, packed_ref, gate_ref, up_ref, down_ref, branch_ref, out_ref, *, share, seqs, n_tp
+    core_ref,
+    own_ref,
+    other_ref,
+    packed_ref,
+    gate_ref,
+    up_ref,
+    down_ref,
+    branch_ref,
+    keep_ref,
+    send_ref,
+    *,
+    share,
+    seqs,
+    n_tp,
 ):
     blocks, block_rows, lanes = packed_ref.shape
-    count, model = rows_ref.shape
-    rows = rows_ref[...]
+    core = core_ref[0]
+    half_count, model = own_ref.shape
+    count = 2 * half_count
+    rows = jnp.concatenate((own_ref[...], other_ref[...]), axis=0)
     active = (silu(dot(rows, gate_ref[0])) * dot(rows, up_ref[0])).astype(bf16)
     routed = dot(active, down_ref[0])
     packed = packed_ref[...].reshape(blocks * block_rows, lanes)
@@ -207,22 +250,33 @@
     dense = jnp.where(chosen, dense, 0.0).astype(bf16)
     dense_out = dot_nt(dense, packed)
     branch = sigmoid(
-        jnp.sum(rows.astype(f32) * branch_ref[...].astype(f32), axis=1, keepdims=True)
+        jnp.sum(rows.astype(f32) * branch_ref[...].astype(f32)[None], axis=1, keepdims=True)
     )
     table = jnp.concatenate(
-        [packed_ref[i, :seqs].astype(f32) for i in range(blocks)], axis=0
+        [
+            packed_ref[2 * i + place, :seqs].astype(f32)
+            for place in (core, 1 - core)
+            for i in range(blocks // 2)
+        ],
+        axis=0,
     )
     weight = jnp.sum(
         jnp.where((lane >= 3 * share) & (lane < 3 * share + 2), table, 0.0), axis=1, keepdims=True
     )
     result = weight * routed + branch * dense_out
     half = model // n_tp
-    for j in range(blocks):
+    for i in range(blocks // 2):
         for q in range(n_tp):
-            place = (j * n_tp + q) * seqs
-            out_ref[place : place + seqs] = result[
-                j * seqs : (j + 1) * seqs, q * half : (q + 1) * half
+            place = (i * n_tp + q) * seqs
+            part = slice(q * half, (q + 1) * half)
+            keep_ref[place : place + seqs] = result[i * seqs : (i + 1) * seqs, part]
+            send_ref[place : place + seqs] = result[
+                half_count + i * seqs : half_count + (i + 1) * seqs, part
             ].astype(bf16)
+
+
+def add_kernel(left_ref, right_ref, out_ref):
+    out_ref[...] = (left_ref[...] + right_ref[...].astype(f32)).astype(bf16)
 
 
 def sum_kernel(tp_ref, parts_ref, residual_ref, out_ref, *, n_tp):
@@ -272,6 +326,7 @@
     seqs, model = tokens.shape
     n_ep = lax.axis_size("ep")
     n_tp = lax.axis_size("tp")
+    core_index = (lax.axis_index("ep").astype(jnp.int32) % 2)[None]
     tp_index = lax.axis_index("tp").astype(jnp.int32)[None]
     sds = jax.ShapeDtypeStruct
 
@@ -308,26 +363,41 @@
         w_out,
         ssm_state,
     )
-    part, conv_x_next, conv_b_next, conv_c_next, state_next = pl.pallas_call(
+    part, scaled, keys, decay, conv_x_next, conv_b_next, conv_c_next = pl.pallas_call(
         functools.partial(mixer_kernel, n_tp=n_tp, held=len(held)),
         out_shape=(
             sds((seqs, model), bf16),
-            sds(taps_first(conv_x).shape, bf16),
-            sds(taps_first(conv_b).shape, bf16),
-            sds(taps_first(conv_c).shape, bf16),
-            sds(ssm_state.shape, f32),
+            sds((seqs, w_x.shape[1]), f32),
+            sds((seqs, w_b.shape[1]), f32),
+            sds((seqs, ssm_state.shape[1]), f32),
+            *[sds(taps_first(value).shape, bf16) for value in (conv_x, conv_b, conv_c)],
         ),
         in_specs=[SMEM] + [VMEM] * 2 + [HBM] * len(held),
-        out_specs=(VMEM, VMEM, VMEM, VMEM, HBM),
+        out_specs=(VMEM,) * 4 + (HBM,) * 3,
         scratch_shapes=[pltpu.VMEM(value.shape, value.dtype) for value in held]
+        + [pltpu.VMEM(taps_first(value).shape, bf16) for value in (conv_x, conv_b, conv_c)]
         + [
             pltpu.SemaphoreType.DMA((len(held) - 1,)),
             pltpu.SemaphoreType.DMA((seqs,)),
-            pltpu.SemaphoreType.DMA((seqs,)),
+            pltpu.SemaphoreType.DMA((3,)),
         ],
         compiler_params=pltpu.CompilerParams(vmem_limit_bytes=20 * MIB),
         name="mixer",
     )(tp_index, w_x, w_b, *map(in_hbm, held))
+
+    state_next = pl.pallas_call(
+        advance_kernel,
+        out_shape=sds(ssm_state.shape, f32),
+        in_specs=[VMEM] * 3 + [HBM],
+        out_specs=HBM,
+        scratch_shapes=[
+            pltpu.VMEM(ssm_state.shape, f32),
+            pltpu.SemaphoreType.DMA((seqs,)),
+            pltpu.SemaphoreType.DMA((seqs,)),
+        ],
+        compiler_params=pltpu.CompilerParams(vmem_limit_bytes=12 * MIB),
+        name="advance",
+    )(scaled, keys, decay, in_hbm(ssm_state))
 
     if n_tp == 2:
         other = lax.ppermute(part, "tp", [(0, 1), (1, 0)])
@@ -340,24 +410,46 @@
 
     spread, residual = pl.pallas_call(
         norm_kernel,
-        out_shape=(sds((n_ep * seqs, model), bf16), sds((seqs, model), bf16)),
+        out_shape=(sds((n_ep // 2 * seqs, model), bf16), sds((seqs, model), bf16)),
         in_specs=[VMEM] * 4,
         out_specs=(VMEM, VMEM),
         compiler_params=pltpu.CompilerParams(vmem_limit_bytes=4 * MIB),
         cost_estimate=LONG,
         name="norm",
     )(tokens, part, other, norm2_gain[None])
-    everyone = lax.all_to_all(spread, "ep", split_axis=0, concat_axis=0, tiled=True)
-
-    outgoing = pl.pallas_call(
+    groups = [[2 * chip + core for chip in range(n_ep // 2)] for core in range(2)]
+    swap = [(i, i ^ 1) for i in range(n_ep)]
+    own_core = lax.all_to_all(
+        spread, "ep", split_axis=0, concat_axis=0, tiled=True, axis_index_groups=groups
+    )
+    other_core = lax.ppermute(own_core, "ep", swap)
+
+    blocks = (n_ep // 2 * n_tp * seqs, model // n_tp)
+    keep, send = pl.pallas_call(
         functools.partial(experts_kernel, share=share, seqs=seqs, n_tp=n_tp),
-        out_shape=sds((n_ep * n_tp * seqs, model // n_tp), bf16),
-        in_specs=[VMEM] * 6,
-        out_specs=VMEM,
+        out_shape=(sds(blocks, f32), sds(blocks, bf16)),
+        in_specs=[SMEM] + [VMEM] * 7,
+        out_specs=(VMEM, VMEM),
         compiler_params=pltpu.CompilerParams(vmem_limit_bytes=12 * MIB),
         name="experts",
-    )(everyone, packed, exp_gate, exp_up, exp_down, branch_gate[None])
-    parts = lax.all_to_all(outgoing, ("ep", "tp"), split_axis=0, concat_axis=0, tiled=True)
+    )(core_index, own_core, other_core, packed, exp_gate, exp_up, exp_down, branch_gate)
+    outgoing = pl.pallas_call(
+        add_kernel,
+        out_shape=sds(blocks, bf16),
+        in_specs=[VMEM] * 2,
+        out_specs=VMEM,
+        compiler_params=pltpu.CompilerParams(vmem_limit_bytes=4 * MIB),
+        name="add",
+    )(keep, lax.ppermute(send, "ep", swap))
+    flat_groups = [[ep * n_tp + q for ep in group for q in range(n_tp)] for group in groups]
+    parts = lax.all_to_all(
+        outgoing,
+        ("ep", "tp"),
+        split_axis=0,
+        concat_axis=0,
+        tiled=True,
+        axis_index_groups=flat_groups,
+    )
 
     mixed = pl.pallas_call(
         functools.partial(sum_kernel, n_tp=n_tp),

time: 59.5 us -> 57 us (0.958)
  blocking collectives: 12.4 us -> 0 us
  starting transfers between devices: 12.5 us -> 17.1 us
  Pallas kernels: 11.5 us -> 14.1 us
  waiting for transfers between devices: 19.1 us -> 21.7 us
    all_to_all x1 -> x0, blocking collectives: 12.4 us -> none  [body(): lax.all_to_all(outgoing, ('ep', 'tp'), split_axis=0, concat_axis=0, tiled...]
    all_to_all x1 -> x2, starting transfers between devices: 3.53 us -> 10.2 us  [the longest x1 6.36 us: body(): lax.all_to_all(spread, 'ep', split_axis=0, concat_axis=0, tiled=True, axi...]
    pallas_call x1 -> x3, Pallas kernels: 0.83 us -> 5.55 us  [the longest x1 4.1 us: body(): pl.pallas_call(advance_kernel, out_shape=sds(ssm_state.shape, f32), in_sp...]
    ppermute x0 -> x2, waiting for transfers between devices: none -> 2.46 us  [the longest x1 1.33 us: body(): lax.ppermute(send, 'ep', swap)]
    all_to_all x1, starting transfers between devices: 5.94 us -> 3.53 us  [body(): lax.all_to_all(packed, 'ep', split_axis=0, concat_axis=0, tiled=True)]
    pallas_call x1, Pallas kernels: 7.22 us -> 5.09 us  [body(): pl.pallas_call(functools.partial(mixer_kernel, n_tp=n_tp, held=len(held))...]
    ppermute x1, waiting for transfers between devices: 0.01 us -> 1.72 us  [body(): other = lax.ppermute(part, 'tp', [(0, 1), (1, 0)])]
    all_to_all x1 -> x2, waiting for transfers between devices: 9.96 us -> 8.97 us  [the longest x1 5.27 us: body(): lax.all_to_all(spread, 'ep', split_axis=0, concat_axis=0, tiled=True, axi...]
  transfers between devices with their start and end apart: 3 -> 6, of which waited for: 2 -> 6; matrix products, arithmetic and copies ran while one was open for 0% -> 0% of each run, Pallas kernels for 5% -> 11%
where the time goes in v3:
time: 57 us; the launch traced here: 56.5 us
  waiting for transfers between devices  21.7 us (38%)
  starting transfers between devices  17.1 us (30%)
  Pallas kernels  14.1 us (25%)
  local copies, waits for them, and re-layouts  2.84 us (5%)
  between operations  0.74 us (1%)
    all_to_all x1, waiting for transfers between devices, body(): lax.all_to_all(packed, 'ep', split_axis=0, concat_axis=0, tiled=True)  8.56 us
    all_to_all x1, starting transfers between devices, body(): lax.all_to_all(spread, 'ep', split_axis=0, concat_axis=0, tiled=True, axi...  6.36 us
    all_to_all x1, waiting for transfers between devices, body(): lax.all_to_all(spread, 'ep', split_axis=0, concat_axis=0, tiled=True, axi...  5.27 us
    pallas_call x1, Pallas kernels, body(): pl.pallas_call(functools.partial(mixer_kernel, n_tp=n_tp, held=len(held))...  5.09 us
    pallas_call x1, Pallas kernels, body(): pl.pallas_call(advance_kernel, out_shape=sds(ssm_state.shape, f32), in_sp...  4.1 us
    all_to_all x1, starting transfers between devices, body(): lax.all_to_all(outgoing, ('ep', 'tp'), split_axis=0, concat_axis=0, tiled...  3.82 us
    all_to_all x1, waiting for transfers between devices, body(): lax.all_to_all(outgoing, ('ep', 'tp'), split_axis=0, concat_axis=0, tiled...  3.7 us
    all_to_all x1, starting transfers between devices, body(): lax.all_to_all(packed, 'ep', split_axis=0, concat_axis=0, tiled=True)  3.53 us
  transfers between devices with their start and end apart: 6, of which 6 were waited for; matrix products, arithmetic and copies ran while one was open for 0% of the time, Pallas kernels for 11%

profile of v3, /device:TPU:0, one launch (start us, length us, event | category | flops | bytes accessed | tf_op | source)
XLA Modules:
  0.0 56.5 jit_solution(12185708061626124108)
XLA Ops:
  0.6 0.0 copy-start
  0.7 1.6 %copy-done = bf16[1024,1024]{1,0:T(8,128)(2,1)S(1)} copy-done((bf16[1024,1024]{1,0:T(8,128)(2,1)S(1)}, bf16[1024,1024]{1,0:T(8,128)(2,1)}, u32[]{:S(2)}) %copy-start) | copy-done | bytes 2097176
  2.2 0.0 copy-start.1
  2.2 1.2 %copy-done.1 = bf16[1024,512]{1,0:T(8,128)(2,1)S(1)} copy-done((bf16[1024,512]{1,0:T(8,128)(2,1)S(1)}, bf16[1024,512]{1,0:T(8,128)(2,1)}, u32[]{:S(2)}) %copy-start.1) | copy-done | bytes 1048600
  3.5 5.1 %mixer.1 = (bf16[8,1024]{1,0:T(8,128)(2,1)S(1)}, f32[8,1024]{1,0:T(8,128)S(1)}, f32[8,512]{1,0:T(8,128)S(1)}, f32[8,16]{1,0:T(8,128)S(1)}, bf16[3,8,1024]{2,1,0:...) custom-call(s32[1]{0:T(128)} %bitcast.refs_0_.tp_ref, bf16[1024,1024]{1,0:T(8,128)(2,1)S(1)} %copy-done, ...), custom_call_target="tpu_custom_call" | custom-call | tf_op jit(solution)/shard_map/mixer/pallas_call | solution.py:366
  8.6 3.0 %collective-permute-start = (bf16[8,1024]{1,0:T(8,128)(2,1)S(1)}, bf16[8,1024]{1,0:T(8,128)(2,1)S(1)}, u32[]{:S(2)}, u32[]{:S(2)}) collective-permute-start(bf16[8,1024]{1,0:T(8,128)(2,1)S(1)} %get-tuple-element.16.own_ref), channel_id=1, source_target_pairs={{0,1},{1,0},{2,3},{3,2},{4,5},{5,4},{6,7},{7,6},{8,9},{9,8},{10,11... | collective-permute-start | bytes 49160 | tf_op jit(solution)/shard_map/ppermute | solution.py:403
  11.6 1.7 %collective-permute-done.other_ref = bf16[8,1024]{1,0:T(8,128)(2,1)S(1)} collective-permute-done((bf16[8,1024]{1,0:T(8,128)(2,1)S(1)}, bf16[8,1024]{1,0:T(8,128)(2,1)S(1)}, u32[]{:S(2)}, u32[]{:S(2)}) %collective-permute-start) | collective-permute-done | bytes 16416 | tf_op jit(solution)/shard_map/ppermute | solution.py:403
  13.3 0.0 copy-done.5
  13.3 0.0 copy-done.7
  13.3 0.8 %norm.1 = (bf16[64,1024]{1,0:T(8,128)(2,1)}, bf16[8,1024]{1,0:T(8,128)(2,1)S(1)}) custom-call(bf16[8,1024]{1,0:T(8,128)(2,1)S(1)} %copy-done.5, bf16[8,1024]{1,0:T(8,128)(2,1)S(1)} %get-tuple-element.16.own_ref, bf16[8,1024]{1,0:T(8,128)(2,1)S(1)} %collective-permute-done.other_ref, f32[1,1024]{1,0:T(1,128)S(1)} %bitcast.23), custom_call_target="tpu_custom_call" | custom-call | flops 10000000000 | bytes 1000000 | tf_op jit(solution)/shard_map/norm/pallas_call | solution.py:411
  14.1 6.4 %all-to-all-start = ((bf16[8,8,1024]{2,1,0:T(8,128)(2,1)}), bf16[8,8,1024]{2,1,0:T(8,128)(2,1)S(1)}, u32[]{:S(2)}, u32[]{:S(2)}) async-start(bf16[8,8,1024]{2,1,0:T(8,128)(2,1)} %bitcast.12), calls=%async_computation | async-start | bytes 262144 | tf_op jit(solution)/shard_map/all_to_all | solution.py:422
  20.4 0.0 copy-start.3
  20.5 0.0 copy-start.4
  20.5 0.0 copy-start.6
  20.5 2.0 %pack.1 = bf16[16,64,128]{2,1,0:T(8,128)(2,1)} custom-call(bf16[64,512]{1,0:T(8,128)(2,1)} %gate_ref.2, bf16[64,512]{1,0:T(8,128)(2,1)} %up_ref.2, bf16[64,512]{1,0:T(8,128)(2,1)} %bitcast.33, s32[8,6]{1,0:T(8,128)} %ids_ref.1, f32[8,6]{1,0:T(8,128)} %weights_ref.1), custom_call_target="tpu_custom_call" | custom-call | flops 10000000000 | bytes 1000000 | tf_op jit(solution)/shard_map/pack/pallas_call | solution.py:336
  22.5 5.3 %all-to-all-done = bf16[8,8,1024]{2,1,0:T(8,128)(2,1)S(1)} async-done(((bf16[8,8,1024]{2,1,0:T(8,128)(2,1)}), bf16[8,8,1024]{2,1,0:T(8,128)(2,1)S(1)}, u32[]{:S(2)}, u32[]{:S(2)}) %all-to-all-start) | async-done | bytes 131104 | tf_op jit(solution)/shard_map/all_to_all | solution.py:422
  27.8 3.5 %all-to-all-start.1 = ((bf16[16,64,128]{2,1,0:T(8,128)(2,1)}), bf16[16,64,128]{2,1,0:T(8,128)(2,1)S(1)}, u32[]{:S(2)}, u32[]{:S(2)}) async-start(bf16[16,64,128]{2,1,0:T(8,128)(2,1)} %pack.1), calls=%async_computation.1 | async-start | bytes 524288 | tf_op jit(solution)/shard_map/all_to_all | solution.py:345
  31.3 0.3 collective-permute-start.1
  31.6 1.1 %collective-permute-done.1.other_ref = bf16[64,1024]{1,0:T(8,128)(2,1)S(1)} collective-permute-done((bf16[64,1024]{1,0:T(8,128)(2,1)S(1)}, bf16[64,1024]{1,0:T(8,128)(2,1)S(1)}, u32[]{:S(2)}, u32[]{:S(2)}) %collective-permute-start.1) | collective-permute-done | bytes 131104 | tf_op jit(solution)/shard_map/ppermute | solution.py:425
  32.7 8.6 %all-to-all-done.1.packed_ref = bf16[16,64,128]{2,1,0:T(8,128)(2,1)S(1)} async-done(((bf16[16,64,128]{2,1,0:T(8,128)(2,1)}), bf16[16,64,128]{2,1,0:T(8,128)(2,1)S(1)}, u32[]{:S(2)}, u32[]{:S(2)}) %all-to-all-start.1) | async-done | bytes 262176 | tf_op jit(solution)/shard_map/all_to_all | solution.py:345
  41.3 0.0 copy-done.2
  41.3 0.0 copy-done.3
  41.3 0.0 copy-done.4
  41.3 0.0 copy-done.6
  41.3 0.8 %experts.1 = (f32[128,512]{1,0:T(8,128)S(1)}, bf16[128,512]{1,0:T(8,128)(2,1)S(1)}) custom-call(s32[1]{0:T(128)} %bitcast.1.core_ref, bf16[64,1024]{1,0:T(8,128)(2,1)S(1)} %bitcast.22, bf16[64,1024]{1,0:T(8,128)(2,1)S(1)} %collective-permute-done.1.other_ref, bf16[16,64,128]{2,1,0:T(8,128)(2,1)S(1)} %all-to-all-done.1.packed_ref, ...), custom_call_target="tpu_custom_call" | custom-call | tf_op jit(solution)/shard_map/experts/pallas_call | solution.py:428
  42.2 0.1 collective-permute-start.2
  42.2 1.3 %collective-permute-done.2.right_ref = bf16[128,512]{1,0:T(8,128)(2,1)S(1)} collective-permute-done((bf16[128,512]{1,0:T(8,128)(2,1)S(1)}, bf16[128,512]{1,0:T(8,128)(2,1)S(1)}, u32[]{:S(2)}, u32[]{:S(2)}) %collective-permute-start.2) | collective-permute-done | bytes 131104 | tf_op jit(solution)/shard_map/ppermute | solution.py:443
  43.6 0.7 %add.6 = bf16[128,512]{1,0:T(8,128)(2,1)} custom-call(f32[128,512]{1,0:T(8,128)S(1)} %get-tuple-element.18.left_ref, bf16[128,512]{1,0:T(8,128)(2,1)S(1)} %collective-permute-done.2.right_ref), custom_call_target="tpu_custom_call" | custom-call | tf_op jit(solution)/shard_map/add/pallas_call | solution.py:436
  44.3 3.8 %all-to-all-start.2 = ((bf16[16,8,512]{2,1,0:T(8,128)(2,1)}), bf16[16,8,512]{2,1,0:T(8,128)(2,1)S(1)}, u32[]{:S(2)}, u32[]{:S(2)}) async-start(bf16[16,8,512]{2,1,0:T(8,128)(2,1)} %bitcast.15), calls=%async_computation.2 | async-start | bytes 262144 | tf_op jit(solution)/shard_map/all_to_all | solution.py:445
  48.1 4.1 %advance.1 = f32[8,16,64,128]{3,2,1,0:T(8,128)} custom-call(f32[8,1024]{1,0:T(8,128)S(1)} %get-tuple-element.21.scaled_ref, f32[8,512]{1,0:T(8,128)S(1)} %get-tuple-element.22.key_ref, f32[8,16]{1,0:T(8,128)S(1)} %get-tuple-element.23.decay_ref, f32[8,16,64,128]{3,2,1,0:T(8,128)} %state_hbm.1), custom_call_target="tpu_custom_call" | custom-call | tf_op jit(solution)/shard_map/advance/pallas_call | solution.py:388
  52.2 3.7 %all-to-all-done.2 = bf16[16,8,512]{2,1,0:T(8,128)(2,1)S(1)} async-done(((bf16[16,8,512]{2,1,0:T(8,128)(2,1)}), bf16[16,8,512]{2,1,0:T(8,128)(2,1)S(1)}, u32[]{:S(2)}, u32[]{:S(2)}) %all-to-all-start.2) | async-done | bytes 131104 | tf_op jit(solution)/shard_map/all_to_all | solution.py:445
  55.9 0.6 %total.1 = bf16[8,512]{1,0:T(8,128)(2,1)} custom-call(s32[1]{0:T(128)} %bitcast.refs_0_.tp_ref, bf16[128,512]{1,0:T(8,128)(2,1)S(1)} %bitcast.20, bf16[8,1024]{1,0:T(8,128)(2,1)S(1)} %get-tuple-element.20.residual_ref), custom_call_target="tpu_custom_call" | custom-call | tf_op jit(solution)/shard_map/total/pallas_call | solution.py:454
  (3 shorter events, 0.0 us)
Async XLA Ops:
  0.6 1.6 %copy-start = (bf16[1024,1024]{1,0:T(8,128)(2,1)S(1)}, bf16[1024,1024]{1,0:T(8,128)(2,1)}, u32[]{:S(2)}) copy-start(bf16[1024,1024]{1,0:T(8,128)(2,1)} %refs_1_.1) | copy-start | bytes 6291460
  2.2 1.2 %copy-start.1 = (bf16[1024,512]{1,0:T(8,128)(2,1)S(1)}, bf16[1024,512]{1,0:T(8,128)(2,1)}, u32[]{:S(2)}) copy-start(bf16[1024,512]{1,0:T(8,128)(2,1)} %refs_2_.1) | copy-start | bytes 3145732
  3.5 9.9 %copy-start.5 = (bf16[8,1024]{1,0:T(8,128)(2,1)S(1)}, bf16[8,1024]{1,0:T(8,128)(2,1)}, u32[]{:S(2)}) copy-start(bf16[8,1024]{1,0:T(8,128)(2,1)} %tokens_ref.1) | copy-start | bytes 49156
  3.5 9.9 %copy-start.7 = (f32[1024]{0:T(1024)S(1)}, f32[1024]{0:T(1024)}, u32[]{:S(2)}) copy-start(f32[1024]{0:T(1024)} %param.48) | copy-start | bytes 12292
  8.6 4.8 %collective-permute-start = (bf16[8,1024]{1,0:T(8,128)(2,1)S(1)}, bf16[8,1024]{1,0:T(8,128)(2,1)S(1)}, u32[]{:S(2)}, u32[]{:S(2)}) collective-permute-start(bf16[8,1024]{1,0:T(8,128)(2,1)S(1)} %get-tuple-element.16.own_ref), channel_id=1, source_target_pairs={{0,1},{1,0},{2,3},{3,2},{4,5},{5,4},{6,7},{7,6},{8,9},{9,8},{10,11... | collective-permute-start | bytes 49160 | tf_op jit(solution)/shard_map/ppermute | solution.py:403
  14.1 13.7 %all-to-all-start = ((bf16[8,8,1024]{2,1,0:T(8,128)(2,1)}), bf16[8,8,1024]{2,1,0:T(8,128)(2,1)S(1)}, u32[]{:S(2)}, u32[]{:S(2)}) async-start(bf16[8,8,1024]{2,1,0:T(8,128)(2,1)} %bitcast.12), calls=%async_computation | async-start | bytes 262144 | tf_op jit(solution)/shard_map/all_to_all | solution.py:422
  20.4 20.9 %copy-start.2 = (bf16[1,1024,256]{2,1,0:T(8,128)(2,1)S(1)}, bf16[1,1024,256]{2,1,0:T(8,128)(2,1)}, u32[]{:S(2)}) copy-start(bf16[1,1024,256]{2,1,0:T(8,128)(2,1)} %gate_ref.3) | copy-start | bytes 1572868
  20.4 20.9 %copy-start.3 = (bf16[1,1024,256]{2,1,0:T(8,128)(2,1)S(1)}, bf16[1,1024,256]{2,1,0:T(8,128)(2,1)}, u32[]{:S(2)}) copy-start(bf16[1,1024,256]{2,1,0:T(8,128)(2,1)} %up_ref.3) | copy-start | bytes 1572868
  20.5 20.9 %copy-start.4 = (bf16[1,256,1024]{2,1,0:T(8,128)(2,1)S(1)}, bf16[1,256,1024]{2,1,0:T(8,128)(2,1)}, u32[]{:S(2)}) copy-start(bf16[1,256,1024]{2,1,0:T(8,128)(2,1)} %down_ref.1) | copy-start | bytes 1572868
  20.5 20.8 %copy-start.6 = (bf16[1024]{0:T(1024)(128)(2,1)S(1)}, bf16[1024]{0:T(1024)(128)(2,1)}, u32[]{:S(2)}) copy-start(bf16[1024]{0:T(1024)(128)(2,1)} %branch_ref.1) | copy-start | bytes 6148
  27.8 13.5 %all-to-all-start.1 = ((bf16[16,64,128]{2,1,0:T(8,128)(2,1)}), bf16[16,64,128]{2,1,0:T(8,128)(2,1)S(1)}, u32[]{:S(2)}, u32[]{:S(2)}) async-start(bf16[16,64,128]{2,1,0:T(8,128)(2,1)} %pack.1), calls=%async_computation.1 | async-start | bytes 524288 | tf_op jit(solution)/shard_map/all_to_all | solution.py:345
  31.3 1.4 %collective-permute-start.1 = (bf16[64,1024]{1,0:T(8,128)(2,1)S(1)}, bf16[64,1024]{1,0:T(8,128)(2,1)S(1)}, u32[]{:S(2)}, u32[]{:S(2)}) collective-permute-start(bf16[64,1024]{1,0:T(8,128)(2,1)S(1)} %bitcast.21), channel_id=1, source_target_pairs={{0,2},{2,0},{4,6},{6,4},{8,10},{10,8},{12,14},{14,12},{16,18},{18,... | collective-permute-start | bytes 393224 | tf_op jit(solution)/shard_map/ppermute | solution.py:425
  42.2 1.4 %collective-permute-start.2 = (bf16[128,512]{1,0:T(8,128)(2,1)S(1)}, bf16[128,512]{1,0:T(8,128)(2,1)S(1)}, u32[]{:S(2)}, u32[]{:S(2)}) collective-permute-start(bf16[128,512]{1,0:T(8,128)(2,1)S(1)} %get-tuple-element.19), channel_id=1, source_target_pairs={{0,2},{2,0},{4,6},{6,4},{8,10},{10,8},{12,14},{14,12},{16,18},{18,... | collective-permute-start | bytes 393224 | tf_op jit(solution)/shard_map/ppermute | solution.py:443
  44.3 11.6 %all-to-all-start.2 = ((bf16[16,8,512]{2,1,0:T(8,128)(2,1)}), bf16[16,8,512]{2,1,0:T(8,128)(2,1)S(1)}, u32[]{:S(2)}, u32[]{:S(2)}) async-start(bf16[16,8,512]{2,1,0:T(8,128)(2,1)} %bitcast.15), calls=%async_computation.2 | async-start | bytes 262144 | tf_op jit(solution)/shard_map/all_to_all | solution.py:445

commit v4 on v3

--- a/solution.py
+++ b/solution.py
@@ -1,5 +1,4 @@
 import functools
-import math
 
 import jax
 import jax.numpy as jnp
@@ -16,7 +15,7 @@
 SMEM = pl.BlockSpec(memory_space=pltpu.SMEM)
 HBM = pl.BlockSpec(memory_space=pltpu.HBM)
 MIB = 1 << 20
-LONG = pl.CostEstimate(flops=10**10, bytes_accessed=10**6, transcendentals=0)
+LANES = 128
 
 
 def dot(left, right):
@@ -54,39 +53,42 @@
     return values.transpose(1, 0, 2)
 
 
-def pack_kernel(gate_ref, up_ref, down_ref, ids_ref, weights_ref, out_ref, *, dests):
-    rows, hidden = gate_ref.shape
-    share = hidden // dests
-    lanes = out_ref.shape[2]
-    seqs, top_count = ids_ref.shape
-    gate = gate_ref[...].astype(f32)
-    up = up_ref[...].astype(f32)
-    down = down_ref[...].astype(f32)
-    ids = ids_ref[...]
-    weights = weights_ref[...]
-    expert = lax.broadcasted_iota(jnp.int32, (seqs, dests), 1)
-    weight_of = jnp.zeros((seqs, dests), f32)
-    for k in range(top_count):
-        weight_of += jnp.where(ids[:, k : k + 1] == expert, weights[:, k : k + 1], 0.0)
-    high = weight_of.astype(bf16).astype(f32)
-    low = weight_of - high
-    if rows > seqs:
-        rest = jnp.zeros((rows - seqs, dests), f32)
-        high = jnp.concatenate((high, rest), axis=0)
-        low = jnp.concatenate((low, rest), axis=0)
-    for j in range(dests):
-        part = slice(j * share, (j + 1) * share)
-        block = [gate[:, part], up[:, part], down[:, part], high[:, j : j + 1], low[:, j : j + 1]]
-        spare = lanes - 3 * share - 2
-        if spare:
-            block.append(jnp.zeros((rows, spare), f32))
-        out_ref[j] = jnp.concatenate(block, axis=1).astype(bf16)
+def fold_of(rows, share):
+    fold = 1
+    while 4 * fold * share <= LANES and rows % (32 * fold) == 0:
+        fold *= 2
+    return fold
+
+
+def packed_rows(rows, share, seqs):
+    fold = fold_of(rows, share)
+    return rows // fold + rows // (2 * fold) + seqs
+
+
+def side_by_side(values, fold):
+    rows, width = values.shape
+    count, stride = rows // fold, LANES // fold
+    pieces = []
+    for k in range(fold):
+        pieces.append(values[k * count : (k + 1) * count])
+        if stride > width:
+            pieces.append(jnp.zeros((count, stride - width), f32))
+    return jnp.concatenate(pieces, axis=1)
+
+
+def pack(gate, up, down, ids, weights, dest, fold):
+    seqs, _ = ids.shape
+    weight = jnp.sum(jnp.where(ids == dest, weights, 0.0), axis=1, keepdims=True)
+    high = weight.astype(bf16).astype(f32)
+    tail = jnp.concatenate((high, weight - high, jnp.zeros((seqs, LANES - 2), f32)), axis=1)
+    both = side_by_side(jnp.concatenate((gate, up), axis=1), fold)
+    return jnp.concatenate((both, side_by_side(down, 2 * fold), tail), axis=0)
 
 
 def mixer_kernel(*refs, n_tp, held):
-    tp_ref, w_x, w_b = refs[:3]
-    sources = refs[3 : 3 + held]
-    part_ref, scaled_ref, key_ref, decay_ref = refs[3 + held : 7 + held]
+    place_ref = refs[0]
+    sources = refs[1 : 1 + held]
+    part_ref, scaled_ref, key_ref, decay_ref, own_ref, other_ref = refs[1 + held : 7 + held]
     conv_outs = refs[7 + held : 10 + held]
     targets = refs[10 + held : 10 + 2 * held]
     conv_x_next, conv_b_next, conv_c_next = conv_next = refs[10 + 2 * held : 13 + 2 * held]
@@ -105,6 +107,13 @@
         conv_x_ref,
         conv_b_ref,
         conv_c_ref,
+        gate_ref,
+        up_ref,
+        down_ref,
+        ids_ref,
+        weights_ref,
+        w_x,
+        w_b,
         w_c,
         w_z,
         w_out,
@@ -117,23 +126,39 @@
     width = channels // groups
     copy = pltpu.make_async_copy
     loads = [copy(sources[i], targets[i], in_sems.at[i]) for i in range(held - 1)]
-    *small_loads, load_c, load_z, load_out = loads
+    *small_loads, load_x, load_b, load_c, load_z, load_out = loads
     state_loads = [copy(sources[-1].at[s], state.at[s], state_sems.at[s]) for s in range(seqs)]
     stores = [copy(conv_next[i], conv_outs[i], out_sems.at[i]) for i in range(3)]
-    for load in [*small_loads, load_c, *state_loads, load_z, load_out]:
+    for load in [*small_loads, load_x, load_b, load_c, *state_loads, load_z, load_out]:
         load.start()
     for load in small_loads:
         load.wait()
 
     normed = rms_rows(tokens_ref[...].astype(f32), gain_ref[...]).astype(bf16)
     dt_all = dot_nt(normed, w_dt_ref[...])
-    own = tp_ref[0]
+    own = place_ref[0]
     dt_raw = jnp.zeros((seqs, heads), f32)
     for i in range(n_tp):
         dt_raw += jnp.where(own == i, dt_all[:, i * heads : (i + 1) * heads], 0.0)
     shifted = dt_raw + dt_bias_ref[...]
     step = jnp.maximum(shifted, 0.0) + jnp.log1p(jnp.exp(-jnp.abs(shifted)))
     decay = jnp.exp(-step * jnp.exp(a_log_ref[...]))
+
+    first = place_ref[1] == 0
+    gate = gate_ref[...].astype(f32)
+    up = up_ref[...].astype(f32)
+    down = down_ref[...].astype(f32)
+    ids = ids_ref[...]
+    weights = weights_ref[...]
+    share = gate.shape[1] // (2 * own_ref.shape[0])
+    fold = fold_of(gate.shape[0], share)
+    for chip in range(own_ref.shape[0]):
+        even, odd = [
+            pack(*[value[:, j * share : (j + 1) * share] for value in (gate, up, down)], ids, weights, j, fold)
+            for j in (2 * chip, 2 * chip + 1)
+        ]
+        own_ref[chip] = jnp.where(first, even, odd).astype(bf16)
+        other_ref[chip] = jnp.where(first, odd, even).astype(bf16)
 
     def short_conv(previous_ref, fresh, taps_ref, out_ref):
         taps = taps_ref[...].astype(f32)
@@ -147,7 +172,9 @@
     def projected(ref):
         return dot(normed, ref[...]).astype(bf16).astype(f32)
 
+    load_x.wait()
     xs = short_conv(conv_x_ref, projected(w_x), taps_x_ref, conv_x_next)
+    load_b.wait()
     bs = short_conv(conv_b_ref, projected(w_b), taps_b_ref, conv_b_next)
     load_c.wait()
     cs = short_conv(conv_c_ref, projected(w_c), taps_c_ref, conv_c_next)
@@ -209,70 +236,146 @@
         store.wait()
 
 
-def norm_kernel(tokens_ref, own_ref, other_ref, gain_ref, spread_ref, residual_ref):
-    seqs = tokens_ref.shape[0]
+def norm_kernel(
+    tokens_ref, own_ref, other_ref, gain_ref, kept_ref, swapped_ref, spread_ref, residual_ref
+):
+    _, model = tokens_ref.shape
+    chips, block, _ = kept_ref.shape
     summed = own_ref[...].astype(f32) + other_ref[...].astype(f32)
     residual = (tokens_ref[...].astype(f32) + summed).astype(bf16)
     residual_ref[...] = residual
-    normed = rms_rows(residual.astype(f32), gain_ref[...]).astype(bf16)
-    for j in range(spread_ref.shape[0] // seqs):
-        spread_ref[j * seqs : (j + 1) * seqs] = normed
-
-
-def experts_kernel(
-    core_ref,
-    own_ref,
-    other_ref,
-    packed_ref,
+    normed = rms_rows(residual.astype(f32), gain_ref[...])
+    tiles = jnp.concatenate(
+        [normed[:, k * LANES : (k + 1) * LANES] for k in range(model // LANES)], axis=0
+    ).astype(bf16)
+    count = tiles.shape[0]
+    for chip in range(chips):
+        spread_ref[chip, :count] = tiles
+        spread_ref[chip, count : count + block] = kept_ref[chip]
+        spread_ref[chip, count + block :] = swapped_ref[chip]
+
+
+def token_rows(tiles_ref, seqs, model):
+    rows = []
+    for chip in range(tiles_ref.shape[0]):
+        tiles = tiles_ref[chip, : seqs * model // LANES]
+        rows.append(
+            jnp.concatenate(
+                [tiles[k * seqs : (k + 1) * seqs] for k in range(model // LANES)], axis=1
+            )
+        )
+    return jnp.concatenate(rows, axis=0)
+
+
+def branches(rows, table, gate_ref, up_ref, down_ref, branch_ref, wide, back, share):
+    active = (silu(dot(rows, gate_ref[0])) * dot(rows, up_ref[0])).astype(bf16)
+    routed = dot(active, down_ref[0])
+    hidden = dot(rows, wide)
+    lane = lax.broadcasted_iota(jnp.int32, hidden.shape, 1)
+    dense = silu(hidden) * pltpu.roll(hidden, LANES - share, 1)
+    dense = jnp.where(lane < share, dense, 0.0).astype(bf16)
+    dense_out = dot_nt(dense, back)
+    branch = sigmoid(
+        jnp.sum(rows.astype(f32) * branch_ref[...].astype(f32)[None], axis=1, keepdims=True)
+    )
+    weight = jnp.sum(jnp.where(lane < 2, table, 0.0), axis=1, keepdims=True)
+    return weight * routed + branch * dense_out
+
+
+def store_parts(out_ref, result, seqs, n_tp):
+    half = result.shape[1] // n_tp
+    for i in range(result.shape[0] // seqs):
+        for q in range(n_tp):
+            place = (i * n_tp + q) * seqs
+            value = result[i * seqs : (i + 1) * seqs, q * half : (q + 1) * half]
+            out_ref[place : place + seqs] = value.astype(out_ref.dtype)
+
+
+def own_experts_kernel(
+    place_ref,
+    got_ref,
     gate_ref,
     up_ref,
     down_ref,
     branch_ref,
     keep_ref,
+    wide_ref,
+    back_ref,
+    table_ref,
+    *,
+    share,
+    seqs,
+    n_tp,
+):
+    model = wide_ref.shape[0]
+    chips, total, _ = got_ref.shape
+    rows = model // (2 * chips)
+    count = seqs * model // LANES
+    block = (total - count) // 2
+    fold = fold_of(rows, share)
+    core = place_ref[1]
+    wide_rows, back_rows = rows // fold, rows // (2 * fold)
+    for chip in range(chips):
+        for parity in range(2):
+            start = count + jnp.where(core == parity, 0, block)
+            start = pl.multiple_of(start, 8)
+            source = (2 * chip + parity) * rows
+            wide = got_ref[chip, pl.ds(start, wide_rows)].astype(f32)
+            for k in range(fold):
+                moved = pltpu.roll(wide, (LANES - k * LANES // fold) % LANES, 1) if k else wide
+                place = source + k * wide_rows
+                wide_ref[place : place + wide_rows] = moved.astype(bf16)
+            back = got_ref[chip, pl.ds(pl.multiple_of(start + wide_rows, 8), back_rows)].astype(f32)
+            for k in range(2 * fold):
+                moved = pltpu.roll(back, LANES - k * LANES // (2 * fold), 1) if k else back
+                place = source + k * back_rows
+                back_ref[place : place + back_rows] = moved.astype(bf16)
+    tail = count + block - seqs
+    table = jnp.concatenate([got_ref[i, tail : tail + seqs].astype(f32) for i in range(chips)], axis=0)
+    table_ref[...] = jnp.concatenate(
+        [got_ref[i, total - seqs :].astype(f32) for i in range(chips)], axis=0
+    )
+    result = branches(
+        token_rows(got_ref, seqs, model),
+        table,
+        gate_ref,
+        up_ref,
+        down_ref,
+        branch_ref,
+        wide_ref[...],
+        back_ref[...],
+        share,
+    )
+    store_parts(keep_ref, result, seqs, n_tp)
+
+
+def other_experts_kernel(
+    got_ref,
+    gate_ref,
+    up_ref,
+    down_ref,
+    branch_ref,
+    wide_ref,
+    back_ref,
+    table_ref,
     send_ref,
     *,
     share,
     seqs,
     n_tp,
 ):
-    blocks, block_rows, lanes = packed_ref.shape
-    core = core_ref[0]
-    half_count, model = own_ref.shape
-    count = 2 * half_count
-    rows = jnp.concatenate((own_ref[...], other_ref[...]), axis=0)
-    active = (silu(dot(rows, gate_ref[0])) * dot(rows, up_ref[0])).astype(bf16)
-    routed = dot(active, down_ref[0])
-    packed = packed_ref[...].reshape(blocks * block_rows, lanes)
-    hidden = dot(rows, packed)
-    lane = lax.broadcasted_iota(jnp.int32, (count, lanes), 1)
-    dense = silu(pltpu.roll(hidden, 2 * share, 1)) * pltpu.roll(hidden, share, 1)
-    chosen = (lane >= 2 * share) & (lane < 3 * share)
-    dense = jnp.where(chosen, dense, 0.0).astype(bf16)
-    dense_out = dot_nt(dense, packed)
-    branch = sigmoid(
-        jnp.sum(rows.astype(f32) * branch_ref[...].astype(f32)[None], axis=1, keepdims=True)
-    )
-    table = jnp.concatenate(
-        [
-            packed_ref[2 * i + place, :seqs].astype(f32)
-            for place in (core, 1 - core)
-            for i in range(blocks // 2)
-        ],
-        axis=0,
-    )
-    weight = jnp.sum(
-        jnp.where((lane >= 3 * share) & (lane < 3 * share + 2), table, 0.0), axis=1, keepdims=True
-    )
-    result = weight * routed + branch * dense_out
-    half = model // n_tp
-    for i in range(blocks // 2):
-        for q in range(n_tp):
-            place = (i * n_tp + q) * seqs
-            part = slice(q * half, (q + 1) * half)
-            keep_ref[place : place + seqs] = result[i * seqs : (i + 1) * seqs, part]
-            send_ref[place : place + seqs] = result[
-                half_count + i * seqs : half_count + (i + 1) * seqs, part
-            ].astype(bf16)
+    result = branches(
+        token_rows(got_ref, seqs, wide_ref.shape[0]),
+        table_ref[...],
+        gate_ref,
+        up_ref,
+        down_ref,
+        branch_ref,
+        wide_ref[...],
+        back_ref[...],
+        share,
+    )
+    store_parts(send_ref, result, seqs, n_tp)
 
 
 def add_kernel(left_ref, right_ref, out_ref):
@@ -326,24 +429,15 @@
     seqs, model = tokens.shape
     n_ep = lax.axis_size("ep")
     n_tp = lax.axis_size("tp")
-    core_index = (lax.axis_index("ep").astype(jnp.int32) % 2)[None]
-    tp_index = lax.axis_index("tp").astype(jnp.int32)[None]
+    place = jnp.stack((lax.axis_index("tp"), lax.axis_index("ep") % 2)).astype(jnp.int32)
     sds = jax.ShapeDtypeStruct
 
     rows, hidden = dense_gate.shape
     share = hidden // n_ep
-    lanes = 128 * math.ceil((3 * share + 2) / 128)
-    packed = pl.pallas_call(
-        functools.partial(pack_kernel, dests=n_ep),
-        out_shape=pltpu.HBM((n_ep, rows, lanes), bf16),
-        in_specs=[VMEM] * 5,
-        out_specs=VMEM,
-        compiler_params=pltpu.CompilerParams(vmem_limit_bytes=4 * MIB),
-        cost_estimate=LONG,
-        name="pack",
-    )(*map(in_hbm, (dense_gate, dense_up, dense_down.T, route_ids, route_weights)))
-    packed = lax.all_to_all(packed, "ep", split_axis=0, concat_axis=0, tiled=True)
-
+    chips = n_ep // 2
+    block = packed_rows(rows, share, seqs)
+    groups = [[2 * chip + core for chip in range(chips)] for core in range(2)]
+    swap = [(i, i ^ 1) for i in range(n_ep)]
     held = (
         tokens,
         norm1_gain[None],
@@ -358,22 +452,31 @@
         taps_first(conv_x),
         taps_first(conv_b),
         taps_first(conv_c),
+        dense_gate,
+        dense_up,
+        dense_down.T,
+        route_ids,
+        route_weights,
+        w_x,
+        w_b,
         w_c,
         w_z,
         w_out,
         ssm_state,
     )
-    part, scaled, keys, decay, conv_x_next, conv_b_next, conv_c_next = pl.pallas_call(
+    part, scaled, keys, decay, kept, parted, conv_x_next, conv_b_next, conv_c_next = pl.pallas_call(
         functools.partial(mixer_kernel, n_tp=n_tp, held=len(held)),
         out_shape=(
             sds((seqs, model), bf16),
             sds((seqs, w_x.shape[1]), f32),
             sds((seqs, w_b.shape[1]), f32),
             sds((seqs, ssm_state.shape[1]), f32),
+            sds((chips, block, LANES), bf16),
+            sds((chips, block, LANES), bf16),
             *[sds(taps_first(value).shape, bf16) for value in (conv_x, conv_b, conv_c)],
         ),
-        in_specs=[SMEM] + [VMEM] * 2 + [HBM] * len(held),
-        out_specs=(VMEM,) * 4 + (HBM,) * 3,
+        in_specs=[SMEM] + [HBM] * len(held),
+        out_specs=(VMEM,) * 6 + (HBM,) * 3,
         scratch_shapes=[pltpu.VMEM(value.shape, value.dtype) for value in held]
         + [pltpu.VMEM(taps_first(value).shape, bf16) for value in (conv_x, conv_b, conv_c)]
         + [
@@ -383,7 +486,7 @@
         ],
         compiler_params=pltpu.CompilerParams(vmem_limit_bytes=20 * MIB),
         name="mixer",
-    )(tp_index, w_x, w_b, *map(in_hbm, held))
+    )(place, *map(in_hbm, held))
 
     state_next = pl.pallas_call(
         advance_kernel,
@@ -408,34 +511,48 @@
             total = total + gathered[i]
         other = total - part.astype(f32)
 
+    swapped = lax.ppermute(parted, "ep", swap)
+    tile_rows = seqs * model // LANES
     spread, residual = pl.pallas_call(
         norm_kernel,
-        out_shape=(sds((n_ep // 2 * seqs, model), bf16), sds((seqs, model), bf16)),
-        in_specs=[VMEM] * 4,
+        out_shape=(sds((chips, tile_rows + 2 * block, LANES), bf16), sds((seqs, model), bf16)),
+        in_specs=[VMEM] * 6,
         out_specs=(VMEM, VMEM),
         compiler_params=pltpu.CompilerParams(vmem_limit_bytes=4 * MIB),
-        cost_estimate=LONG,
         name="norm",
-    )(tokens, part, other, norm2_gain[None])
-    groups = [[2 * chip + core for chip in range(n_ep // 2)] for core in range(2)]
-    swap = [(i, i ^ 1) for i in range(n_ep)]
-    own_core = lax.all_to_all(
+    )(tokens, part, other, norm2_gain[None], kept, swapped)
+    got = lax.all_to_all(
         spread, "ep", split_axis=0, concat_axis=0, tiled=True, axis_index_groups=groups
     )
-    other_core = lax.ppermute(own_core, "ep", swap)
-
-    blocks = (n_ep // 2 * n_tp * seqs, model // n_tp)
-    keep, send = pl.pallas_call(
-        functools.partial(experts_kernel, share=share, seqs=seqs, n_tp=n_tp),
-        out_shape=(sds(blocks, f32), sds(blocks, bf16)),
-        in_specs=[SMEM] + [VMEM] * 7,
-        out_specs=(VMEM, VMEM),
+    got_other = lax.ppermute(got, "ep", swap)
+
+    parts_shape = (chips * n_tp * seqs, model // n_tp)
+    sizes = dict(share=share, seqs=seqs, n_tp=n_tp)
+    expert_weights = (exp_gate, exp_up, exp_down, branch_gate)
+    keep, wide, back, table = pl.pallas_call(
+        functools.partial(own_experts_kernel, **sizes),
+        out_shape=(
+            sds(parts_shape, f32),
+            sds((model, LANES), bf16),
+            sds((model, LANES), bf16),
+            sds((chips * seqs, LANES), f32),
+        ),
+        in_specs=[SMEM] + [VMEM] * 5,
+        out_specs=(VMEM,) * 4,
         compiler_params=pltpu.CompilerParams(vmem_limit_bytes=12 * MIB),
-        name="experts",
-    )(core_index, own_core, other_core, packed, exp_gate, exp_up, exp_down, branch_gate)
+        name="own_experts",
+    )(place, got, *expert_weights)
+    send = pl.pallas_call(
+        functools.partial(other_experts_kernel, **sizes),
+        out_shape=sds(parts_shape, bf16),
+        in_specs=[VMEM] * 8,
+        out_specs=VMEM,
+        compiler_params=pltpu.CompilerParams(vmem_limit_bytes=12 * MIB),
+        name="other_experts",
+    )(got_other, *expert_weights, wide, back, table)
     outgoing = pl.pallas_call(
         add_kernel,
-        out_shape=sds(blocks, bf16),
+        out_shape=sds(parts_shape, bf16),
         in_specs=[VMEM] * 2,
         out_specs=VMEM,
         compiler_params=pltpu.CompilerParams(vmem_limit_bytes=4 * MIB),
@@ -458,7 +575,7 @@
         out_specs=VMEM,
         compiler_params=pltpu.CompilerParams(vmem_limit_bytes=4 * MIB),
         name="total",
-    )(tp_index, parts, residual)
+    )(place, parts, residual)
     return (
         mixed,
         state_next,

time: 57 us -> 47.6 us (0.84)
  blocking collectives: 0 us -> 17.1 us
  waiting for transfers between devices: 21.7 us -> 6.87 us
  starting transfers between devices: 17.1 us -> 7.5 us
  local copies, waits for them, and re-layouts: 2.84 us -> 0.03 us
  Pallas kernels: 14.1 us -> 15 us
    all_to_all x0 -> x1, blocking collectives: none -> 17.1 us  [body(): lax.all_to_all(spread, 'ep', split_axis=0, concat_axis=0, tiled=True, axi...]
    all_to_all x2 -> x0, waiting for transfers between devices: 13.8 us -> none  [the longest x1 8.56 us: body(): lax.all_to_all(packed, 'ep', split_axis=0, concat_axis=0, tiled=True)]
    all_to_all x2 -> x0, starting transfers between devices: 9.9 us -> none  [the longest x1 6.36 us: body(): lax.all_to_all(spread, 'ep', split_axis=0, concat_axis=0, tiled=True, axi...]
    unnamed x16 -> x12, local copies, waits for them, and re-layouts: 2.84 us -> 0.03 us
    pallas_call x1, Pallas kernels: 5.09 us -> 6.87 us  [body(): pl.pallas_call(functools.partial(mixer_kernel, n_tp=n_tp, held=len(held))...]
    pallas_call x4, Pallas kernels: 4.31 us -> 2.88 us  [the longest x1 1.33 us: body(): pl.pallas_call(functools.partial(own_experts_kernel, **sizes), out_shape=...]
    ppermute x1 -> x2, waiting for transfers between devices: 1.12 us -> 0.31 us  [the longest x1 0.31 us: body(): got_other = lax.ppermute(got, 'ep', swap)]
  transfers between devices with their start and end apart: 6 -> 5, of which waited for: 6 -> 4; matrix products, arithmetic and copies ran while one was open for 0% -> 0% of each run, Pallas kernels for 11% -> 11%
where the time goes in v4:
time: 47.6 us; the launch traced here: 47.4 us
  blocking collectives  17.1 us (36%)
  Pallas kernels  15 us (32%)
  starting transfers between devices  7.5 us (16%)
  waiting for transfers between devices  6.87 us (14%)
  between operations  0.74 us (2%)
    all_to_all x1, blocking collectives, body(): lax.all_to_all(spread, 'ep', split_axis=0, concat_axis=0, tiled=True, axi...  17.1 us
    pallas_call x1, Pallas kernels, body(): pl.pallas_call(functools.partial(mixer_kernel, n_tp=n_tp, held=len(held))...  6.87 us
    all_to_all x1, starting transfers between devices, body(): lax.all_to_all(outgoing, ('ep', 'tp'), split_axis=0, concat_axis=0, tiled...  4.12 us
    pallas_call x1, Pallas kernels, body(): pl.pallas_call(advance_kernel, out_shape=sds(ssm_state.shape, f32), in_sp...  4.1 us
    all_to_all x1, waiting for transfers between devices, body(): lax.all_to_all(outgoing, ('ep', 'tp'), split_axis=0, concat_axis=0, tiled...  3.69 us
    ppermute x1, starting transfers between devices, body(): other = lax.ppermute(part, 'tp', [(0, 1), (1, 0)])  2.55 us
    ppermute x1, waiting for transfers between devices, body(): other = lax.ppermute(part, 'tp', [(0, 1), (1, 0)])  1.72 us
    pallas_call x1, Pallas kernels, body(): pl.pallas_call(functools.partial(own_experts_kernel, **sizes), out_shape=...  1.33 us
  transfers between devices with their start and end apart: 5, of which 4 were waited for; matrix products, arithmetic and copies ran while one was open for 0% of the time, Pallas kernels for 11%

profile of v4, /device:TPU:0, one launch (start us, length us, event | category | flops | bytes accessed | tf_op | source)
XLA Modules:
  0.0 47.4 jit_solution(11365847508990758836)
XLA Ops:
  0.6 0.1 pad_add_fusion.refs_0_.place_ref.tp_ref
  0.7 0.0 copy-start.3
  0.7 0.0 copy-start.5
  0.7 0.0 copy-start
  0.7 0.0 copy-start.1
  0.7 0.0 copy-start.2
  0.7 0.0 copy-start.4
  0.8 6.9 %mixer.1 = (bf16[8,1024]{1,0:T(8,128)(2,1)S(1)}, f32[8,1024]{1,0:T(8,128)S(1)}, f32[8,512]{1,0:T(8,128)S(1)}, f32[8,16]{1,0:T(8,128)S(1)}, bf16[8,56,128]{2,1,0:...) custom-call(s32[2]{0:T(128)S(1)} %pad_add_fusion.refs_0_.place_ref.t, ...), custom_call_target="tpu_custom_call" | custom-call | tf_op jit(solution)/shard_map/mixer/pallas_call | solution.py:467
  7.6 0.6 %collective-permute-start.1 = (bf16[8,56,128]{2,1,0:T(8,128)(2,1)S(1)}, bf16[8,56,128]{2,1,0:T(8,128)(2,1)S(1)}, u32[]{:S(2)}, u32[]{:S(2)}) collective-permute-start(bf16[8,56,128]{2,1,0:T(8,128)(2,1)S(1)} %get-tuple-element.22), channel_id=1, source_target_pairs={{0,2},{2,0},{4,6},{6,4},{8,10},{10,8},{12,14},{14,12},{16,18},{18,... | collective-permute-start | bytes 344072 | tf_op jit(solution)/shard_map/ppermute | solution.py:514
  8.2 2.6 %collective-permute-start = (bf16[8,1024]{1,0:T(8,128)(2,1)S(1)}, bf16[8,1024]{1,0:T(8,128)(2,1)S(1)}, u32[]{:S(2)}, u32[]{:S(2)}) collective-permute-start(bf16[8,1024]{1,0:T(8,128)(2,1)S(1)} %get-tuple-element.20.own_ref), channel_id=1, source_target_pairs={{0,1},{1,0},{2,3},{3,2},{4,5},{5,4},{6,7},{7,6},{8,9},{9,8},{10,11... | collective-permute-start | bytes 49160 | tf_op jit(solution)/shard_map/ppermute | solution.py:506
  10.7 1.7 %collective-permute-done.other_ref = bf16[8,1024]{1,0:T(8,128)(2,1)S(1)} collective-permute-done((bf16[8,1024]{1,0:T(8,128)(2,1)S(1)}, bf16[8,1024]{1,0:T(8,128)(2,1)S(1)}, u32[]{:S(2)}, u32[]{:S(2)}) %collective-permute-start) | collective-permute-done | bytes 16416 | tf_op jit(solution)/shard_map/ppermute | solution.py:506
  12.5 0.0 collective-permute-done.1.swapped_ref
  12.5 0.0 copy-done.3
  12.5 0.0 copy-done.5
  12.5 0.1 norm.1
  12.6 17.1 %all_to_all.16.got_ref = bf16[8,176,128]{2,1,0:T(8,128)(2,1)S(1)} all-to-all(bf16[8,176,128]{2,1,0:T(8,128)(2,1)S(1)} %get-tuple-element.23), channel_id=1, replica_groups={{0,4,8,12,16,20,24,28},{2,6,10,14,18,22,26,30},{1,5,9,13,17,21,25,29},{..., dimensions={0} | all-to-all | bytes 720896 | tf_op jit(solution)/shard_map/all_to_all | solution.py:524
  29.7 0.0 collective-permute-start.2
  29.7 0.0 copy-done
  29.7 0.0 copy-done.1
  29.7 0.0 copy-done.2
  29.7 0.0 copy-done.4
  29.8 1.3 %own_experts.1 = (f32[128,512]{1,0:T(8,128)S(1)}, bf16[1024,128]{1,0:T(8,128)(2,1)S(1)}, bf16[1024,128]{1,0:T(8,128)(2,1)S(1)}, f32[64,128]{1,0:T(8,128)S(1)}) custom-call(s32[2]{0:T(128)S(1)} %pad_add_fusion.refs_0_.place_ref.tp_ref, bf16[8,176,128]{2,1,0:T(8,128)(2,1)S(1)} %all_to_all.16.got_ref, bf16[1,1024,256]{2,1,0:T(8,128)(2,1)S(1)} %copy-done, ...), custom_call_target="tpu_custom_call" | custom-call | tf_op jit(solution)/shard_map/own_experts/pallas_call | solution.py:532
  31.1 0.3 collective-permute-done.2.got_ref
  31.4 0.8 %other_experts.1 = bf16[128,512]{1,0:T(8,128)(2,1)S(1)} custom-call(bf16[8,176,128]{2,1,0:T(8,128)(2,1)S(1)} %collective-permute-done.2.got_ref, bf16[1,1024,256]{2,1,0:T(8,128)(2,1)S(1)} %copy-done, bf16[1,1024,256]{2,1,0:T(8,128)(2,1)S(1)} %copy-done.1, bf16[1,256,1024]{2,1,0:T(8,128)(2,1)S(1)} %copy-done.2, bf16[1024]{0:T(1024)(128)(2,1)S(1)} %copy-done.4, ...), custom_call_target="tpu_custom_call" | custom-call | tf_op jit(solution)/shard_map/other_experts/pallas_call | solution.py:545
  32.2 0.3 collective-permute-start.3
  32.4 1.1 %collective-permute-done.3.right_ref = bf16[128,512]{1,0:T(8,128)(2,1)S(1)} collective-permute-done((bf16[128,512]{1,0:T(8,128)(2,1)S(1)}, bf16[128,512]{1,0:T(8,128)(2,1)S(1)}, u32[]{:S(2)}, u32[]{:S(2)}) %collective-permute-start.3) | collective-permute-done | bytes 131104 | tf_op jit(solution)/shard_map/ppermute | solution.py:560
  33.6 0.7 %add.8 = bf16[128,512]{1,0:T(8,128)(2,1)} custom-call(f32[128,512]{1,0:T(8,128)S(1)} %get-tuple-element.24.left_ref, bf16[128,512]{1,0:T(8,128)(2,1)S(1)} %collective-permute-done.3.right_ref), custom_call_target="tpu_custom_call" | custom-call | tf_op jit(solution)/shard_map/add/pallas_call | solution.py:553
  34.3 4.1 %all-to-all-start.1 = ((bf16[16,8,512]{2,1,0:T(8,128)(2,1)}), bf16[16,8,512]{2,1,0:T(8,128)(2,1)S(1)}, u32[]{:S(2)}, u32[]{:S(2)}) async-start(bf16[16,8,512]{2,1,0:T(8,128)(2,1)} %bitcast.13), calls=%async_computation.1 | async-start | bytes 262144 | tf_op jit(solution)/shard_map/all_to_all | solution.py:562
  38.4 4.1 %advance.1 = f32[8,16,64,128]{3,2,1,0:T(8,128)} custom-call(f32[8,1024]{1,0:T(8,128)S(1)} %get-tuple-element.29.scaled_ref, f32[8,512]{1,0:T(8,128)S(1)} %get-tuple-element.30.key_ref, f32[8,16]{1,0:T(8,128)S(1)} %get-tuple-element.31.decay_ref, f32[8,16,64,128]{3,2,1,0:T(8,128)} %state_hbm.1), custom_call_target="tpu_custom_call" | custom-call | tf_op jit(solution)/shard_map/advance/pallas_call | solution.py:491
  42.5 3.7 %all-to-all-done.1 = bf16[16,8,512]{2,1,0:T(8,128)(2,1)S(1)} async-done(((bf16[16,8,512]{2,1,0:T(8,128)(2,1)}), bf16[16,8,512]{2,1,0:T(8,128)(2,1)S(1)}, u32[]{:S(2)}, u32[]{:S(2)}) %all-to-all-start.1) | async-done | bytes 131104 | tf_op jit(solution)/shard_map/all_to_all | solution.py:562
  46.2 1.2 %total.1 = bf16[8,512]{1,0:T(8,128)(2,1)} custom-call(s32[2]{0:T(128)S(1)} %pad_add_fusion.refs_0_.place_ref.tp_ref, bf16[128,512]{1,0:T(8,128)(2,1)S(1)} %bitcast.18, bf16[8,1024]{1,0:T(8,128)(2,1)S(1)} %get-tuple-element.28.residual_ref), custom_call_target="tpu_custom_call" | custom-call | tf_op jit(solution)/shard_map/total/pallas_call | solution.py:571
Async XLA Ops:
  0.7 11.7 %copy-start.3 = (bf16[8,1024]{1,0:T(8,128)(2,1)S(1)}, bf16[8,1024]{1,0:T(8,128)(2,1)}, u32[]{:S(2)}) copy-start(bf16[8,1024]{1,0:T(8,128)(2,1)} %tokens_ref.1) | copy-start | bytes 49156
  0.7 11.7 %copy-start.5 = (f32[1024]{0:T(1024)S(1)}, f32[1024]{0:T(1024)}, u32[]{:S(2)}) copy-start(f32[1024]{0:T(1024)} %param.48) | copy-start | bytes 12292
  0.7 29.0 %copy-start = (bf16[1,1024,256]{2,1,0:T(8,128)(2,1)S(1)}, bf16[1,1024,256]{2,1,0:T(8,128)(2,1)}, u32[]{:S(2)}) copy-start(bf16[1,1024,256]{2,1,0:T(8,128)(2,1)} %gate_ref.3) | copy-start | bytes 1572868
  0.7 29.0 %copy-start.1 = (bf16[1,1024,256]{2,1,0:T(8,128)(2,1)S(1)}, bf16[1,1024,256]{2,1,0:T(8,128)(2,1)}, u32[]{:S(2)}) copy-start(bf16[1,1024,256]{2,1,0:T(8,128)(2,1)} %up_ref.3) | copy-start | bytes 1572868
  0.7 29.0 %copy-start.2 = (bf16[1,256,1024]{2,1,0:T(8,128)(2,1)S(1)}, bf16[1,256,1024]{2,1,0:T(8,128)(2,1)}, u32[]{:S(2)}) copy-start(bf16[1,256,1024]{2,1,0:T(8,128)(2,1)} %down_ref.3) | copy-start | bytes 1572868
  0.7 29.0 %copy-start.4 = (bf16[1024]{0:T(1024)(128)(2,1)S(1)}, bf16[1024]{0:T(1024)(128)(2,1)}, u32[]{:S(2)}) copy-start(bf16[1024]{0:T(1024)(128)(2,1)} %branch_ref.3) | copy-start | bytes 6148
  7.6 4.8 %collective-permute-start.1 = (bf16[8,56,128]{2,1,0:T(8,128)(2,1)S(1)}, bf16[8,56,128]{2,1,0:T(8,128)(2,1)S(1)}, u32[]{:S(2)}, u32[]{:S(2)}) collective-permute-start(bf16[8,56,128]{2,1,0:T(8,128)(2,1)S(1)} %get-tuple-element.22), channel_id=1, source_target_pairs={{0,2},{2,0},{4,6},{6,4},{8,10},{10,8},{12,14},{14,12},{16,18},{18,... | collective-permute-start | bytes 344072 | tf_op jit(solution)/shard_map/ppermute | solution.py:514
  8.2 4.3 %collective-permute-start = (bf16[8,1024]{1,0:T(8,128)(2,1)S(1)}, bf16[8,1024]{1,0:T(8,128)(2,1)S(1)}, u32[]{:S(2)}, u32[]{:S(2)}) collective-permute-start(bf16[8,1024]{1,0:T(8,128)(2,1)S(1)} %get-tuple-element.20.own_ref), channel_id=1, source_target_pairs={{0,1},{1,0},{2,3},{3,2},{4,5},{5,4},{6,7},{7,6},{8,9},{9,8},{10,11... | collective-permute-start | bytes 49160 | tf_op jit(solution)/shard_map/ppermute | solution.py:506
  29.7 1.7 %collective-permute-start.2 = (bf16[8,176,128]{2,1,0:T(8,128)(2,1)S(1)}, bf16[8,176,128]{2,1,0:T(8,128)(2,1)S(1)}, u32[]{:S(2)}, u32[]{:S(2)}) collective-permute-start(bf16[8,176,128]{2,1,0:T(8,128)(2,1)S(1)} %all_to_all.16.got_ref), channel_id=1, source_target_pairs={{0,2},{2,0},{4,6},{6,4},{8,10},{10,8},{12,14},{14,12},{16,18},{18,... | collective-permute-start | bytes 1081352 | tf_op jit(solution)/shard_map/ppermute | solution.py:527
  32.2 1.4 %collective-permute-start.3 = (bf16[128,512]{1,0:T(8,128)(2,1)S(1)}, bf16[128,512]{1,0:T(8,128)(2,1)S(1)}, u32[]{:S(2)}, u32[]{:S(2)}) collective-permute-start(bf16[128,512]{1,0:T(8,128)(2,1)S(1)} %other_experts.1), channel_id=1, source_target_pairs={{0,2},{2,0},{4,6},{6,4},{8,10},{10,8},{12,14},{14,12},{16,18},{18,... | collective-permute-start | bytes 393224 | tf_op jit(solution)/shard_map/ppermute | solution.py:560
  34.3 11.9 %all-to-all-start.1 = ((bf16[16,8,512]{2,1,0:T(8,128)(2,1)}), bf16[16,8,512]{2,1,0:T(8,128)(2,1)S(1)}, u32[]{:S(2)}, u32[]{:S(2)}) async-start(bf16[16,8,512]{2,1,0:T(8,128)(2,1)} %bitcast.13), calls=%async_computation.1 | async-start | bytes 262144 | tf_op jit(solution)/shard_map/all_to_all | solution.py:562

commit v5 on v4

v5 whole, which is shorter than its diff:
```python
import functools

import jax
import jax.numpy as jnp
from jax import lax
from jax.experimental import pallas as pl
from jax.experimental.pallas import tpu as pltpu
from jax.sharding import PartitionSpec as P


epsilon = 1e-06
f32 = jnp.float32
bf16 = jnp.bfloat16
VMEM = pl.BlockSpec(memory_space=pltpu.VMEM)
SMEM = pl.BlockSpec(memory_space=pltpu.SMEM)
HBM = pl.BlockSpec(memory_space=pltpu.HBM)
MIB = 1 << 20
LANES = 128


def dot(left, right):
    return lax.dot_general(left, right, (((1,), (0,)), ((), ())), preferred_element_type=f32)


def dot_nt(left, right):
    return lax.dot_general(left, right, (((1,), (1,)), ((), ())), preferred_element_type=f32)


def silu(value):
    return value / (1.0 + jnp.exp(-value))


def sigmoid(value):
    return 1.0 / (1.0 + jnp.exp(-value))


def rms_rows(values, gain):
    return values * lax.rsqrt(jnp.mean(values * values, axis=-1, keepdims=True) + epsilon) * gain


def spread_heads(values, width):
    rows, heads = values.shape
    return jnp.concatenate(
        [jnp.broadcast_to(values[:, h : h + 1], (rows, width)) for h in range(heads)], axis=1
    )


def in_hbm(values):
    return pltpu.with_memory_space_constraint(values, pltpu.HBM)


def taps_first(values):
    return values.transpose(1, 0, 2)


def fold_of(rows, share):
    fold = 1
    while 4 * fold * share <= LANES and rows % (32 * fold) == 0:
        fold *= 2
    return fold


def packed_rows(rows, share, seqs):
    fold = fold_of(rows, share)
    return rows // fold + rows // (2 * fold) + seqs


def side_by_side(values, fold):
    rows, width = values.shape
    count, stride = rows // fold, LANES // fold
    pieces = []
    for k in range(fold):
        pieces.append(values[k * count : (k + 1) * count])
        if stride > width:
            pieces.append(jnp.zeros((count, stride - width), f32))
    return jnp.concatenate(pieces, axis=1)


def pack(gate, up, down, ids, weights, chip, fold):
    seqs, _ = ids.shape
    tail = []
    for expert in (2 * chip, 2 * chip + 1):
        weight = jnp.sum(jnp.where(ids == expert, weights, 0.0), axis=1, keepdims=True)
        high = weight.astype(bf16).astype(f32)
        tail += [high, weight - high]
    tail = jnp.concatenate((*tail, jnp.zeros((seqs, LANES - 4), f32)), axis=1)
    both = side_by_side(jnp.concatenate((gate, up), axis=1), fold)
    return jnp.concatenate((both, side_by_side(down, 2 * fold), tail), axis=0)


def mixer_kernel(*refs, n_tp, held):
    tp_ref = refs[0]
    sources = refs[1 : 1 + held]
    part_ref, packed_ref = refs[1 + held : 3 + held]
    results = refs[3 + held : 9 + held]
    targets = refs[9 + held : 9 + 2 * held]
    buffers = refs[9 + 2 * held : 15 + 2 * held]
    scaled_ref, key_ref, decay_ref, conv_x_next, conv_b_next, conv_c_next = buffers
    in_sems, state_sems, out_sems = refs[15 + 2 * held :]
    (
        tokens_ref,
        gain_ref,
        w_dt_ref,
        dt_bias_ref,
        a_log_ref,
        d_skip_ref,
        taps_x_ref,
        taps_b_ref,
        taps_c_ref,
        group_gain_ref,
        conv_x_ref,
        conv_b_ref,
        conv_c_ref,
        gate_ref,
        up_ref,
        down_ref,
        ids_ref,
        weights_ref,
        w_x,
        w_b,
        w_c,
        w_z,
        w_out,
        state,
    ) = targets
    seqs, heads, head_dim, state_dim = state.shape
    channels = heads * head_dim
    groups = w_b.shape[1] // state_dim
    per_group = heads // groups
    width = channels // groups
    copy = pltpu.make_async_copy
    loads = [copy(sources[i], targets[i], in_sems.at[i]) for i in range(held - 1)]
    *small_loads, load_x, load_b, load_c, load_z, load_out = loads
    state_loads = [copy(sources[-1].at[s], state.at[s], state_sems.at[s]) for s in range(seqs)]
    stores = [copy(buffers[i], results[i], out_sems.at[i]) for i in range(6)]
    for load in [*small_loads, load_x, load_b, load_c, *state_loads, load_z, load_out]:
        load.start()
    for load in small_loads:
        load.wait()

    normed = rms_rows(tokens_ref[...].astype(f32), gain_ref[...]).astype(bf16)
    dt_all = dot_nt(normed, w_dt_ref[...])
    own = tp_ref[0]
    dt_raw = jnp.zeros((seqs, heads), f32)
    for i in range(n_tp):
        dt_raw += jnp.where(own == i, dt_all[:, i * heads : (i + 1) * heads], 0.0)
    shifted = dt_raw + dt_bias_ref[...]
    step = jnp.maximum(shifted, 0.0) + jnp.log1p(jnp.exp(-jnp.abs(shifted)))
    decay = jnp.exp(-step * jnp.exp(a_log_ref[...]))

    gate = gate_ref[...].astype(f32)
    up = up_ref[...].astype(f32)
    down = down_ref[...].astype(f32)
    ids = ids_ref[...]
    weights = weights_ref[...]
    chips = packed_ref.shape[0]
    share = gate.shape[1] // chips
    fold = fold_of(gate.shape[0], share)
    for chip in range(chips):
        part = slice(chip * share, (chip + 1) * share)
        packed_ref[chip] = pack(
            gate[:, part], up[:, part], down[:, part], ids, weights, chip, fold
        ).astype(bf16)

    def short_conv(previous_ref, fresh, taps_ref, out_ref):
        taps = taps_ref[...].astype(f32)
        last = taps.shape[0] - 1
        total = fresh * taps[last:]
        for k in range(last):
            total += previous_ref[k].astype(f32) * taps[k : k + 1]
            out_ref[k] = previous_ref[k + 1] if k + 1 < last else fresh.astype(bf16)
        return silu(total)

    def projected(ref):
        return dot(normed, ref[...]).astype(bf16).astype(f32)

    load_x.wait()
    xs = short_conv(conv_x_ref, projected(w_x), taps_x_ref, conv_x_next)
    load_b.wait()
    bs = short_conv(conv_b_ref, projected(w_b), taps_b_ref, conv_b_next)
    load_c.wait()
    cs = short_conv(conv_c_ref, projected(w_c), taps_c_ref, conv_c_next)
    queries = cs.astype(bf16)
    scaled = spread_heads(step, head_dim) * xs
    scaled_ref[...] = scaled
    key_ref[...] = bs
    decay_ref[...] = decay
    for store in stores:
        store.start()
    row = lax.broadcasted_iota(jnp.int32, (seqs, width), 0)
    readout = [jnp.zeros((seqs, width), f32) for _ in range(groups)]
    for s in range(seqs):
        state_loads[s].wait()
        for g in range(groups):
            block = state[s, g * per_group : (g + 1) * per_group].reshape(width, state_dim)
            read = dot_nt(queries[:, g * state_dim : (g + 1) * state_dim], block.astype(bf16))
            readout[g] = jnp.where(row == s, read, readout[g])
    load_z.wait()
    z_gate = silu(projected(w_z))
    skip = spread_heads(d_skip_ref[...], head_dim) * xs
    kept = spread_heads(decay, head_dim)
    mixed = []
    for g in range(groups):
        part = slice(g * width, (g + 1) * width)
        own = slice(g * state_dim, (g + 1) * state_dim)
        match = jnp.sum(bs[:, own] * cs[:, own], axis=1, keepdims=True)
        read = kept[:, part] * readout[g] + scaled[:, part] * match
        gated = (read + skip[:, part]) * z_gate[:, part]
        mixed.append(rms_rows(gated, group_gain_ref[:, part]).astype(bf16))
    load_out.wait()
    part_ref[...] = dot(jnp.concatenate(mixed, axis=1), w_out[...]).astype(bf16)
    for store in stores:
        store.wait()


def advance_kernel(
    scaled_hbm,
    key_hbm,
    decay_hbm,
    state_hbm,
    state_out,
    scaled_ref,
    key_ref,
    decay_ref,
    state,
    small_sems,
    in_sems,
    out_sems,
):
    seqs, heads, head_dim, state_dim = state.shape
    per_group = heads * state_dim // key_ref.shape[1]
    copy = pltpu.make_async_copy
    small_loads = [
        copy(scaled_hbm, scaled_ref, small_sems.at[0]),
        copy(key_hbm, key_ref, small_sems.at[1]),
        copy(decay_hbm, decay_ref, small_sems.at[2]),
    ]
    loads = [copy(state_hbm.at[s], state.at[s], in_sems.at[s]) for s in range(seqs)]
    stores = [copy(state.at[s], state_out.at[s], out_sems.at[s]) for s in range(seqs)]
    for load in [*small_loads, *loads]:
        load.start()
    for load in small_loads:
        load.wait()
    scaled = scaled_ref[...].T
    keys = key_ref[...]
    decay = decay_ref[...]
    for s in range(seqs):
        loads[s].wait()
        for h in range(heads):
            g = h // per_group
            key = keys[s : s + 1, g * state_dim : (g + 1) * state_dim]
            column = scaled[h * head_dim : (h + 1) * head_dim, s : s + 1]
            state[s, h] = decay[s : s + 1, h : h + 1] * state[s, h] + column * key
        stores[s].start()
    for store in stores:
        store.wait()


def norm_kernel(tokens_ref, own_ref, other_ref, gain_ref, packed_ref, spread_ref, residual_ref):
    _, model = tokens_ref.shape
    summed = own_ref[...].astype(f32) + other_ref[...].astype(f32)
    residual = (tokens_ref[...].astype(f32) + summed).astype(bf16)
    residual_ref[...] = residual
    normed = rms_rows(residual.astype(f32), gain_ref[...])
    tiles = jnp.concatenate(
        [normed[:, k * LANES : (k + 1) * LANES] for k in range(model // LANES)], axis=0
    ).astype(bf16)
    count = tiles.shape[0]
    for chip in range(packed_ref.shape[0]):
        spread_ref[chip, :count] = tiles
        spread_ref[chip, count:] = packed_ref[chip]


def token_rows(tiles_ref, seqs, model):
    rows = []
    for chip in range(tiles_ref.shape[0]):
        tiles = tiles_ref[chip, : seqs * model // LANES]
        rows.append(
            jnp.concatenate(
                [tiles[k * seqs : (k + 1) * seqs] for k in range(model // LANES)], axis=1
            )
        )
    return jnp.concatenate(rows, axis=0)


def experts_kernel(core_ref, got_ref, branch_ref, *refs, seqs, model):
    result_ref, rows_ref, scale_ref = refs[-3:]
    chips, total, _ = got_ref.shape
    core = core_ref[0]
    rows = token_rows(got_ref, seqs, model)
    table = jnp.concatenate(
        [got_ref[i, total - seqs :].astype(f32) for i in range(chips)], axis=0
    )
    lane = lax.broadcasted_iota(jnp.int32, table.shape, 1)
    result = jnp.zeros((chips * seqs, model), f32)
    for index in range(2):
        gate_ref, up_ref, down_ref = refs[3 * index : 3 * index + 3]
        expert = core if index == 0 else 1 - core
        weight = jnp.sum(jnp.where(lane // 2 == expert, table, 0.0), axis=1, keepdims=True)
        active = (silu(dot(rows, gate_ref[0])) * dot(rows, up_ref[0])).astype(bf16)
        result += weight * dot(active, down_ref[0])
    result_ref[...] = result
    rows_ref[...] = rows
    branch = sigmoid(
        jnp.sum(rows.astype(f32) * branch_ref[...].astype(f32)[None], axis=1, keepdims=True)
    )
    scale_ref[...] = jnp.broadcast_to(branch, scale_ref.shape)


def dense_kernel(
    core_ref, got_ref, other_ref, routed_ref, rows_ref, scale_ref, out_ref, wide_ref, back_ref, *, share, seqs, n_tp
):
    model = wide_ref.shape[0]
    chips = got_ref.shape[0]
    rows = model // (2 * chips)
    start = seqs * model // LANES
    fold = fold_of(rows, share)
    core = core_ref[0]
    wide_rows, back_rows = rows // fold, rows // (2 * fold)

    def unfold(values, count, target_ref, source):
        height = values.shape[0]
        target_ref[pl.ds(pl.multiple_of(source, 8), height)] = values
        wider = values.astype(f32)
        for k in range(1, count):
            moved = pltpu.roll(wider, LANES - k * LANES // count, 1).astype(bf16)
            target_ref[pl.ds(pl.multiple_of(source + k * height, 8), height)] = moved

    for chip in range(chips):
        for ref, parity in ((got_ref, core), (other_ref, 1 - core)):
            source = (2 * chip + parity) * rows
            wide = ref[chip, start : start + wide_rows]
            back = ref[chip, start + wide_rows : start + wide_rows + back_rows]
            unfold(wide, fold, wide_ref, source)
            unfold(back, 2 * fold, back_ref, source)
    own = rows_ref[...]
    hidden = dot(own, wide_ref[...])
    lane = lax.broadcasted_iota(jnp.int32, hidden.shape, 1)
    dense = silu(hidden) * pltpu.roll(hidden, LANES - share, 1)
    dense = jnp.where(lane < share, dense, 0.0).astype(bf16)
    result = routed_ref[...] + scale_ref[:, :1] * dot_nt(dense, back_ref[...])
    half = model // n_tp
    for i in range(chips):
        for q in range(n_tp):
            place = (i * n_tp + q) * seqs
            value = result[i * seqs : (i + 1) * seqs, q * half : (q + 1) * half]
            out_ref[place : place + seqs] = value.astype(bf16)


def sum_kernel(tp_ref, parts_ref, residual_ref, out_ref, *, n_tp):
    seqs, half = out_ref.shape
    own = tp_ref[0]
    total = jnp.zeros((seqs, half), f32)
    for q in range(n_tp):
        total += jnp.where(
            own == q, residual_ref[:, q * half : (q + 1) * half].astype(f32), 0.0
        )
    for i in range(parts_ref.shape[0] // seqs):
        total += parts_ref[i * seqs : (i + 1) * seqs].astype(f32)
    out_ref[...] = total.astype(bf16)


def body(
    tokens,
    ssm_state,
    conv_x,
    conv_b,
    conv_c,
    w_x,
    w_z,
    w_b,
    w_c,
    w_dt,
    dt_bias,
    a_log,
    d_skip,
    taps_x,
    taps_b,
    taps_c,
    norm1_gain,
    group_gain,
    w_out,
    norm2_gain,
    route_ids,
    route_weights,
    exp_gate,
    exp_up,
    exp_down,
    dense_gate,
    dense_up,
    dense_down,
    branch_gate,
):
    seqs, model = tokens.shape
    n_ep = lax.axis_size("ep")
    n_tp = lax.axis_size("tp")
    tp_index = lax.axis_index("tp").astype(jnp.int32)[None]
    core_index = (lax.axis_index("ep") % 2).astype(jnp.int32)[None]
    sds = jax.ShapeDtypeStruct

    rows, hidden = dense_gate.shape
    chips = n_ep // 2
    share = hidden // chips
    block = packed_rows(rows, share, seqs)
    groups = [[2 * chip + core for chip in range(chips)] for core in range(2)]
    swap = [(i, i ^ 1) for i in range(n_ep)]
    held = (
        tokens,
        norm1_gain[None],
        w_dt.T,
        dt_bias[None],
        a_log[None],
        d_skip[None],
        taps_x,
        taps_b,
        taps_c,
        group_gain[None],
        taps_first(conv_x),
        taps_first(conv_b),
        taps_first(conv_c),
        dense_gate,
        dense_up,
        dense_down.T,
        route_ids,
        route_weights,
        w_x,
        w_b,
        w_c,
        w_z,
        w_out,
        ssm_state,
    )
    results = (
        sds((seqs, w_x.shape[1]), f32),
        sds((seqs, w_b.shape[1]), f32),
        sds((seqs, ssm_state.shape[1]), f32),
        *[sds(taps_first(value).shape, bf16) for value in (conv_x, conv_b, conv_c)],
    )
    part, packed, scaled, keys, decay, conv_x_next, conv_b_next, conv_c_next = pl.pallas_call(
        functools.partial(mixer_kernel, n_tp=n_tp, held=len(held)),
        out_shape=(
            sds((seqs, model), bf16),
            sds((chips, block, LANES), bf16),
            *[pltpu.HBM(value.shape, value.dtype) for value in results],
        ),
        in_specs=[SMEM] + [HBM] * len(held),
        out_specs=(VMEM,) * 2 + (HBM,) * 6,
        scratch_shapes=[pltpu.VMEM(value.shape, value.dtype) for value in held]
        + [pltpu.VMEM(value.shape, value.dtype) for value in results]
        + [
            pltpu.SemaphoreType.DMA((len(held) - 1,)),
            pltpu.SemaphoreType.DMA((seqs,)),
            pltpu.SemaphoreType.DMA((len(results),)),
        ],
        compiler_params=pltpu.CompilerParams(vmem_limit_bytes=20 * MIB),
        name="mixer",
    )(tp_index, *map(in_hbm, held))

    state_next = pl.pallas_call(
        advance_kernel,
        out_shape=sds(ssm_state.shape, f32),
        in_specs=[HBM] * 4,
        out_specs=HBM,
        scratch_shapes=[
            *[pltpu.VMEM(value.shape, f32) for value in (scaled, keys, decay, ssm_state)],
            pltpu.SemaphoreType.DMA((3,)),
            pltpu.SemaphoreType.DMA((seqs,)),
            pltpu.SemaphoreType.DMA((seqs,)),
        ],
        compiler_params=pltpu.CompilerParams(vmem_limit_bytes=12 * MIB),
        name="advance",
    )(*map(in_hbm, (scaled, keys, decay, ssm_state)))

    if n_tp == 2:
        other = lax.ppermute(part, "tp", [(0, 1), (1, 0)])
    else:
        gathered = lax.all_gather(part, "tp", axis=0).astype(f32)
        total = gathered[0]
        for i in range(1, n_tp):
            total = total + gathered[i]
        other = total - part.astype(f32)

    tile_rows = seqs * model // LANES
    spread, residual = pl.pallas_call(
        norm_kernel,
        out_shape=(sds((chips, tile_rows + block, LANES), bf16), sds((seqs, model), bf16)),
        in_specs=[VMEM] * 5,
        out_specs=(VMEM, VMEM),
        compiler_params=pltpu.CompilerParams(vmem_limit_bytes=4 * MIB),
        name="norm",
    )(tokens, part, other, norm2_gain[None], packed)
    got = lax.all_to_all(
        spread, "ep", split_axis=0, concat_axis=0, tiled=True, axis_index_groups=groups
    )
    own_experts = (exp_gate, exp_up, exp_down)
    other_experts = [lax.ppermute(value, "ep", swap) for value in own_experts]
    got_other = lax.ppermute(got, "ep", swap)

    routed, own_rows, scale = pl.pallas_call(
        functools.partial(experts_kernel, seqs=seqs, model=model),
        out_shape=(
            sds((chips * seqs, model), f32),
            sds((chips * seqs, model), bf16),
            sds((chips * seqs, LANES), f32),
        ),
        in_specs=[SMEM] + [VMEM] * 8,
        out_specs=(VMEM,) * 3,
        compiler_params=pltpu.CompilerParams(vmem_limit_bytes=12 * MIB),
        name="experts",
    )(core_index, got, branch_gate, *own_experts, *other_experts)
    outgoing = pl.pallas_call(
        functools.partial(dense_kernel, share=share, seqs=seqs, n_tp=n_tp),
        out_shape=sds((chips * n_tp * seqs, model // n_tp), bf16),
        in_specs=[SMEM] + [VMEM] * 5,
        out_specs=VMEM,
        scratch_shapes=[pltpu.VMEM((model, LANES), bf16), pltpu.VMEM((model, LANES), bf16)],
        compiler_params=pltpu.CompilerParams(vmem_limit_bytes=8 * MIB),
        name="dense",
    )(core_index, got, got_other, routed, own_rows, scale)
    flat_groups = [[ep * n_tp + q for ep in group for q in range(n_tp)] for group in groups]
    parts = lax.all_to_all(
        outgoing,
        ("ep", "tp"),
        split_axis=0,
        concat_axis=0,
        tiled=True,
        axis_index_groups=flat_groups,
    )

    mixed = pl.pallas_call(
        functools.partial(sum_kernel, n_tp=n_tp),
        out_shape=sds((seqs, model // n_tp), bf16),
        in_specs=[SMEM, VMEM, VMEM],
        out_specs=VMEM,
        compiler_params=pltpu.CompilerParams(vmem_limit_bytes=4 * MIB),
        name="total",
    )(tp_index, parts, residual)
    return (
        mixed,
        state_next,
        taps_first(conv_x_next),
        taps_first(conv_b_next),
        taps_first(conv_c_next),
    )


def solution(mesh):
    return jax.shard_map(
        body,
        mesh=mesh,
        in_specs=(
            P("ep", None),
            P("ep", "tp", None, None),
            P("ep", None, "tp"),
            P("ep", None, "tp"),
            P("ep", None, "tp"),
            P(None, "tp"),
            P(None, "tp"),
            P(None, "tp"),
            P(None, "tp"),
            P(),
            P("tp"),
            P("tp"),
            P("tp"),
            P(None, "tp"),
            P(None, "tp"),
            P(None, "tp"),
            P(),
            P("tp"),
            P("tp", None),
            P(),
            P("ep", None),
            P("ep", None),
            P("ep", None, "tp"),
            P("ep", None, "tp"),
            P("ep", "tp", None),
            P("ep", "tp"),
            P("ep", "tp"),
            P("tp", "ep"),
            P(),
        ),
        out_specs=(
            P("ep", "tp"),
            P("ep", "tp", None, None),
            P("ep", None, "tp"),
            P("ep", None, "tp"),
            P("ep", None, "tp"),
        ),
        check_vma=False,
    )
```

time: 47.6 us -> 45.8 us (0.962)
  blocking collectives: 17.1 us -> 0 us
  waiting for transfers between devices: 6.87 us -> 14.1 us
  starting transfers between devices: 7.5 us -> 14.7 us
  Pallas kernels: 15 us -> 15.8 us
    all_to_all x1 -> x0, blocking collectives: 17.1 us -> none  [body(): lax.all_to_all(spread, 'ep', split_axis=0, concat_axis=0, tiled=True, axi...]
    all_to_all x0 -> x1, waiting for transfers between devices: none -> 8.8 us  [body(): lax.all_to_all(spread, 'ep', split_axis=0, concat_axis=0, tiled=True, axi...]
    all_to_all x0 -> x1, starting transfers between devices: none -> 6.36 us  [body(): lax.all_to_all(spread, 'ep', split_axis=0, concat_axis=0, tiled=True, axi...]
    ppermute x2 -> x3, waiting for transfers between devices: 1.15 us -> 0.01 us  [body(): other_experts = [lax.ppermute(value, 'ep', swap) for value in own_experts]]
    pallas_call x1, Pallas kernels: 4.1 us -> 5.12 us  [body(): pl.pallas_call(advance_kernel, out_shape=sds(ssm_state.shape, f32), in_sp...]
    all_to_all x1, waiting for transfers between devices: 3.69 us -> 2.68 us  [body(): lax.all_to_all(outgoing, ('ep', 'tp'), split_axis=0, concat_axis=0, tiled...]
    pallas_call x4 -> x3, Pallas kernels: 2.88 us -> 3.74 us  [the longest x1 2.06 us: body(): pl.pallas_call(functools.partial(dense_kernel, share=share, seqs=seqs, n_...]
    ppermute x1, waiting for transfers between devices: 0.31 us -> 0.9 us  [body(): got_other = lax.ppermute(got, 'ep', swap)]
  transfers between devices with their start and end apart: 5 -> 7, of which waited for: 4 -> 4; matrix products, arithmetic and copies ran while one was open for 0% -> 0% of each run, Pallas kernels for 11% -> 13%
where the time goes in v5:
time: 45.8 us; the launch traced here: 45.4 us
  Pallas kernels  15.8 us (34%)
  starting transfers between devices  14.7 us (32%)
  waiting for transfers between devices  14.1 us (31%)
  between operations  0.77 us (2%)
    all_to_all x1, waiting for transfers between devices, body(): lax.all_to_all(spread, 'ep', split_axis=0, concat_axis=0, tiled=True, axi...  8.8 us
    all_to_all x1, starting transfers between devices, body(): lax.all_to_all(spread, 'ep', split_axis=0, concat_axis=0, tiled=True, axi...  6.36 us
    pallas_call x1, Pallas kernels, body(): pl.pallas_call(functools.partial(mixer_kernel, n_tp=n_tp, held=len(held))...  6.32 us
    pallas_call x1, Pallas kernels, body(): pl.pallas_call(advance_kernel, out_shape=sds(ssm_state.shape, f32), in_sp...  5.12 us
    all_to_all x1, starting transfers between devices, body(): lax.all_to_all(outgoing, ('ep', 'tp'), split_axis=0, concat_axis=0, tiled...  4.67 us
    ppermute x1, starting transfers between devices, body(): other = lax.ppermute(part, 'tp', [(0, 1), (1, 0)])  3.03 us
    all_to_all x1, waiting for transfers between devices, body(): lax.all_to_all(outgoing, ('ep', 'tp'), split_axis=0, concat_axis=0, tiled...  2.68 us
    pallas_call x1, Pallas kernels, body(): pl.pallas_call(functools.partial(dense_kernel, share=share, seqs=seqs, n_...  2.06 us
  transfers between devices with their start and end apart: 7, of which 4 were waited for; matrix products, arithmetic and copies ran while one was open for 0% of the time, Pallas kernels for 13%

profile of v5, /device:TPU:0, one launch (start us, length us, event | category | flops | bytes accessed | tf_op | source)
XLA Modules:
  0.0 45.4 jit_solution(2769806571321270064)
XLA Ops:
  0.6 0.0 copy-start.3
  0.7 0.0 copy-start.4
  0.7 0.0 copy-start
  0.7 0.0 copy-start.1
  0.7 0.0 copy-start.2
  0.7 0.0 copy-start.5
  0.7 6.3 %mixer.1 = (bf16[8,1024]{1,0:T(8,128)(2,1)S(1)}, bf16[8,104,128]{2,1,0:T(8,128)(2,1)S(1)}, f32[8,1024]{1,0:T(8,128)}, f32[8,512]{1,0:T(8,128)}, f32[8,16]{1,0:T(...) custom-call(s32[1]{0:T(128)} %bitcast.refs_0_.tp_ref, ...), custom_call_target="tpu_custom_call" | custom-call | tf_op jit(solution)/shard_map/mixer/pallas_call | solution.py:439
  7.0 3.0 %collective-permute-start = (bf16[8,1024]{1,0:T(8,128)(2,1)S(1)}, bf16[8,1024]{1,0:T(8,128)(2,1)S(1)}, u32[]{:S(2)}, u32[]{:S(2)}) collective-permute-start(bf16[8,1024]{1,0:T(8,128)(2,1)S(1)} %get-tuple-element.18.own_ref), channel_id=1, source_target_pairs={{0,1},{1,0},{2,3},{3,2},{4,5},{5,4},{6,7},{7,6},{8,9},{9,8},{10,11... | collective-permute-start | bytes 49160 | tf_op jit(solution)/shard_map/ppermute | solution.py:475
  10.1 1.7 %collective-permute-done.other_ref = bf16[8,1024]{1,0:T(8,128)(2,1)S(1)} collective-permute-done((bf16[8,1024]{1,0:T(8,128)(2,1)S(1)}, bf16[8,1024]{1,0:T(8,128)(2,1)S(1)}, u32[]{:S(2)}, u32[]{:S(2)}) %collective-permute-start) | collective-permute-done | bytes 16416 | tf_op jit(solution)/shard_map/ppermute | solution.py:475
  11.8 0.0 copy-done.3
  11.8 0.0 copy-done.4
  11.8 0.8 %norm.1 = (bf16[8,168,128]{2,1,0:T(8,128)(2,1)}, bf16[8,1024]{1,0:T(8,128)(2,1)S(1)}) custom-call(bf16[8,1024]{1,0:T(8,128)(2,1)S(1)} %copy-done.3, bf16[8,1024]{1,0:T(8,128)(2,1)S(1)} %get-tuple-element.18.own_ref, bf16[8,1024]{1,0:T(8,128)(2,1)S(1)} %collective-permute-done.other_ref, f32[1,1024]{1,0:T(1,128)S(1)} %bitcast.19, ...), custom_call_target="tpu_custom_call" | custom-call | tf_op jit(solution)/shard_map/norm/pallas_call | solution.py:484
  12.6 6.4 %all-to-all-start = ((bf16[8,168,128]{2,1,0:T(8,128)(2,1)}), bf16[8,168,128]{2,1,0:T(8,128)(2,1)S(1)}, u32[]{:S(2)}, u32[]{:S(2)}) async-start(bf16[8,168,128]{2,1,0:T(8,128)(2,1)} %get-tuple-element.20), calls=%async_computation | async-start | bytes 688128 | tf_op jit(solution)/shard_map/all_to_all | solution.py:492
  19.0 0.0 copy-done
  19.0 0.1 collective-permute-start.2
  19.1 0.0 copy-done.1
  19.1 0.5 %collective-permute-start.3 = (bf16[1,1024,256]{2,1,0:T(8,128)(2,1)S(1)}, bf16[1,1024,256]{2,1,0:T(8,128)(2,1)S(1)}, u32[]{:S(2)}, u32[]{:S(2)}) collective-permute-start(bf16[1,1024,256]{2,1,0:T(8,128)(2,1)S(1)} %copy-done.1), channel_id=1, source_target_pairs={{0,2},{2,0},{4,6},{6,4},{8,10},{10,8},{12,14},{14,12},{16,18},{18,... | collective-permute-start | bytes 1572872 | tf_op jit(solution)/shard_map/ppermute | solution.py:496
  19.6 0.0 copy-done.2
  19.6 0.1 collective-permute-start.4
  19.7 8.8 %all-to-all-done.got_ref = bf16[8,168,128]{2,1,0:T(8,128)(2,1)S(1)} async-done(((bf16[8,168,128]{2,1,0:T(8,128)(2,1)}), bf16[8,168,128]{2,1,0:T(8,128)(2,1)S(1)}, u32[]{:S(2)}, u32[]{:S(2)}) %all-to-all-start) | async-done | bytes 344096 | tf_op jit(solution)/shard_map/all_to_all | solution.py:492
  28.5 0.0 collective-permute-start.1
  28.5 0.0 collective-permute-done.2.refs_3_
  28.5 0.0 collective-permute-done.3.refs_4_
  28.5 0.0 collective-permute-done.4.refs_5_
  28.5 0.0 copy-done.5
  28.5 0.8 %experts.1 = (f32[64,1024]{1,0:T(8,128)S(1)}, bf16[64,1024]{1,0:T(8,128)(2,1)S(1)}, f32[64,128]{1,0:T(8,128)S(1)}) custom-call(s32[1]{0:T(128)} %bitcast.1.core_ref, bf16[8,168,128]{2,1,0:T(8,128)(2,1)S(1)} %all-to-all-done.got_ref, bf16[1024]{0:T(1024)(128)(2,1)S(1)} %copy-done.5, bf16[1,1024,256]{2,1,0:T(8,128)(2,1)S(1)} %copy-done, ...), custom_call_target="tpu_custom_call" | custom-call | tf_op jit(solution)/shard_map/experts/pallas_call | solution.py:499
  29.4 0.9 %collective-permute-done.1.other_ref = bf16[8,168,128]{2,1,0:T(8,128)(2,1)} collective-permute-done((bf16[8,168,128]{2,1,0:T(8,128)(2,1)S(1)}, bf16[8,168,128]{2,1,0:T(8,128)(2,1)}, u32[]{:S(2)}, u32[]{:S(2)}) %collective-permute-start.1) | collective-permute-done | bytes 344096 | tf_op jit(solution)/shard_map/ppermute | solution.py:497
  30.3 2.1 %dense.1 = bf16[128,512]{1,0:T(8,128)(2,1)} custom-call(s32[1]{0:T(128)} %bitcast.1.core_ref, bf16[8,168,128]{2,1,0:T(8,128)(2,1)S(1)} %all-to-all-done.got_ref, bf16[8,168,128]{2,1,0:T(8,128)(2,1)} %collective-permute-done.1.other_ref, f32[64,1024]{1,0:T(8,128)S(1)} %get-tuple-element.21.routed_ref, bf16[64,1024]{1,0:T(8,128)(2,1)S(1)} %get-tuple-element.22.rows_ref, ...), custom_call_target="tpu_custom_call" | custom-call | tf_op jit(solution)/shard_map/dense/pallas_call | solution.py:511
  32.3 4.7 %all-to-all-start.1 = ((bf16[16,8,512]{2,1,0:T(8,128)(2,1)}), bf16[16,8,512]{2,1,0:T(8,128)(2,1)S(1)}, u32[]{:S(2)}, u32[]{:S(2)}) async-start(bf16[16,8,512]{2,1,0:T(8,128)(2,1)} %bitcast.13), calls=%async_computation.1 | async-start | bytes 262144 | tf_op jit(solution)/shard_map/all_to_all | solution.py:521
  37.0 5.1 %advance.1 = f32[8,16,64,128]{3,2,1,0:T(8,128)} custom-call(f32[8,1024]{1,0:T(8,128)} %get-tuple-element.25.scaled_hbm, f32[8,512]{1,0:T(8,128)} %get-tuple-element.26.key_hbm, f32[8,16]{1,0:T(8,128)} %get-tuple-element.27.decay_hbm, f32[8,16,64,128]{3,2,1,0:T(8,128)} %state_hbm.1), custom_call_target="tpu_custom_call" | custom-call | tf_op jit(solution)/shard_map/advance/pallas_call | solution.py:459
  42.1 2.7 %all-to-all-done.1 = bf16[16,8,512]{2,1,0:T(8,128)(2,1)S(1)} async-done(((bf16[16,8,512]{2,1,0:T(8,128)(2,1)}), bf16[16,8,512]{2,1,0:T(8,128)(2,1)S(1)}, u32[]{:S(2)}, u32[]{:S(2)}) %all-to-all-start.1) | async-done | bytes 131104 | tf_op jit(solution)/shard_map/all_to_all | solution.py:521
  44.8 0.6 %total.1 = bf16[8,512]{1,0:T(8,128)(2,1)} custom-call(s32[1]{0:T(128)} %bitcast.refs_0_.tp_ref, bf16[128,512]{1,0:T(8,128)(2,1)S(1)} %bitcast.18, bf16[8,1024]{1,0:T(8,128)(2,1)S(1)} %get-tuple-element.24.residual_ref), custom_call_target="tpu_custom_call" | custom-call | tf_op jit(solution)/shard_map/total/pallas_call | solution.py:530
Async XLA Ops:
  0.6 11.1 %copy-start.3 = (bf16[8,1024]{1,0:T(8,128)(2,1)S(1)}, bf16[8,1024]{1,0:T(8,128)(2,1)}, u32[]{:S(2)}) copy-start(bf16[8,1024]{1,0:T(8,128)(2,1)} %tokens_ref.1) | copy-start | bytes 49156
  0.7 11.1 %copy-start.4 = (f32[1024]{0:T(1024)S(1)}, f32[1024]{0:T(1024)}, u32[]{:S(2)}) copy-start(f32[1024]{0:T(1024)} %param.48) | copy-start | bytes 12292
  0.7 18.3 %copy-start = (bf16[1,1024,256]{2,1,0:T(8,128)(2,1)S(1)}, bf16[1,1024,256]{2,1,0:T(8,128)(2,1)}, u32[]{:S(2)}) copy-start(bf16[1,1024,256]{2,1,0:T(8,128)(2,1)} %refs_0_.1) | copy-start | bytes 1572868
  0.7 18.4 %copy-start.1 = (bf16[1,1024,256]{2,1,0:T(8,128)(2,1)S(1)}, bf16[1,1024,256]{2,1,0:T(8,128)(2,1)}, u32[]{:S(2)}) copy-start(bf16[1,1024,256]{2,1,0:T(8,128)(2,1)} %refs_1_.3) | copy-start | bytes 1572868
  0.7 18.9 %copy-start.2 = (bf16[1,256,1024]{2,1,0:T(8,128)(2,1)S(1)}, bf16[1,256,1024]{2,1,0:T(8,128)(2,1)}, u32[]{:S(2)}) copy-start(bf16[1,256,1024]{2,1,0:T(8,128)(2,1)} %refs_2_.1) | copy-start | bytes 1572868
  0.7 27.8 %copy-start.5 = (bf16[1024]{0:T(1024)(128)(2,1)S(1)}, bf16[1024]{0:T(1024)(128)(2,1)}, u32[]{:S(2)}) copy-start(bf16[1024]{0:T(1024)(128)(2,1)} %branch_ref.1) | copy-start | bytes 6148
  7.0 4.8 %collective-permute-start = (bf16[8,1024]{1,0:T(8,128)(2,1)S(1)}, bf16[8,1024]{1,0:T(8,128)(2,1)S(1)}, u32[]{:S(2)}, u32[]{:S(2)}) collective-permute-start(bf16[8,1024]{1,0:T(8,128)(2,1)S(1)} %get-tuple-element.18.own_ref), channel_id=1, source_target_pairs={{0,1},{1,0},{2,3},{3,2},{4,5},{5,4},{6,7},{7,6},{8,9},{9,8},{10,11... | collective-permute-start | bytes 49160 | tf_op jit(solution)/shard_map/ppermute | solution.py:475
  12.6 15.8 %all-to-all-start = ((bf16[8,168,128]{2,1,0:T(8,128)(2,1)}), bf16[8,168,128]{2,1,0:T(8,128)(2,1)S(1)}, u32[]{:S(2)}, u32[]{:S(2)}) async-start(bf16[8,168,128]{2,1,0:T(8,128)(2,1)} %get-tuple-element.20), calls=%async_computation | async-start | bytes 688128 | tf_op jit(solution)/shard_map/all_to_all | solution.py:492
  19.0 9.5 %collective-permute-start.2 = (bf16[1,1024,256]{2,1,0:T(8,128)(2,1)S(1)}, bf16[1,1024,256]{2,1,0:T(8,128)(2,1)S(1)}, u32[]{:S(2)}, u32[]{:S(2)}) collective-permute-start(bf16[1,1024,256]{2,1,0:T(8,128)(2,1)S(1)} %copy-done), channel_id=1, source_target_pairs={{0,2},{2,0},{4,6},{6,4},{8,10},{10,8},{12,14},{14,12},{16,18},{18,... | collective-permute-start | bytes 1572872 | tf_op jit(solution)/shard_map/ppermute | solution.py:496
  19.1 9.4 %collective-permute-start.3 = (bf16[1,1024,256]{2,1,0:T(8,128)(2,1)S(1)}, bf16[1,1024,256]{2,1,0:T(8,128)(2,1)S(1)}, u32[]{:S(2)}, u32[]{:S(2)}) collective-permute-start(bf16[1,1024,256]{2,1,0:T(8,128)(2,1)S(1)} %copy-done.1), channel_id=1, source_target_pairs={{0,2},{2,0},{4,6},{6,4},{8,10},{10,8},{12,14},{14,12},{16,18},{18,... | collective-permute-start | bytes 1572872 | tf_op jit(solution)/shard_map/ppermute | solution.py:496
  19.6 8.9 %collective-permute-start.4 = (bf16[1,256,1024]{2,1,0:T(8,128)(2,1)S(1)}, bf16[1,256,1024]{2,1,0:T(8,128)(2,1)S(1)}, u32[]{:S(2)}, u32[]{:S(2)}) collective-permute-start(bf16[1,256,1024]{2,1,0:T(8,128)(2,1)S(1)} %copy-done.2), channel_id=1, source_target_pairs={{0,2},{2,0},{4,6},{6,4},{8,10},{10,8},{12,14},{14,12},{16,18},{18,... | collective-permute-start | bytes 1572872 | tf_op jit(solution)/shard_map/ppermute | solution.py:496
  28.5 1.8 %collective-permute-start.1 = (bf16[8,168,128]{2,1,0:T(8,128)(2,1)S(1)}, bf16[8,168,128]{2,1,0:T(8,128)(2,1)}, u32[]{:S(2)}, u32[]{:S(2)}) collective-permute-start(bf16[8,168,128]{2,1,0:T(8,128)(2,1)S(1)} %all-to-all-done.got_ref), channel_id=1, source_target_pairs={{0,2},{2,0},{4,6},{6,4},{8,10},{10,8},{12,14},{14,12},{16,18},{18,... | collective-permute-start | bytes 1032200 | tf_op jit(solution)/shard_map/ppermute | solution.py:497
  32.3 12.5 %all-to-all-start.1 = ((bf16[16,8,512]{2,1,0:T(8,128)(2,1)}), bf16[16,8,512]{2,1,0:T(8,128)(2,1)S(1)}, u32[]{:S(2)}, u32[]{:S(2)}) async-start(bf16[16,8,512]{2,1,0:T(8,128)(2,1)} %bitcast.13), calls=%async_computation.1 | async-start | bytes 262144 | tf_op jit(solution)/shard_map/all_to_all | solution.py:521

commit v6 on v5

--- a/solution.py
+++ b/solution.py
@@ -60,9 +60,15 @@
     return fold
 
 
+def back_fold_of(rows, share):
+    fold = 1
+    while 2 * fold * rows <= LANES and share % (16 * fold) == 0:
+        fold *= 2
+    return fold
+
+
 def packed_rows(rows, share, seqs):
-    fold = fold_of(rows, share)
-    return rows // fold + rows // (2 * fold) + seqs
+    return rows // fold_of(rows, share) + share // back_fold_of(rows, share) + seqs
 
 
 def side_by_side(values, fold):
@@ -76,7 +82,7 @@
     return jnp.concatenate(pieces, axis=1)
 
 
-def pack(gate, up, down, ids, weights, chip, fold):
+def pack(gate, up, down, ids, weights, chip):
     seqs, _ = ids.shape
     tail = []
     for expert in (2 * chip, 2 * chip + 1):
@@ -84,8 +90,10 @@
         high = weight.astype(bf16).astype(f32)
         tail += [high, weight - high]
     tail = jnp.concatenate((*tail, jnp.zeros((seqs, LANES - 4), f32)), axis=1)
-    both = side_by_side(jnp.concatenate((gate, up), axis=1), fold)
-    return jnp.concatenate((both, side_by_side(down, 2 * fold), tail), axis=0)
+    rows, share = gate.shape
+    both = side_by_side(jnp.concatenate((gate, up), axis=1), fold_of(rows, share))
+    back = side_by_side(down, back_fold_of(rows, share))
+    return jnp.concatenate((both, back, tail), axis=0)
 
 
 def mixer_kernel(*refs, n_tp, held):
@@ -131,7 +139,15 @@
     copy = pltpu.make_async_copy
     loads = [copy(sources[i], targets[i], in_sems.at[i]) for i in range(held - 1)]
     *small_loads, load_x, load_b, load_c, load_z, load_out = loads
-    state_loads = [copy(sources[-1].at[s], state.at[s], state_sems.at[s]) for s in range(seqs)]
+    batch = seqs // 2
+    state_loads = [
+        copy(
+            sources[-1].at[pl.ds(i * batch, batch)],
+            state.at[pl.ds(i * batch, batch)],
+            state_sems.at[i],
+        )
+        for i in range(2)
+    ]
     stores = [copy(buffers[i], results[i], out_sems.at[i]) for i in range(6)]
     for load in [*small_loads, load_x, load_b, load_c, *state_loads, load_z, load_out]:
         load.start()
@@ -150,16 +166,15 @@
 
     gate = gate_ref[...].astype(f32)
     up = up_ref[...].astype(f32)
-    down = down_ref[...].astype(f32)
+    down = down_ref[...].astype(f32).T
     ids = ids_ref[...]
     weights = weights_ref[...]
     chips = packed_ref.shape[0]
     share = gate.shape[1] // chips
-    fold = fold_of(gate.shape[0], share)
     for chip in range(chips):
         part = slice(chip * share, (chip + 1) * share)
         packed_ref[chip] = pack(
-            gate[:, part], up[:, part], down[:, part], ids, weights, chip, fold
+            gate[:, part], up[:, part], down[part], ids, weights, chip
         ).astype(bf16)
 
     def short_conv(previous_ref, fresh, taps_ref, out_ref):
@@ -190,7 +205,8 @@
     row = lax.broadcasted_iota(jnp.int32, (seqs, width), 0)
     readout = [jnp.zeros((seqs, width), f32) for _ in range(groups)]
     for s in range(seqs):
-        state_loads[s].wait()
+        if s % batch == 0:
+            state_loads[s // batch].wait()
         for g in range(groups):
             block = state[s, g * per_group : (g + 1) * per_group].reshape(width, state_dim)
             read = dot_nt(queries[:, g * state_dim : (g + 1) * state_dim], block.astype(bf16))
@@ -235,8 +251,10 @@
         copy(key_hbm, key_ref, small_sems.at[1]),
         copy(decay_hbm, decay_ref, small_sems.at[2]),
     ]
-    loads = [copy(state_hbm.at[s], state.at[s], in_sems.at[s]) for s in range(seqs)]
-    stores = [copy(state.at[s], state_out.at[s], out_sems.at[s]) for s in range(seqs)]
+    batch = max(1, seqs // 4)
+    spans = [pl.ds(first, batch) for first in range(0, seqs, batch)]
+    loads = [copy(state_hbm.at[p], state.at[p], in_sems.at[i]) for i, p in enumerate(spans)]
+    stores = [copy(state.at[p], state_out.at[p], out_sems.at[i]) for i, p in enumerate(spans)]
     for load in [*small_loads, *loads]:
         load.start()
     for load in small_loads:
@@ -245,13 +263,15 @@
     keys = key_ref[...]
     decay = decay_ref[...]
     for s in range(seqs):
-        loads[s].wait()
+        if s % batch == 0:
+            loads[s // batch].wait()
         for h in range(heads):
             g = h // per_group
             key = keys[s : s + 1, g * state_dim : (g + 1) * state_dim]
             column = scaled[h * head_dim : (h + 1) * head_dim, s : s + 1]
             state[s, h] = decay[s : s + 1, h : h + 1] * state[s, h] + column * key
-        stores[s].start()
+        if (s + 1) % batch == 0:
+            stores[s // batch].start()
     for store in stores:
         store.wait()
 
@@ -283,62 +303,99 @@
     return jnp.concatenate(rows, axis=0)
 
 
-def experts_kernel(core_ref, got_ref, branch_ref, *refs, seqs, model):
-    result_ref, rows_ref, scale_ref = refs[-3:]
+def unfold(packed_ref, parity, start, share, wide_ref):
+    chips = packed_ref.shape[0]
+    rows = wide_ref.shape[0] // (2 * chips)
+    fold = fold_of(rows, share)
+    height = rows // fold
+    wide_ref[...] = jnp.zeros(wide_ref.shape, bf16)
+    for chip in range(chips):
+        source = (2 * chip + parity) * rows
+        values = packed_ref[chip, start : start + height]
+        wide_ref[pl.ds(pl.multiple_of(source, 8), height)] = values
+        wider = values.astype(f32)
+        for k in range(1, fold):
+            moved = pltpu.roll(wider, LANES - k * LANES // fold, 1).astype(bf16)
+            wide_ref[pl.ds(pl.multiple_of(source + k * height, 8), height)] = moved
+
+
+def down_rows(own_ref, other_ref, first, start, share, rows):
+    fold = back_fold_of(rows, share)
+    height, stride = share // fold, LANES // fold
+    pieces = []
+    for chip in range(own_ref.shape[0]):
+        own, other = [
+            jnp.concatenate(
+                [values[:, k * stride : k * stride + rows] for k in range(fold)], axis=0
+            )
+            for values in (
+                own_ref[chip, start : start + height].astype(f32),
+                other_ref[chip, start : start + height].astype(f32),
+            )
+        ]
+        pieces += [jnp.where(first, own, other), jnp.where(first, other, own)]
+    return jnp.concatenate(pieces, axis=1).astype(bf16)
+
+
+def experts_kernel(core_ref, got_ref, branch_ref, *refs, share, seqs, model):
+    gate, up, other_gate, other_up, other_down, down_hbm = refs[:6]
+    result_ref, rows_ref, hidden_ref, scale_ref, wide_ref, down, sem = refs[6:]
+    load = pltpu.make_async_copy(down_hbm, down, sem.at[0])
+    load.start()
     chips, total, _ = got_ref.shape
     core = core_ref[0]
     rows = token_rows(got_ref, seqs, model)
+    rows_ref[...] = rows
     table = jnp.concatenate(
         [got_ref[i, total - seqs :].astype(f32) for i in range(chips)], axis=0
     )
     lane = lax.broadcasted_iota(jnp.int32, table.shape, 1)
-    result = jnp.zeros((chips * seqs, model), f32)
-    for index in range(2):
-        gate_ref, up_ref, down_ref = refs[3 * index : 3 * index + 3]
-        expert = core if index == 0 else 1 - core
-        weight = jnp.sum(jnp.where(lane // 2 == expert, table, 0.0), axis=1, keepdims=True)
-        active = (silu(dot(rows, gate_ref[0])) * dot(rows, up_ref[0])).astype(bf16)
-        result += weight * dot(active, down_ref[0])
-    result_ref[...] = result
-    rows_ref[...] = rows
+
+    def active(gate_ref, up_ref):
+        return (silu(dot(rows, gate_ref[0])) * dot(rows, up_ref[0])).astype(bf16)
+
+    def weight_of(expert):
+        return jnp.sum(jnp.where(lane // 2 == expert, table, 0.0), axis=1, keepdims=True)
+
+    own_active = active(gate, up)
+    other = weight_of(1 - core) * dot(active(other_gate, other_up), other_down[0])
     branch = sigmoid(
         jnp.sum(rows.astype(f32) * branch_ref[...].astype(f32)[None], axis=1, keepdims=True)
     )
     scale_ref[...] = jnp.broadcast_to(branch, scale_ref.shape)
+    unfold(got_ref, core, seqs * model // LANES, share, wide_ref)
+    hidden_ref[...] = dot(rows, wide_ref[...])
+    load.wait()
+    result_ref[...] = other + weight_of(core) * dot(own_active, down[0])
 
 
 def dense_kernel(
-    core_ref, got_ref, other_ref, routed_ref, rows_ref, scale_ref, out_ref, wide_ref, back_ref, *, share, seqs, n_tp
+    core_ref,
+    own_ref,
+    other_ref,
+    routed_ref,
+    rows_ref,
+    half_ref,
+    scale_ref,
+    out_ref,
+    wide_ref,
+    *,
+    share,
+    seqs,
+    n_tp,
 ):
     model = wide_ref.shape[0]
-    chips = got_ref.shape[0]
+    chips = other_ref.shape[0]
     rows = model // (2 * chips)
+    core = core_ref[0]
     start = seqs * model // LANES
-    fold = fold_of(rows, share)
-    core = core_ref[0]
-    wide_rows, back_rows = rows // fold, rows // (2 * fold)
-
-    def unfold(values, count, target_ref, source):
-        height = values.shape[0]
-        target_ref[pl.ds(pl.multiple_of(source, 8), height)] = values
-        wider = values.astype(f32)
-        for k in range(1, count):
-            moved = pltpu.roll(wider, LANES - k * LANES // count, 1).astype(bf16)
-            target_ref[pl.ds(pl.multiple_of(source + k * height, 8), height)] = moved
-
-    for chip in range(chips):
-        for ref, parity in ((got_ref, core), (other_ref, 1 - core)):
-            source = (2 * chip + parity) * rows
-            wide = ref[chip, start : start + wide_rows]
-            back = ref[chip, start + wide_rows : start + wide_rows + back_rows]
-            unfold(wide, fold, wide_ref, source)
-            unfold(back, 2 * fold, back_ref, source)
-    own = rows_ref[...]
-    hidden = dot(own, wide_ref[...])
-    lane = lax.broadcasted_iota(jnp.int32, hidden.shape, 1)
+    unfold(other_ref, 1 - core, start, share, wide_ref)
+    hidden = half_ref[...] + dot(rows_ref[...], wide_ref[...])
     dense = silu(hidden) * pltpu.roll(hidden, LANES - share, 1)
-    dense = jnp.where(lane < share, dense, 0.0).astype(bf16)
-    result = routed_ref[...] + scale_ref[:, :1] * dot_nt(dense, back_ref[...])
+    start += rows // fold_of(rows, share)
+    back = down_rows(own_ref, other_ref, core == 0, start, share, rows)
+    dense_out = dot(dense[:, :share].astype(bf16), back)
+    result = routed_ref[...] + scale_ref[:, :1] * dense_out
     half = model // n_tp
     for i in range(chips):
         for q in range(n_tp):
@@ -496,27 +553,33 @@
     other_experts = [lax.ppermute(value, "ep", swap) for value in own_experts]
     got_other = lax.ppermute(got, "ep", swap)
 
-    routed, own_rows, scale = pl.pallas_call(
-        functools.partial(experts_kernel, seqs=seqs, model=model),
+    dense_inputs = pl.pallas_call(
+        functools.partial(experts_kernel, share=share, seqs=seqs, model=model),
         out_shape=(
             sds((chips * seqs, model), f32),
             sds((chips * seqs, model), bf16),
             sds((chips * seqs, LANES), f32),
+            sds((chips * seqs, LANES), f32),
         ),
-        in_specs=[SMEM] + [VMEM] * 8,
-        out_specs=(VMEM,) * 3,
+        in_specs=[SMEM] + [VMEM] * 7 + [HBM],
+        out_specs=(VMEM,) * 4,
+        scratch_shapes=[
+            pltpu.VMEM((model, LANES), bf16),
+            pltpu.VMEM(exp_down.shape, bf16),
+            pltpu.SemaphoreType.DMA((1,)),
+        ],
         compiler_params=pltpu.CompilerParams(vmem_limit_bytes=12 * MIB),
         name="experts",
-    )(core_index, got, branch_gate, *own_experts, *other_experts)
+    )(core_index, got, branch_gate, exp_gate, exp_up, *other_experts, in_hbm(exp_down))
     outgoing = pl.pallas_call(
         functools.partial(dense_kernel, share=share, seqs=seqs, n_tp=n_tp),
         out_shape=sds((chips * n_tp * seqs, model // n_tp), bf16),
-        in_specs=[SMEM] + [VMEM] * 5,
+        in_specs=[SMEM] + [VMEM] * 6,
         out_specs=VMEM,
-        scratch_shapes=[pltpu.VMEM((model, LANES), bf16), pltpu.VMEM((model, LANES), bf16)],
+        scratch_shapes=[pltpu.VMEM((model, LANES), bf16)],
         compiler_params=pltpu.CompilerParams(vmem_limit_bytes=8 * MIB),
         name="dense",
-    )(core_index, got, got_other, routed, own_rows, scale)
+    )(core_index, got, got_other, *dense_inputs)
     flat_groups = [[ep * n_tp + q for ep in group for q in range(n_tp)] for group in groups]
     parts = lax.all_to_all(
         outgoing,

time: 45.8 us -> 44.7 us (0.976)
  Pallas kernels: 15.8 us -> 15.1 us
    pallas_call x1, Pallas kernels: 0.84 us -> 1.86 us  [body(): pl.pallas_call(functools.partial(experts_kernel, share=share, seqs=seqs,...]
    pallas_call x1, Pallas kernels: 2.06 us -> 1.11 us  [body(): pl.pallas_call(functools.partial(dense_kernel, share=share, seqs=seqs, n_...]
    ppermute x1, waiting for transfers between devices: 0.9 us -> 0.01 us  [body(): got_other = lax.ppermute(got, 'ep', swap)]
    all_to_all x1, waiting for transfers between devices: 2.68 us -> 3.28 us  [body(): lax.all_to_all(outgoing, ('ep', 'tp'), split_axis=0, concat_axis=0, tiled...]
    pallas_call x1, Pallas kernels: 6.32 us -> 5.81 us  [body(): pl.pallas_call(functools.partial(mixer_kernel, n_tp=n_tp, held=len(held))...]
  transfers between devices with their start and end apart: 7 -> 7, of which waited for: 4 -> 3; matrix products, arithmetic and copies ran while one was open for 0% -> 0% of each run, Pallas kernels for 13% -> 15%
where the time goes in v6:
time: 44.7 us; the launch traced here: 44.4 us
  Pallas kernels  15.1 us (34%)
  starting transfers between devices  14.7 us (33%)
  waiting for transfers between devices  13.8 us (31%)
  between operations  0.77 us (2%)
    all_to_all x1, waiting for transfers between devices, body(): lax.all_to_all(spread, 'ep', split_axis=0, concat_axis=0, tiled=True, axi...  8.8 us
    all_to_all x1, starting transfers between devices, body(): lax.all_to_all(spread, 'ep', split_axis=0, concat_axis=0, tiled=True, axi...  6.36 us
    pallas_call x1, Pallas kernels, body(): pl.pallas_call(functools.partial(mixer_kernel, n_tp=n_tp, held=len(held))...  5.81 us
    pallas_call x1, Pallas kernels, body(): pl.pallas_call(advance_kernel, out_shape=sds(ssm_state.shape, f32), in_sp...  4.82 us
    all_to_all x1, starting transfers between devices, body(): lax.all_to_all(outgoing, ('ep', 'tp'), split_axis=0, concat_axis=0, tiled...  4.67 us
    all_to_all x1, waiting for transfers between devices, body(): lax.all_to_all(outgoing, ('ep', 'tp'), split_axis=0, concat_axis=0, tiled...  3.28 us
    ppermute x1, starting transfers between devices, body(): other = lax.ppermute(part, 'tp', [(0, 1), (1, 0)])  3.03 us
    pallas_call x1, Pallas kernels, body(): pl.pallas_call(functools.partial(experts_kernel, share=share, seqs=seqs,...  1.86 us
  transfers between devices with their start and end apart: 7, of which 3 were waited for; matrix products, arithmetic and copies ran while one was open for 0% of the time, Pallas kernels for 15%

profile of v6, /device:TPU:0, one launch (start us, length us, event | category | flops | bytes accessed | tf_op | source)
XLA Modules:
  0.0 44.4 jit_solution(14239718113910052146)
XLA Ops:
  0.6 0.0 copy-start.2
  0.7 0.0 copy-start.3
  0.7 0.0 copy-start
  0.7 0.0 copy-start.1
  0.7 0.0 copy-start.4
  0.7 5.8 %mixer.1 = (bf16[8,1024]{1,0:T(8,128)(2,1)S(1)}, bf16[8,104,128]{2,1,0:T(8,128)(2,1)S(1)}, f32[8,1024]{1,0:T(8,128)}, f32[8,512]{1,0:T(8,128)}, f32[8,16]{1,0:T(...) custom-call(s32[1]{0:T(128)} %bitcast.refs_0_.tp_ref, ...), custom_call_target="tpu_custom_call" | custom-call | tf_op jit(solution)/shard_map/mixer/pallas_call | solution.py:496
  6.5 3.0 %collective-permute-start = (bf16[8,1024]{1,0:T(8,128)(2,1)S(1)}, bf16[8,1024]{1,0:T(8,128)(2,1)S(1)}, u32[]{:S(2)}, u32[]{:S(2)}) collective-permute-start(bf16[8,1024]{1,0:T(8,128)(2,1)S(1)} %get-tuple-element.19.own_ref), channel_id=1, source_target_pairs={{0,1},{1,0},{2,3},{3,2},{4,5},{5,4},{6,7},{7,6},{8,9},{9,8},{10,11... | collective-permute-start | bytes 49160 | tf_op jit(solution)/shard_map/ppermute | solution.py:532
  9.5 1.7 %collective-permute-done.other_ref = bf16[8,1024]{1,0:T(8,128)(2,1)S(1)} collective-permute-done((bf16[8,1024]{1,0:T(8,128)(2,1)S(1)}, bf16[8,1024]{1,0:T(8,128)(2,1)S(1)}, u32[]{:S(2)}, u32[]{:S(2)}) %collective-permute-start) | collective-permute-done | bytes 16416 | tf_op jit(solution)/shard_map/ppermute | solution.py:532
  11.3 0.0 copy-done.2
  11.3 0.0 copy-done.3
  11.3 0.8 %norm.1 = (bf16[8,168,128]{2,1,0:T(8,128)(2,1)}, bf16[8,1024]{1,0:T(8,128)(2,1)S(1)}) custom-call(bf16[8,1024]{1,0:T(8,128)(2,1)S(1)} %copy-done.2, bf16[8,1024]{1,0:T(8,128)(2,1)S(1)} %get-tuple-element.19.own_ref, bf16[8,1024]{1,0:T(8,128)(2,1)S(1)} %collective-permute-done.other_ref, f32[1,1024]{1,0:T(1,128)S(1)} %bitcast.19, ...), custom_call_target="tpu_custom_call" | custom-call | tf_op jit(solution)/shard_map/norm/pallas_call | solution.py:541
  12.1 6.4 %all-to-all-start = ((bf16[8,168,128]{2,1,0:T(8,128)(2,1)}), bf16[8,168,128]{2,1,0:T(8,128)(2,1)S(1)}, u32[]{:S(2)}, u32[]{:S(2)}) async-start(bf16[8,168,128]{2,1,0:T(8,128)(2,1)} %get-tuple-element.21), calls=%async_computation | async-start | bytes 688128 | tf_op jit(solution)/shard_map/all_to_all | solution.py:549
  18.5 0.0 copy-done
  18.5 0.1 collective-permute-start.2
  18.6 0.0 copy-done.1
  18.6 0.5 %collective-permute-start.3 = (bf16[1,1024,256]{2,1,0:T(8,128)(2,1)S(1)}, bf16[1,1024,256]{2,1,0:T(8,128)(2,1)S(1)}, u32[]{:S(2)}, u32[]{:S(2)}) collective-permute-start(bf16[1,1024,256]{2,1,0:T(8,128)(2,1)S(1)} %copy-done.1), channel_id=1, source_target_pairs={{0,2},{2,0},{4,6},{6,4},{8,10},{10,8},{12,14},{14,12},{16,18},{18,... | collective-permute-start | bytes 1572872 | tf_op jit(solution)/shard_map/ppermute | solution.py:553
  19.1 0.1 collective-permute-start.4
  19.1 8.8 %all-to-all-done.got_ref.own_ref = bf16[8,168,128]{2,1,0:T(8,128)(2,1)S(1)} async-done(((bf16[8,168,128]{2,1,0:T(8,128)(2,1)}), bf16[8,168,128]{2,1,0:T(8,128)(2,1)S(1)}, u32[]{:S(2)}, u32[]{:S(2)}) %all-to-all-start) | async-done | bytes 344096 | tf_op jit(solution)/shard_map/all_to_all | solution.py:549
  28.0 0.0 collective-permute-start.1
  28.0 0.0 collective-permute-done.2.refs_2_
  28.0 0.0 collective-permute-done.3.refs_3_
  28.0 0.0 collective-permute-done.4.refs_4_
  28.0 0.0 copy-done.4
  28.0 1.9 %experts.1 = (f32[64,1024]{1,0:T(8,128)S(1)}, bf16[64,1024]{1,0:T(8,128)(2,1)S(1)}, f32[64,128]{1,0:T(8,128)S(1)}, f32[64,128]{1,0:T(8,128)S(1)}) custom-call(s32[1]{0:T(128)} %bitcast.1.core_ref, bf16[8,168,128]{2,1,0:T(8,128)(2,1)S(1)} %all-to-all-done.got_ref.own_ref, bf16[1024]{0:T(1024)(128)(2,1)S(1)} %copy-done.4, bf16[1,1024,256]{2,1,0:T(8,128)(2,1)S(1)} %copy-done, ...), custom_call_target="tpu_custom_call" | custom-call | tf_op jit(solution)/shard_map/experts/pallas_call | solution.py:556
  29.9 0.0 collective-permute-done.1.other_ref
  29.9 1.1 %dense.1 = bf16[128,512]{1,0:T(8,128)(2,1)} custom-call(s32[1]{0:T(128)} %bitcast.1.core_ref, bf16[8,168,128]{2,1,0:T(8,128)(2,1)S(1)} %all-to-all-done.got_ref.own_ref, bf16[8,168,128]{2,1,0:T(8,128)(2,1)S(1)} %collective-permute-done.1.other_ref, f32[64,1024]{1,0:T(8,128)S(1)} %get-tuple-element.22.routed_ref, ...), custom_call_target="tpu_custom_call" | custom-call | tf_op jit(solution)/shard_map/dense/pallas_call | solution.py:574
  31.0 4.7 %all-to-all-start.1 = ((bf16[16,8,512]{2,1,0:T(8,128)(2,1)}), bf16[16,8,512]{2,1,0:T(8,128)(2,1)S(1)}, u32[]{:S(2)}, u32[]{:S(2)}) async-start(bf16[16,8,512]{2,1,0:T(8,128)(2,1)} %bitcast.13), calls=%async_computation.1 | async-start | bytes 262144 | tf_op jit(solution)/shard_map/all_to_all | solution.py:584
  35.7 4.8 %advance.1 = f32[8,16,64,128]{3,2,1,0:T(8,128)} custom-call(f32[8,1024]{1,0:T(8,128)} %get-tuple-element.27.scaled_hbm, f32[8,512]{1,0:T(8,128)} %get-tuple-element.28.key_hbm, f32[8,16]{1,0:T(8,128)} %get-tuple-element.29.decay_hbm, f32[8,16,64,128]{3,2,1,0:T(8,128)} %state_hbm.1), custom_call_target="tpu_custom_call" | custom-call | tf_op jit(solution)/shard_map/advance/pallas_call | solution.py:516
  40.5 3.3 %all-to-all-done.1 = bf16[16,8,512]{2,1,0:T(8,128)(2,1)S(1)} async-done(((bf16[16,8,512]{2,1,0:T(8,128)(2,1)}), bf16[16,8,512]{2,1,0:T(8,128)(2,1)S(1)}, u32[]{:S(2)}, u32[]{:S(2)}) %all-to-all-start.1) | async-done | bytes 131104 | tf_op jit(solution)/shard_map/all_to_all | solution.py:584
  43.8 0.6 %total.1 = bf16[8,512]{1,0:T(8,128)(2,1)} custom-call(s32[1]{0:T(128)} %bitcast.refs_0_.tp_ref, bf16[128,512]{1,0:T(8,128)(2,1)S(1)} %bitcast.18, bf16[8,1024]{1,0:T(8,128)(2,1)S(1)} %get-tuple-element.26.residual_ref), custom_call_target="tpu_custom_call" | custom-call | tf_op jit(solution)/shard_map/total/pallas_call | solution.py:593
Async XLA Ops:
  0.6 10.6 %copy-start.2 = (bf16[8,1024]{1,0:T(8,128)(2,1)S(1)}, bf16[8,1024]{1,0:T(8,128)(2,1)}, u32[]{:S(2)}) copy-start(bf16[8,1024]{1,0:T(8,128)(2,1)} %tokens_ref.1) | copy-start | bytes 49156
  0.7 10.6 %copy-start.3 = (f32[1024]{0:T(1024)S(1)}, f32[1024]{0:T(1024)}, u32[]{:S(2)}) copy-start(f32[1024]{0:T(1024)} %param.48) | copy-start | bytes 12292
  0.7 17.8 %copy-start = (bf16[1,1024,256]{2,1,0:T(8,128)(2,1)S(1)}, bf16[1,1024,256]{2,1,0:T(8,128)(2,1)}, u32[]{:S(2)}) copy-start(bf16[1,1024,256]{2,1,0:T(8,128)(2,1)} %refs_0_.1) | copy-start | bytes 1572868
  0.7 17.9 %copy-start.1 = (bf16[1,1024,256]{2,1,0:T(8,128)(2,1)S(1)}, bf16[1,1024,256]{2,1,0:T(8,128)(2,1)}, u32[]{:S(2)}) copy-start(bf16[1,1024,256]{2,1,0:T(8,128)(2,1)} %refs_1_.3) | copy-start | bytes 1572868
  0.7 27.3 %copy-start.4 = (bf16[1024]{0:T(1024)(128)(2,1)S(1)}, bf16[1024]{0:T(1024)(128)(2,1)}, u32[]{:S(2)}) copy-start(bf16[1024]{0:T(1024)(128)(2,1)} %branch_ref.1) | copy-start | bytes 6148
  6.5 4.8 %collective-permute-start = (bf16[8,1024]{1,0:T(8,128)(2,1)S(1)}, bf16[8,1024]{1,0:T(8,128)(2,1)S(1)}, u32[]{:S(2)}, u32[]{:S(2)}) collective-permute-start(bf16[8,1024]{1,0:T(8,128)(2,1)S(1)} %get-tuple-element.19.own_ref), channel_id=1, source_target_pairs={{0,1},{1,0},{2,3},{3,2},{4,5},{5,4},{6,7},{7,6},{8,9},{9,8},{10,11... | collective-permute-start | bytes 49160 | tf_op jit(solution)/shard_map/ppermute | solution.py:532
  12.1 15.8 %all-to-all-start = ((bf16[8,168,128]{2,1,0:T(8,128)(2,1)}), bf16[8,168,128]{2,1,0:T(8,128)(2,1)S(1)}, u32[]{:S(2)}, u32[]{:S(2)}) async-start(bf16[8,168,128]{2,1,0:T(8,128)(2,1)} %get-tuple-element.21), calls=%async_computation | async-start | bytes 688128 | tf_op jit(solution)/shard_map/all_to_all | solution.py:549
  18.5 9.5 %collective-permute-start.2 = (bf16[1,1024,256]{2,1,0:T(8,128)(2,1)S(1)}, bf16[1,1024,256]{2,1,0:T(8,128)(2,1)S(1)}, u32[]{:S(2)}, u32[]{:S(2)}) collective-permute-start(bf16[1,1024,256]{2,1,0:T(8,128)(2,1)S(1)} %copy-done), channel_id=1, source_target_pairs={{0,2},{2,0},{4,6},{6,4},{8,10},{10,8},{12,14},{14,12},{16,18},{18,... | collective-permute-start | bytes 1572872 | tf_op jit(solution)/shard_map/ppermute | solution.py:553
  18.6 9.4 %collective-permute-start.3 = (bf16[1,1024,256]{2,1,0:T(8,128)(2,1)S(1)}, bf16[1,1024,256]{2,1,0:T(8,128)(2,1)S(1)}, u32[]{:S(2)}, u32[]{:S(2)}) collective-permute-start(bf16[1,1024,256]{2,1,0:T(8,128)(2,1)S(1)} %copy-done.1), channel_id=1, source_target_pairs={{0,2},{2,0},{4,6},{6,4},{8,10},{10,8},{12,14},{14,12},{16,18},{18,... | collective-permute-start | bytes 1572872 | tf_op jit(solution)/shard_map/ppermute | solution.py:553
  19.1 8.9 %collective-permute-start.4 = (bf16[1,256,1024]{2,1,0:T(8,128)(2,1)}, bf16[1,256,1024]{2,1,0:T(8,128)(2,1)S(1)}, u32[]{:S(2)}, u32[]{:S(2)}) collective-permute-start(bf16[1,256,1024]{2,1,0:T(8,128)(2,1)} %refs_5_.1), channel_id=1, source_target_pairs={{0,2},{2,0},{4,6},{6,4},{8,10},{10,8},{12,14},{14,12},{16,18},{18,... | collective-permute-start | bytes 1572872 | tf_op jit(solution)/shard_map/ppermute | solution.py:553
  28.0 1.9 %collective-permute-start.1 = (bf16[8,168,128]{2,1,0:T(8,128)(2,1)S(1)}, bf16[8,168,128]{2,1,0:T(8,128)(2,1)S(1)}, u32[]{:S(2)}, u32[]{:S(2)}) collective-permute-start(bf16[8,168,128]{2,1,0:T(8,128)(2,1)S(1)} %all-to-all-done.got_ref.own_ref), channel_id=1, source_target_pairs={{0,2},{2,0},{4,6},{6,4},{8,10},{10,8},{12,14},{14,12},{16,18},{18,... | collective-permute-start | bytes 1032200 | tf_op jit(solution)/shard_map/ppermute | solution.py:554
  31.0 12.8 %all-to-all-start.1 = ((bf16[16,8,512]{2,1,0:T(8,128)(2,1)}), bf16[16,8,512]{2,1,0:T(8,128)(2,1)S(1)}, u32[]{:S(2)}, u32[]{:S(2)}) async-start(bf16[16,8,512]{2,1,0:T(8,128)(2,1)} %bitcast.13), calls=%async_computation.1 | async-start | bytes 262144 | tf_op jit(solution)/shard_map/all_to_all | solution.py:584

commit v7 on v6

--- a/solution.py
+++ b/solution.py
@@ -149,7 +149,7 @@
         for i in range(2)
     ]
     stores = [copy(buffers[i], results[i], out_sems.at[i]) for i in range(6)]
-    for load in [*small_loads, load_x, load_b, load_c, *state_loads, load_z, load_out]:
+    for load in [*small_loads[:2], load_x, *small_loads[2:], load_b, load_c, *state_loads, load_z, load_out]:
         load.start()
     for load in small_loads:
         load.wait()
@@ -338,10 +338,8 @@
 
 
 def experts_kernel(core_ref, got_ref, branch_ref, *refs, share, seqs, model):
-    gate, up, other_gate, other_up, other_down, down_hbm = refs[:6]
-    result_ref, rows_ref, hidden_ref, scale_ref, wide_ref, down, sem = refs[6:]
-    load = pltpu.make_async_copy(down_hbm, down, sem.at[0])
-    load.start()
+    gate, up, other_gate, other_up, other_down = refs[:5]
+    result_ref, rows_ref, hidden_ref, scale_ref, active_ref, weight_ref, wide_ref = refs[5:]
     chips, total, _ = got_ref.shape
     core = core_ref[0]
     rows = token_rows(got_ref, seqs, model)
@@ -357,16 +355,15 @@
     def weight_of(expert):
         return jnp.sum(jnp.where(lane // 2 == expert, table, 0.0), axis=1, keepdims=True)
 
-    own_active = active(gate, up)
-    other = weight_of(1 - core) * dot(active(other_gate, other_up), other_down[0])
+    active_ref[...] = active(gate, up)
+    weight_ref[...] = jnp.broadcast_to(weight_of(core), weight_ref.shape)
+    result_ref[...] = weight_of(1 - core) * dot(active(other_gate, other_up), other_down[0])
     branch = sigmoid(
         jnp.sum(rows.astype(f32) * branch_ref[...].astype(f32)[None], axis=1, keepdims=True)
     )
     scale_ref[...] = jnp.broadcast_to(branch, scale_ref.shape)
     unfold(got_ref, core, seqs * model // LANES, share, wide_ref)
     hidden_ref[...] = dot(rows, wide_ref[...])
-    load.wait()
-    result_ref[...] = other + weight_of(core) * dot(own_active, down[0])
 
 
 def dense_kernel(
@@ -377,6 +374,9 @@
     rows_ref,
     half_ref,
     scale_ref,
+    active_ref,
+    weight_ref,
+    down_ref,
     out_ref,
     wide_ref,
     *,
@@ -395,7 +395,8 @@
     start += rows // fold_of(rows, share)
     back = down_rows(own_ref, other_ref, core == 0, start, share, rows)
     dense_out = dot(dense[:, :share].astype(bf16), back)
-    result = routed_ref[...] + scale_ref[:, :1] * dense_out
+    own_out = weight_ref[:, :1] * dot(active_ref[...], down_ref[0])
+    result = routed_ref[...] + own_out + scale_ref[:, :1] * dense_out
     half = model // n_tp
     for i in range(chips):
         for q in range(n_tp):
@@ -560,26 +561,27 @@
             sds((chips * seqs, model), bf16),
             sds((chips * seqs, LANES), f32),
             sds((chips * seqs, LANES), f32),
+            sds((chips * seqs, exp_gate.shape[2]), bf16),
+            sds((chips * seqs, LANES), f32),
         ),
-        in_specs=[SMEM] + [VMEM] * 7 + [HBM],
-        out_specs=(VMEM,) * 4,
+        in_specs=[SMEM] + [VMEM] * 7,
+        out_specs=(VMEM,) * 6,
         scratch_shapes=[
             pltpu.VMEM((model, LANES), bf16),
-            pltpu.VMEM(exp_down.shape, bf16),
-            pltpu.SemaphoreType.DMA((1,)),
         ],
         compiler_params=pltpu.CompilerParams(vmem_limit_bytes=12 * MIB),
+        cost_estimate=pl.CostEstimate(flops=10**10, bytes_accessed=10**6, transcendentals=0),
         name="experts",
-    )(core_index, got, branch_gate, exp_gate, exp_up, *other_experts, in_hbm(exp_down))
+    )(core_index, got, branch_gate, exp_gate, exp_up, *other_experts)
     outgoing = pl.pallas_call(
         functools.partial(dense_kernel, share=share, seqs=seqs, n_tp=n_tp),
         out_shape=sds((chips * n_tp * seqs, model // n_tp), bf16),
-        in_specs=[SMEM] + [VMEM] * 6,
+        in_specs=[SMEM] + [VMEM] * 9,
         out_specs=VMEM,
         scratch_shapes=[pltpu.VMEM((model, LANES), bf16)],
         compiler_params=pltpu.CompilerParams(vmem_limit_bytes=8 * MIB),
         name="dense",
-    )(core_index, got, got_other, *dense_inputs)
+    )(core_index, got, got_other, *dense_inputs, exp_down)
     flat_groups = [[ep * n_tp + q for ep in group for q in range(n_tp)] for group in groups]
     parts = lax.all_to_all(
         outgoing,

time: 44.7 us -> 44.1 us (0.987)
  Pallas kernels: 15.1 us -> 13.9 us
  waiting for transfers between devices: 13.8 us -> 14.4 us
    pallas_call x1, Pallas kernels: 1.86 us -> 0.71 us  [body(): pl.pallas_call(functools.partial(experts_kernel, share=share, seqs=seqs,...]
    ppermute x1, waiting for transfers between devices: 0.01 us -> 0.9 us  [body(): got_other = lax.ppermute(got, 'ep', swap)]
  transfers between devices with their start and end apart: 7 -> 7, of which waited for: 3 -> 4; matrix products, arithmetic and copies ran while one was open for 0% -> 0% of each run, Pallas kernels for 15% -> 13%
where the time goes in v7:
time: 44.1 us; the launch traced here: 43.8 us
  starting transfers between devices  14.7 us (33%)
  waiting for transfers between devices  14.4 us (33%)
  Pallas kernels  13.9 us (32%)
  between operations  0.77 us (2%)
    all_to_all x1, waiting for transfers between devices, body(): lax.all_to_all(spread, 'ep', split_axis=0, concat_axis=0, tiled=True, axi...  8.8 us
    all_to_all x1, starting transfers between devices, body(): lax.all_to_all(spread, 'ep', split_axis=0, concat_axis=0, tiled=True, axi...  6.36 us
    pallas_call x1, Pallas kernels, body(): pl.pallas_call(functools.partial(mixer_kernel, n_tp=n_tp, held=len(held))...  5.74 us
    pallas_call x1, Pallas kernels, body(): pl.pallas_call(advance_kernel, out_shape=sds(ssm_state.shape, f32), in_sp...  4.82 us
    all_to_all x1, starting transfers between devices, body(): lax.all_to_all(outgoing, ('ep', 'tp'), split_axis=0, concat_axis=0, tiled...  4.67 us
    ppermute x1, starting transfers between devices, body(): other = lax.ppermute(part, 'tp', [(0, 1), (1, 0)])  3.03 us
    all_to_all x1, waiting for transfers between devices, body(): lax.all_to_all(outgoing, ('ep', 'tp'), split_axis=0, concat_axis=0, tiled...  2.97 us
    ppermute x1, waiting for transfers between devices, body(): other = lax.ppermute(part, 'tp', [(0, 1), (1, 0)])  1.72 us
  transfers between devices with their start and end apart: 7, of which 4 were waited for; matrix products, arithmetic and copies ran while one was open for 0% of the time, Pallas kernels for 13%

profile of v7, /device:TPU:0, one launch (start us, length us, event | category | flops | bytes accessed | tf_op | source)
XLA Modules:
  0.0 43.8 jit_solution(13229634308211417598)
XLA Ops:
  0.6 0.0 copy-start.1
  0.7 0.0 copy-start.2
  0.7 0.0 copy-start.3
  0.7 0.0 copy-start.4
  0.7 0.0 copy-start
  0.7 0.0 copy-start.5
  0.7 5.7 %mixer.1 = (bf16[8,1024]{1,0:T(8,128)(2,1)S(1)}, bf16[8,104,128]{2,1,0:T(8,128)(2,1)S(1)}, f32[8,1024]{1,0:T(8,128)}, f32[8,512]{1,0:T(8,128)}, f32[8,16]{1,0:T(...) custom-call(s32[1]{0:T(128)} %bitcast.refs_0_.tp_ref, ...), custom_call_target="tpu_custom_call" | custom-call | tf_op jit(solution)/shard_map/mixer/pallas_call | solution.py:497
  6.5 3.0 %collective-permute-start = (bf16[8,1024]{1,0:T(8,128)(2,1)S(1)}, bf16[8,1024]{1,0:T(8,128)(2,1)S(1)}, u32[]{:S(2)}, u32[]{:S(2)}) collective-permute-start(bf16[8,1024]{1,0:T(8,128)(2,1)S(1)} %get-tuple-element.21.own_ref), channel_id=1, source_target_pairs={{0,1},{1,0},{2,3},{3,2},{4,5},{5,4},{6,7},{7,6},{8,9},{9,8},{10,11... | collective-permute-start | bytes 49160 | tf_op jit(solution)/shard_map/ppermute | solution.py:533
  9.5 1.7 %collective-permute-done.other_ref = bf16[8,1024]{1,0:T(8,128)(2,1)S(1)} collective-permute-done((bf16[8,1024]{1,0:T(8,128)(2,1)S(1)}, bf16[8,1024]{1,0:T(8,128)(2,1)S(1)}, u32[]{:S(2)}, u32[]{:S(2)}) %collective-permute-start) | collective-permute-done | bytes 16416 | tf_op jit(solution)/shard_map/ppermute | solution.py:533
  11.2 0.0 copy-done.1
  11.2 0.0 copy-done.2
  11.2 0.8 %norm.1 = (bf16[8,168,128]{2,1,0:T(8,128)(2,1)}, bf16[8,1024]{1,0:T(8,128)(2,1)S(1)}) custom-call(bf16[8,1024]{1,0:T(8,128)(2,1)S(1)} %copy-done.1, bf16[8,1024]{1,0:T(8,128)(2,1)S(1)} %get-tuple-element.21.own_ref, bf16[8,1024]{1,0:T(8,128)(2,1)S(1)} %collective-permute-done.other_ref, f32[1,1024]{1,0:T(1,128)S(1)} %bitcast.19, ...), custom_call_target="tpu_custom_call" | custom-call | tf_op jit(solution)/shard_map/norm/pallas_call | solution.py:542
  12.1 6.4 %all-to-all-start = ((bf16[8,168,128]{2,1,0:T(8,128)(2,1)}), bf16[8,168,128]{2,1,0:T(8,128)(2,1)S(1)}, u32[]{:S(2)}, u32[]{:S(2)}) async-start(bf16[8,168,128]{2,1,0:T(8,128)(2,1)} %get-tuple-element.23), calls=%async_computation | async-start | bytes 688128 | tf_op jit(solution)/shard_map/all_to_all | solution.py:550
  18.4 0.0 copy-done.3
  18.4 0.1 collective-permute-start.2
  18.5 0.0 copy-done.4
  18.5 0.5 %collective-permute-start.3 = (bf16[1,1024,256]{2,1,0:T(8,128)(2,1)S(1)}, bf16[1,1024,256]{2,1,0:T(8,128)(2,1)S(1)}, u32[]{:S(2)}, u32[]{:S(2)}) collective-permute-start(bf16[1,1024,256]{2,1,0:T(8,128)(2,1)S(1)} %copy-done.4), channel_id=1, source_target_pairs={{0,2},{2,0},{4,6},{6,4},{8,10},{10,8},{12,14},{14,12},{16,18},{18,... | collective-permute-start | bytes 1572872 | tf_op jit(solution)/shard_map/ppermute | solution.py:554
  19.0 0.0 copy-done
  19.0 0.1 collective-permute-start.4
  19.1 8.8 %all-to-all-done.got_ref.own_ref = bf16[8,168,128]{2,1,0:T(8,128)(2,1)S(1)} async-done(((bf16[8,168,128]{2,1,0:T(8,128)(2,1)}), bf16[8,168,128]{2,1,0:T(8,128)(2,1)S(1)}, u32[]{:S(2)}, u32[]{:S(2)}) %all-to-all-start) | async-done | bytes 344096 | tf_op jit(solution)/shard_map/all_to_all | solution.py:550
  27.9 0.0 collective-permute-start.1
  27.9 0.0 collective-permute-done.2.refs_2_
  27.9 0.0 collective-permute-done.3.refs_3_
  27.9 0.0 collective-permute-done.4.refs_4_
  27.9 0.0 copy-done.5
  27.9 0.7 %experts.1 = (f32[64,1024]{1,0:T(8,128)S(1)}, bf16[64,1024]{1,0:T(8,128)(2,1)S(1)}, f32[64,128]{1,0:T(8,128)S(1)}, f32[64,128]{1,0:T(8,128)S(1)}, bf16[64,256]{1,0:T(8,128)(2,1)S(1)}, /*index=5*/f32[64,128]{1,0:T(8,128)S(1)}) custom-call(s32[1]{0:T(128)} %bitcast.1.core_ref, bf16[8,168,128]{2,1,0:T(8,128)(2,1)S(1)} %all-to-all-done.got_ref.own_ref, ...), custom_call_target="tpu_custom_call" | custom-call | flops 10000000000 | bytes 1000000 | tf_op jit(solution)/shard_map/experts/pallas_call | solution.py:557
  28.6 0.9 %collective-permute-done.1.other_ref = bf16[8,168,128]{2,1,0:T(8,128)(2,1)S(1)} collective-permute-done((bf16[8,168,128]{2,1,0:T(8,128)(2,1)S(1)}, bf16[8,168,128]{2,1,0:T(8,128)(2,1)S(1)}, u32[]{:S(2)}, u32[]{:S(2)}) %collective-permute-start.1) | collective-permute-done | bytes 344096 | tf_op jit(solution)/shard_map/ppermute | solution.py:555
  29.5 1.2 %dense.1 = bf16[128,512]{1,0:T(8,128)(2,1)} custom-call(s32[1]{0:T(128)} %bitcast.1.core_ref, bf16[8,168,128]{2,1,0:T(8,128)(2,1)S(1)} %all-to-all-done.got_ref.own_ref, bf16[8,168,128]{2,1,0:T(8,128)(2,1)S(1)} %collective-permute-done.1.other_ref, f32[64,1024]{1,0:T(8,128)S(1)} %get-tuple-element.24.routed_ref, ...), custom_call_target="tpu_custom_call" | custom-call | tf_op jit(solution)/shard_map/dense/pallas_call | solution.py:576
  30.7 4.7 %all-to-all-start.1 = ((bf16[16,8,512]{2,1,0:T(8,128)(2,1)}), bf16[16,8,512]{2,1,0:T(8,128)(2,1)S(1)}, u32[]{:S(2)}, u32[]{:S(2)}) async-start(bf16[16,8,512]{2,1,0:T(8,128)(2,1)} %bitcast.13), calls=%async_computation.1 | async-start | bytes 262144 | tf_op jit(solution)/shard_map/all_to_all | solution.py:586
  35.4 4.8 %advance.1 = f32[8,16,64,128]{3,2,1,0:T(8,128)} custom-call(f32[8,1024]{1,0:T(8,128)} %get-tuple-element.31.scaled_hbm, f32[8,512]{1,0:T(8,128)} %get-tuple-element.32.key_hbm, f32[8,16]{1,0:T(8,128)} %get-tuple-element.33.decay_hbm, f32[8,16,64,128]{3,2,1,0:T(8,128)} %state_hbm.1), custom_call_target="tpu_custom_call" | custom-call | tf_op jit(solution)/shard_map/advance/pallas_call | solution.py:517
  40.2 3.0 %all-to-all-done.1 = bf16[16,8,512]{2,1,0:T(8,128)(2,1)S(1)} async-done(((bf16[16,8,512]{2,1,0:T(8,128)(2,1)}), bf16[16,8,512]{2,1,0:T(8,128)(2,1)S(1)}, u32[]{:S(2)}, u32[]{:S(2)}) %all-to-all-start.1) | async-done | bytes 131104 | tf_op jit(solution)/shard_map/all_to_all | solution.py:586
  43.2 0.6 %total.1 = bf16[8,512]{1,0:T(8,128)(2,1)} custom-call(s32[1]{0:T(128)} %bitcast.refs_0_.tp_ref, bf16[128,512]{1,0:T(8,128)(2,1)S(1)} %bitcast.18, bf16[8,1024]{1,0:T(8,128)(2,1)S(1)} %get-tuple-element.30.residual_ref), custom_call_target="tpu_custom_call" | custom-call | tf_op jit(solution)/shard_map/total/pallas_call | solution.py:595
Async XLA Ops:
  0.6 10.6 %copy-start.1 = (bf16[8,1024]{1,0:T(8,128)(2,1)S(1)}, bf16[8,1024]{1,0:T(8,128)(2,1)}, u32[]{:S(2)}) copy-start(bf16[8,1024]{1,0:T(8,128)(2,1)} %tokens_ref.1) | copy-start | bytes 49156
  0.7 10.6 %copy-start.2 = (f32[1024]{0:T(1024)S(1)}, f32[1024]{0:T(1024)}, u32[]{:S(2)}) copy-start(f32[1024]{0:T(1024)} %param.48) | copy-start | bytes 12292
  0.7 17.8 %copy-start.3 = (bf16[1,1024,256]{2,1,0:T(8,128)(2,1)S(1)}, bf16[1,1024,256]{2,1,0:T(8,128)(2,1)}, u32[]{:S(2)}) copy-start(bf16[1,1024,256]{2,1,0:T(8,128)(2,1)} %refs_0_.1) | copy-start | bytes 1572868
  0.7 17.8 %copy-start.4 = (bf16[1,1024,256]{2,1,0:T(8,128)(2,1)S(1)}, bf16[1,1024,256]{2,1,0:T(8,128)(2,1)}, u32[]{:S(2)}) copy-start(bf16[1,1024,256]{2,1,0:T(8,128)(2,1)} %refs_1_.3) | copy-start | bytes 1572868
  0.7 18.3 %copy-start = (bf16[1,256,1024]{2,1,0:T(8,128)(2,1)S(1)}, bf16[1,256,1024]{2,1,0:T(8,128)(2,1)}, u32[]{:S(2)}) copy-start(bf16[1,256,1024]{2,1,0:T(8,128)(2,1)} %down_ref.1) | copy-start | bytes 1572868
  0.7 27.2 %copy-start.5 = (bf16[1024]{0:T(1024)(128)(2,1)S(1)}, bf16[1024]{0:T(1024)(128)(2,1)}, u32[]{:S(2)}) copy-start(bf16[1024]{0:T(1024)(128)(2,1)} %branch_ref.1) | copy-start | bytes 6148
  6.5 4.8 %collective-permute-start = (bf16[8,1024]{1,0:T(8,128)(2,1)S(1)}, bf16[8,1024]{1,0:T(8,128)(2,1)S(1)}, u32[]{:S(2)}, u32[]{:S(2)}) collective-permute-start(bf16[8,1024]{1,0:T(8,128)(2,1)S(1)} %get-tuple-element.21.own_ref), channel_id=1, source_target_pairs={{0,1},{1,0},{2,3},{3,2},{4,5},{5,4},{6,7},{7,6},{8,9},{9,8},{10,11... | collective-permute-start | bytes 49160 | tf_op jit(solution)/shard_map/ppermute | solution.py:533
  12.1 15.8 %all-to-all-start = ((bf16[8,168,128]{2,1,0:T(8,128)(2,1)}), bf16[8,168,128]{2,1,0:T(8,128)(2,1)S(1)}, u32[]{:S(2)}, u32[]{:S(2)}) async-start(bf16[8,168,128]{2,1,0:T(8,128)(2,1)} %get-tuple-element.23), calls=%async_computation | async-start | bytes 688128 | tf_op jit(solution)/shard_map/all_to_all | solution.py:550
  18.4 9.5 %collective-permute-start.2 = (bf16[1,1024,256]{2,1,0:T(8,128)(2,1)S(1)}, bf16[1,1024,256]{2,1,0:T(8,128)(2,1)S(1)}, u32[]{:S(2)}, u32[]{:S(2)}) collective-permute-start(bf16[1,1024,256]{2,1,0:T(8,128)(2,1)S(1)} %copy-done.3), channel_id=1, source_target_pairs={{0,2},{2,0},{4,6},{6,4},{8,10},{10,8},{12,14},{14,12},{16,18},{18,... | collective-permute-start | bytes 1572872 | tf_op jit(solution)/shard_map/ppermute | solution.py:554
  18.5 9.4 %collective-permute-start.3 = (bf16[1,1024,256]{2,1,0:T(8,128)(2,1)S(1)}, bf16[1,1024,256]{2,1,0:T(8,128)(2,1)S(1)}, u32[]{:S(2)}, u32[]{:S(2)}) collective-permute-start(bf16[1,1024,256]{2,1,0:T(8,128)(2,1)S(1)} %copy-done.4), channel_id=1, source_target_pairs={{0,2},{2,0},{4,6},{6,4},{8,10},{10,8},{12,14},{14,12},{16,18},{18,... | collective-permute-start | bytes 1572872 | tf_op jit(solution)/shard_map/ppermute | solution.py:554
  19.0 8.9 %collective-permute-start.4 = (bf16[1,256,1024]{2,1,0:T(8,128)(2,1)S(1)}, bf16[1,256,1024]{2,1,0:T(8,128)(2,1)S(1)}, u32[]{:S(2)}, u32[]{:S(2)}) collective-permute-start(bf16[1,256,1024]{2,1,0:T(8,128)(2,1)S(1)} %copy-done), channel_id=1, source_target_pairs={{0,2},{2,0},{4,6},{6,4},{8,10},{10,8},{12,14},{14,12},{16,18},{18,... | collective-permute-start | bytes 1572872 | tf_op jit(solution)/shard_map/ppermute | solution.py:554
  27.9 1.7 %collective-permute-start.1 = (bf16[8,168,128]{2,1,0:T(8,128)(2,1)S(1)}, bf16[8,168,128]{2,1,0:T(8,128)(2,1)S(1)}, u32[]{:S(2)}, u32[]{:S(2)}) collective-permute-start(bf16[8,168,128]{2,1,0:T(8,128)(2,1)S(1)} %all-to-all-done.got_ref.own_ref), channel_id=1, source_target_pairs={{0,2},{2,0},{4,6},{6,4},{8,10},{10,8},{12,14},{14,12},{16,18},{18,... | collective-permute-start | bytes 1032200 | tf_op jit(solution)/shard_map/ppermute | solution.py:555
  30.7 12.5 %all-to-all-start.1 = ((bf16[16,8,512]{2,1,0:T(8,128)(2,1)}), bf16[16,8,512]{2,1,0:T(8,128)(2,1)S(1)}, u32[]{:S(2)}, u32[]{:S(2)}) async-start(bf16[16,8,512]{2,1,0:T(8,128)(2,1)} %bitcast.13), calls=%async_computation.1 | async-start | bytes 262144 | tf_op jit(solution)/shard_map/all_to_all | solution.py:586
